TPU v7x, 512 devices: a whole 4x4x16 slice. The times are simulated.
512 devices in a mesh: ep: 32 (over z, core), tp: 16 (over y, x).
Axes of the slice: x: 4, y: 4, z: 16, core: 2. Of those that a mesh axis runs over, the one named last changes fastest.
Arguments:
- receptance: bfloat16 [8192, 2048], P('ep', 'tp'), may hold values from -6 to 6
- key_in: bfloat16 [8192, 2048], P('ep', 'tp'), may hold values from -6 to 6
- value_in: bfloat16 [8192, 2048], P('ep', 'tp'), may hold values from -6 to 6
- decay_in: bfloat16 [8192, 2048], P('ep', 'tp'), may hold values from -16 to 2
- rate_in: bfloat16 [8192, 2048], P('ep', 'tp'), may hold values from -12 to 4
- norm_gain: float32 [2048], P('tp'), may hold values from 0.1 to 1.9
- out_weight: bfloat16 [2048, 4096], P('tp'), may hold values from -0.125 to 0.125
- moe_in: bfloat16 [4096, 4096], P('ep'), may hold values from -6 to 6
- ffn_gain: float32 [4096], replicated, may hold values from 0.1 to 1.9
- routes: int32 [4096, 4], P('ep'), may hold values from 0 to 31, all different within a row; in each aligned block of 128 rows (0 to 127, 128 to 255, ...) at most 20 rows name the same one
- route_weights: float32 [4096, 4], P('ep'), may hold values from 0.2 to 1
- gate_weight: bfloat16 [32, 4096, 1024], P('ep', None, 'tp'), may hold values from -0.09375 to 0.09375
- up_weight: bfloat16 [32, 4096, 1024], P('ep', None, 'tp'), may hold values from -0.09375 to 0.09375
- down_weight: bfloat16 [32, 1024, 4096], P('ep', None, 'tp'), may hold values from -0.1875 to 0.1875
Outputs:
- mixer_out: bfloat16 [8192, 4096], P(('ep', 'tp'))
- moe_out: bfloat16 [4096, 4096], P('ep', 'tp')
Inputs may be any that keep to these rules, and one draw needn't show every extreme that they name: `routes`: A row names 4 different experts. Among the 128 rows that one index of ep holds, no expert is named by more than 20 rows, and in every draw some expert is named by exactly 20 of them.
All inputs are finite; a program needn't handle non-finite values.
Results may differ from a plain program's by a relative error of at most 0.025.
Values may be sent and summed in bfloat16 or wider, within the bound.
No kernel may reach another device: no remote copies, remote signals or barrier semaphores. Data moves between devices by JAX's collectives and lax.ppermute only.
A program may use at most 64 MiB of HBM per device.

v0:
```python
import jax
import jax.numpy as jnp
from jax import lax
from jax.sharding import Mesh
from jax.sharding import PartitionSpec as P

HD = 64
BLOCK = 64
EP = ("ep_0", "ep_1")
EP_TP = ("ep_0", "ep_1", "tp")


EXACT_MATMUL = lax.Precision.HIGHEST


def nothing_yet(shard, identity):
    return jax.tree.map(
        lambda a, e: jnp.broadcast_to(jnp.asarray(e, a.dtype), a.shape), shard, identity
    )


def collected_together(shard, axis):
    leaves = jax.tree.leaves(shard)
    turns = sorted(range(len(leaves)), key=lambda k: -leaves[k].size)
    width = (1, *leaves[turns[0]].shape)[-1]
    lines = [
        jnp.pad(leaves[k].reshape(-1), (0, -leaves[k].size % width)).reshape(-1, width)
        for k in turns
    ]
    both, at, found = (lax.all_gather(jnp.concatenate(lines), axis), 0, {})
    for k, line in zip(turns, lines):
        slab = both[:, at : at + len(line)].reshape(len(both), -1)
        found[k] = slab[:, : leaves[k].size].reshape(-1, *leaves[k].shape)
        at += len(line)
    numbers = iter(range(len(leaves)))
    return jax.tree.map(lambda _: found[next(numbers)], shard)


def entering(shard, axes, combine, identity):
    before = start = nothing_yet(shard, identity)
    subtotal = shard
    for axis in reversed(axes):
        peers, position = (lax.axis_size(axis), lax.axis_index(axis))
        pieces = collected_together(
            jax.tree.map(
                lambda part, kind: part.astype(kind), subtotal, (jnp.bfloat16, jnp.bfloat16)
            ),
            axis,
        )
        inside, subtotal = (start, start)
        for k in range(peers):
            passed = k < position
            subtotal = combine(
                subtotal, jax.tree.map(lambda part, own: part[k].astype(own.dtype), pieces, shard)
            )
            inside = jax.tree.map(lambda new, old: jnp.where(passed, new, old), subtotal, inside)
        before = combine(inside, before)
    return before


def in_blocks(shard, dim, peers):
    before, after = (shard.shape[:dim], shard.shape[dim + 1 :])
    return jnp.moveaxis(shard.reshape(*before, peers, -1, *after), dim, 0)


def summed_on_arrival(shard, axis, dim):
    peers = lax.axis_size(axis)
    tiles = lax.all_to_all(in_blocks(shard, dim, peers), axis, 0, 0, tiled=True)
    return jnp.sum(tiles.astype(jnp.float32), axis=0)


def joined_along(tiles, dim):
    tiles = jnp.moveaxis(tiles, 0, dim)
    lengths = tiles.shape
    return tiles.reshape(*lengths[:dim], lengths[dim] * lengths[dim + 1], *lengths[dim + 2 :])


def sent_to_all(shard, axis):
    copies = jnp.broadcast_to(shard, (lax.axis_size(axis), *shard.shape))
    return lax.all_to_all(copies, axis, split_axis=0, concat_axis=0, tiled=True)


def gather_directly(shard, axis, dim):
    return joined_along(sent_to_all(shard, axis), dim)


def einsum_exact(form, left, right):
    return jnp.einsum(form, left, right, precision=EXACT_MATMUL)


def block_tables(receptance, key_in, value_in, decay_in, rate_in):
    token_count, columns = receptance.shape
    head_count = columns // HD
    block_count = token_count // BLOCK

    def to_blocks(array):
        return (
            array.astype(jnp.float32)
            .reshape(block_count, BLOCK, head_count, HD)
            .transpose(2, 0, 1, 3)
        )

    readout = to_blocks(receptance)
    key_rows = to_blocks(key_in)
    value_rows = to_blocks(value_in)
    log_decay = -jnp.exp(-jax.nn.softplus(-to_blocks(decay_in)) - 0.5)
    learn_rate = jax.nn.sigmoid(to_blocks(rate_in))
    unit_key = key_rows / jnp.sqrt(jnp.sum(key_rows * key_rows, axis=-1, keepdims=True) + 1.0)
    inclusive = jnp.cumsum(log_decay, axis=2)
    exclusive = inclusive - log_decay
    block_total = inclusive[:, :, -1:, :]
    probe = -unit_key * jnp.exp(exclusive)
    removal = unit_key * learn_rate
    written = key_rows * learn_rate
    removal_back = removal * jnp.exp(-inclusive)
    written_back = written * jnp.exp(-inclusive)
    readout_scaled = readout * jnp.exp(inclusive)
    removal_tail = removal * jnp.exp(block_total - inclusive)
    written_tail = written * jnp.exp(block_total - inclusive)
    strict = jnp.tril(jnp.ones((BLOCK, BLOCK), jnp.float32), -1)
    closed = jnp.tril(jnp.ones((BLOCK, BLOCK), jnp.float32))
    lower = einsum_exact("hbck,hbsk->hbcs", probe, removal_back) * strict
    lower_write = einsum_exact("hbck,hbsk->hbcs", probe, written_back) * strict
    reach = einsum_exact("hbck,hbsk->hbcs", readout_scaled, removal_back) * closed
    reach_write = einsum_exact("hbck,hbsk->hbcs", readout_scaled, written_back) * closed
    inverse = jnp.eye(BLOCK, dtype=jnp.float32) + lower
    power = lower
    for doubling in range(BLOCK.bit_length() - 2):
        power = einsum_exact("hbcs,hbst->hbct", power, power)
        inverse = inverse + einsum_exact("hbcs,hbst->hbct", inverse, power)
    solved_probe = einsum_exact("hbcs,hbsk->hbck", inverse, probe)
    solved_values = einsum_exact(
        "hbcs,hbsv->hbcv", inverse, einsum_exact("hbcs,hbsv->hbcv", lower_write, value_rows)
    )
    transition = jnp.exp(block_total[:, :, 0, :])[..., None] * jnp.eye(
        HD, dtype=jnp.float32
    ) + einsum_exact("hbck,hbcj->hbkj", removal_tail, solved_probe)
    increment = einsum_exact("hbck,hbcv->hbkv", removal_tail, solved_values) + einsum_exact(
        "hbck,hbcv->hbkv", written_tail, value_rows
    )
    read_state = readout_scaled + einsum_exact("hbcs,hbsk->hbck", reach, solved_probe)
    local_out = einsum_exact("hbcs,hbsv->hbcv", reach, solved_values) + einsum_exact(
        "hbcs,hbsv->hbcv", reach_write, value_rows
    )
    return (transition, increment, read_state, local_out)


def compose(preceding_part, following_part):
    return (
        einsum_exact("quc,qcd->qud", following_part[0], preceding_part[0]),
        einsum_exact("quc,qcd->qud", following_part[0], preceding_part[1]) + following_part[1],
    )


def mixer_half(receptance, key_in, value_in, decay_in, rate_in, norm_gain, out_weight):
    transition, increment, read_state, local_out = block_tables(
        receptance, key_in, value_in, decay_in, rate_in
    )
    head_count = transition.shape[0]
    identity = jnp.broadcast_to(jnp.eye(HD, dtype=jnp.float32), (head_count, HD, HD))
    nothing = jnp.zeros((head_count, HD, HD), jnp.float32)

    def advance(passed_state, pieces):
        return (compose(passed_state, pieces), passed_state)

    (device_map, device_add), (entry_map, entry_add) = lax.scan(
        advance,
        (identity, nothing),
        (jnp.moveaxis(transition, 1, 0), jnp.moveaxis(increment, 1, 0)),
    )
    prior_map, prior_state = entering((device_map, device_add), EP, compose, (identity, nothing))
    entry_state = einsum_exact("bhkj,hjv->bhkv", entry_map, prior_state) + entry_add
    heads_out = einsum_exact("hbck,bhkv->hbcv", read_state, entry_state) + local_out
    center = heads_out - jnp.mean(heads_out, axis=-1, keepdims=True)
    spread = jnp.mean(center * center, axis=-1, keepdims=True)
    normed = center * lax.rsqrt(spread + 1.0) * norm_gain.reshape(head_count, 1, 1, HD)
    mixed = normed.transpose(1, 2, 0, 3).reshape(receptance.shape).astype(jnp.bfloat16)
    product = jnp.dot(mixed, out_weight, preferred_element_type=jnp.float32).astype(jnp.bfloat16)
    product = lax.optimization_barrier(product)
    return summed_on_arrival(product.astype(jnp.float32).astype(jnp.bfloat16), "tp", 0).astype(
        jnp.bfloat16
    )


def expert_half(moe_in, ffn_gain, routes, route_weights, gate_weight, up_weight, down_weight):
    row_count, feature_count = moe_in.shape
    choose_count = routes.shape[1]
    local_experts = gate_weight.shape[0]
    ep_count = lax.axis_size(EP)
    expert_count = local_experts * ep_count
    capacity = 5 * row_count * choose_count // (4 * expert_count)
    row_values = moe_in.astype(jnp.float32)
    scaled = (
        row_values
        * lax.rsqrt(jnp.mean(row_values * row_values, axis=-1, keepdims=True) + 1.0)
        * ffn_gain
    )
    normed_rows = scaled.astype(jnp.bfloat16)
    pairs = routes.reshape(-1)
    pair_count = pairs.shape[0]
    onehot = (pairs[:, None] == jnp.arange(expert_count, dtype=jnp.int32)[None, :]).astype(
        jnp.int32
    )
    slot_rank = jnp.sum((jnp.cumsum(onehot, axis=0) - onehot) * onehot, axis=1)
    position = pairs * capacity + slot_rank
    source = (
        jnp.zeros((expert_count * capacity,), jnp.int32)
        .at[position]
        .set(jnp.arange(pair_count, dtype=jnp.int32) // choose_count)
    )
    filled = jnp.zeros((expert_count * capacity,), jnp.bool_).at[position].set(True)
    outgoing = jnp.where(filled[:, None], normed_rows[source], jnp.zeros((), jnp.bfloat16))
    part_width = feature_count // lax.axis_size("tp")
    piece = lax.dynamic_slice_in_dim(outgoing, lax.axis_index("tp") * part_width, part_width, 1)
    arrived = lax.all_to_all(piece, EP, split_axis=0, concat_axis=0, tiled=True)
    arrived = arrived.reshape(ep_count, local_experts, capacity, part_width)
    rows_piece = lax.all_gather(arrived, "tp", axis=3, tiled=True)
    gate = jnp.einsum("secn,enf->secf", rows_piece, gate_weight, preferred_element_type=jnp.float32)
    up_part = jnp.einsum(
        "secn,enf->secf", rows_piece, up_weight, preferred_element_type=jnp.float32
    )
    hidden = (jax.nn.silu(gate) * up_part).astype(jnp.bfloat16)
    result = jnp.einsum(
        "secf,efd->secd",
        gather_directly(hidden, "tp", 3),
        down_weight,
        preferred_element_type=jnp.float32,
    )
    result = result.astype(jnp.bfloat16).reshape(
        ep_count * local_experts * capacity, down_weight.shape[2]
    )
    returned = lax.all_to_all(result, EP, split_axis=0, concat_axis=0, tiled=True)
    per_pair = (
        returned[position]
        .astype(jnp.float32)
        .reshape(row_count, choose_count, down_weight.shape[2])
    )
    portion = route_weights / jnp.sum(route_weights, axis=-1, keepdims=True)
    return jnp.sum(portion[:, :, None] * per_pair, axis=1).astype(jnp.bfloat16)


def local(
    receptance,
    key_in,
    value_in,
    decay_in,
    rate_in,
    norm_gain,
    out_weight,
    moe_in,
    ffn_gain,
    routes,
    route_weights,
    gate_weight,
    up_weight,
    down_weight,
):
    mixer_out = mixer_half(receptance, key_in, value_in, decay_in, rate_in, norm_gain, out_weight)
    moe_out = expert_half(
        moe_in, ffn_gain, routes, route_weights, gate_weight, up_weight, down_weight
    )
    return (mixer_out, moe_out)


def solution(mesh):
    finer = Mesh(mesh.devices.reshape(16, 2, mesh.shape["tp"]), ("ep_0", "ep_1", "tp"))
    placed = (
        P(EP, "tp"),
        P(EP, "tp"),
        P(EP, "tp"),
        P(EP, "tp"),
        P(EP, "tp"),
        P("tp"),
        P("tp", None),
        P(EP, None),
        P(),
        P(EP, None),
        P(EP, None),
        P(EP, None, "tp"),
        P(EP, None, "tp"),
        P(EP, None, "tp"),
    )
    return jax.shard_map(
        local, mesh=finer, in_specs=placed, out_specs=(P(EP_TP, None), P(EP, "tp")), check_vma=False
    )
```

profile of v0, /device:TPU:1, one launch (start us, length us, event | category | flops | bytes accessed | tf_op | source)
XLA Modules:
  0.0 263.4 jit_solution(5894849103748729832)
XLA Ops:
  10.8 2.4 scatter_custom_fusion.1
  13.2 1.5 fusion.11
  14.8 1.6 fusion.13
  16.3 5.4 %gather_fusion = bf16[640,4096]{1,0:T(8,128)(2,1)} fusion(bf16[128,4096]{1,0:T(8,128)(2,1)S(1)} %fusion.13, s32[1024]{0:T(1024)S(1)} %pad_clamp_fusion.1), kind=kCustom, calls=%fused_computation | custom fusion | bytes 10488320 | tf_op jit(solution)/shard_map/gather | solution.py:212
  21.7 2.4 scatter_custom_fusion
  26.1 16.7 %all-to-all-start.1 = ((bf16[32,20,256]{2,1,0:T(8,128)(2,1)}), bf16[32,20,256]{2,1,0:T(8,128)(2,1)S(1)}, u32[]{:S(2)}, u32[]{:S(2)}) async-start(bf16[32,20,256]{2,1,0:T(8,128)(2,1)} %all_to_all.19), calls=%async_computation.1 | async-start | bytes 786432 | tf_op jit(solution)/shard_map/all_to_all | solution.py:215
  45.4 1.5 convolution_multiply_fusion.1
  51.1 1.3 fusion.47
  55.4 15.2 %all-to-all-done.1 = bf16[32,20,256]{2,1,0:T(8,128)(2,1)S(1)} async-done(((bf16[32,20,256]{2,1,0:T(8,128)(2,1)}), bf16[32,20,256]{2,1,0:T(8,128)(2,1)S(1)}, u32[]{:S(2)}, u32[]{:S(2)}) %all-to-all-start.1) | async-done | bytes 327712 | tf_op jit(solution)/shard_map/all_to_all | solution.py:215
  71.5 7.2 %while.17 = (s32[]{:T(128)}, f32[2,64,64]{2,1,0:T(8,128)S(1)}, f32[2,64,64]{2,1,0:T(8,128)S(1)}, f32[4,2,64,64]{3,2,1,0:T(8,128)}, f32[4,2,64,64]{2,3,1,0:T(8,12...) while((s32[]{:T(128)}, f32[2,64,64]{2,1,0:T(8,128)S(1)}, ...), condition=%wide.region_3.4_spmd.clone, body=%wide.region_2.3_spmd.clone.sunk | while | flops 12607491 | bytes 854124 | solution.py:166
  79.0 2.2 all-gather
  81.9 26.7 %all-gather.1 = bf16[4096,64]{1,0:T(8,128)(2,1)S(1)} all-gather(bf16[256,64]{1,0:T(8,128)(2,1)S(1)} %pad_maximum_fusion.1), channel_id=3, replica_groups=mesh['ep_0'=16,'ep_1'=2,'tp'=16] {'ep_0'}, dimensions={0}, use_global_device_ids=true | all-gather | bytes 557056 | tf_op jit(solution)/shard_map/all_gather | solution.py:30
  115.3 1.3 convolution_multiply_fusion
  116.7 22.8 %all-gather.5.cloned.1.call-done = bf16[32,20,4096]{2,0,1:T(8,128)(2,1)} async-done(((bf16[32,20,256]{2,0,1:T(8,128)(2,1)}), bf16[32,20,4096]{2,0,1:T(8,128)(2,1)}) %all-gather.5.cloned.1.call-update) | async-done | bytes 5242896 | tf_op jit(solution)/shard_map/all_gather | solution.py:217
  139.4 4.2 %convolution_bitcast_fusion.1 = f32[32,1,20,64]{3,0,2,1:T(8,128)S(1)} fusion(bf16[32,20,4096]{2,0,1:T(8,128)(2,1)} %all-gather.5.cloned.1.call-done, bf16[1,4096,64]{1,2,0:T(8,128)(2,1)} %param.27), kind=kOutput, calls=%fused_computation.33 | convolution fusion | flops 335544320 | bytes 5931008 | tf_op jit(solution)/shard_map/secn,enf->secf/dot_general | solution.py:218
  143.7 1.5 fusion.20
  145.2 2.0 broadcast_bitcast_fusion
  147.3 5.2 %reshape.393 = bf16[16,2,20480]{2,1,0:T(2,128)(2,1)} reshape(bf16[16,1,20,32,64]{4,3,2,1,0:T(8,128)(2,1)} %broadcast_bitcast_fusion) | data formatting | bytes 2621440
  152.4 4.7 %all-to-all-start.2 = ((bf16[16,2,20480]{2,1,0:T(2,128)(2,1)}), bf16[16,2,20480]{2,1,0:T(2,128)(2,1)S(1)}, u32[]{:S(2)}, u32[]{:S(2)}) async-start(bf16[16,2,20480]{2,1,0:T(2,128)(2,1)} %reshape.393), calls=%async_computation.2 | async-start | bytes 2621440 | tf_op jit(solution)/shard_map/all_to_all | solution.py:80
  157.1 1.3 fusion.95
  159.0 2.0 convolution_convert_fusion
  161.0 13.8 %all-to-all-done.2 = bf16[16,2,20480]{2,1,0:T(2,128)(2,1)S(1)} async-done(((bf16[16,2,20480]{2,1,0:T(2,128)(2,1)}), bf16[16,2,20480]{2,1,0:T(2,128)(2,1)S(1)}, u32[]{:S(2)}, u32[]{:S(2)}) %all-to-all-start.2) | async-done | bytes 1310752 | tf_op jit(solution)/shard_map/all_to_all | solution.py:80
  175.9 5.2 %all-to-all-start = ((bf16[16,16,4096]{2,1,0:T(8,128)(2,1)}), bf16[16,16,4096]{2,1,0:T(8,128)(2,1)S(1)}, u32[]{:S(2)}, u32[]{:S(2)}) async-start(bf16[16,16,4096]{2,1,0:T(8,128)(2,1)} %bitcast.344), calls=%async_computation | async-start | bytes 4194304 | tf_op jit(solution)/shard_map/all_to_all | solution.py:68
  181.1 5.3 %reshape.394 = bf16[16,1,20,32,64]{4,3,2,1,0:T(8,128)(2,1)} reshape(bf16[16,2,20480]{2,1,0:T(2,128)(2,1)} %copy-done.1) | data formatting | bytes 2621440
  186.4 2.2 bitcast_bitcast_fusion.1
  188.6 3.2 %copy.70 = bf16[32,1,20,16,64]{4,3,0,2,1:T(8,128)(2,1)} copy(bf16[32,1,20,16,64]{4,0,2,1,3:T(8,128)(2,1)S(1)} %bitcast_bitcast_fusion.1) | data formatting | bytes 2621440 | tf_op jit(solution)/shard_map/transpose | solution.py:73
  191.8 4.5 %reshape.322 = bf16[32,20,1024]{2,0,1:T(8,128)(2,1)} reshape(bf16[32,1,20,16,64]{4,3,0,2,1:T(8,128)(2,1)} %copy.70) | data formatting | bytes 2621440 | tf_op jit(solution)/shard_map/reshape.110
  196.3 2.0 convolution_convert_fusion.1
  199.2 8.5 %all-to-all-done = bf16[16,16,4096]{2,1,0:T(8,128)(2,1)S(1)} async-done(((bf16[16,16,4096]{2,1,0:T(8,128)(2,1)}), bf16[16,16,4096]{2,1,0:T(8,128)(2,1)S(1)}, u32[]{:S(2)}, u32[]{:S(2)}) %all-to-all-start) | async-done | bytes 2097184 | tf_op jit(solution)/shard_map/all_to_all | solution.py:68
  207.7 16.8 %all-to-all-start.3 = ((bf16[32,20,256]{2,1,0:T(8,128)(2,1)}), bf16[32,20,256]{2,1,0:T(8,128)(2,1)}, u32[]{:S(2)}, u32[]{:S(2)}) async-start(bf16[32,20,256]{2,1,0:T(8,128)(2,1)} %copy.71), calls=%async_computation.3 | async-start | bytes 786432 | tf_op jit(solution)/shard_map/all_to_all | solution.py:232
  225.7 26.7 %all-to-all-done.3 = bf16[32,20,256]{2,1,0:T(8,128)(2,1)} async-done(((bf16[32,20,256]{2,1,0:T(8,128)(2,1)}), bf16[32,20,256]{2,1,0:T(8,128)(2,1)}, u32[]{:S(2)}, u32[]{:S(2)}) %all-to-all-start.3) | async-done | bytes 327712 | tf_op jit(solution)/shard_map/all_to_all | solution.py:232
  253.4 2.0 gather_fusion.1
  (175 shorter events, 35.9 us)
Async XLA Ops:
  7.2 151.8 %copy-start = (bf16[128,4096]{1,0:T(8,128)(2,1)S(1)}, bf16[128,4096]{1,0:T(8,128)(2,1)}, u32[]{:S(2)}) copy-start(bf16[128,4096]{1,0:T(8,128)(2,1)} %param.22) | copy-start | bytes 3145732
  16.3 26.8 %copy-start.6 = (bf16[256,128]{1,0:T(8,128)(2,1)S(1)}, bf16[256,128]{1,0:T(8,128)(2,1)}, u32[]{:S(2)}) copy-start(bf16[256,128]{1,0:T(8,128)(2,1)} %param.19) | copy-start | bytes 196612
  21.7 21.8 %copy-start.7 = (bf16[256,128]{1,0:T(8,128)(2,1)S(1)}, bf16[256,128]{1,0:T(8,128)(2,1)}, u32[]{:S(2)}) copy-start(bf16[256,128]{1,0:T(8,128)(2,1)} %param.17) | copy-start | bytes 196612
  21.7 22.2 %copy-start.8 = (bf16[256,128]{1,0:T(8,128)(2,1)S(1)}, bf16[256,128]{1,0:T(8,128)(2,1)}, u32[]{:S(2)}) copy-start(bf16[256,128]{1,0:T(8,128)(2,1)} %param.20) | copy-start | bytes 196612
  26.1 44.5 %all-to-all-start.1 = ((bf16[32,20,256]{2,1,0:T(8,128)(2,1)}), bf16[32,20,256]{2,1,0:T(8,128)(2,1)S(1)}, u32[]{:S(2)}, u32[]{:S(2)}) async-start(bf16[32,20,256]{2,1,0:T(8,128)(2,1)} %all_to_all.19), calls=%async_computation.1 | async-start | bytes 786432 | tf_op jit(solution)/shard_map/all_to_all | solution.py:215
  42.9 96.6 %all-gather.5.cloned.1.call-start = ((), (), s32[]{:S(2)}) async-start(), calls=%async_computation.4 | async-start | bytes 5570560 | tf_op jit(solution)/shard_map/all_gather | solution.py:217
  47.7 2.8 %copy-start.9 = (bf16[256,128]{1,0:T(8,128)(2,1)S(1)}, bf16[256,128]{1,0:T(8,128)(2,1)}, u32[]{:S(2)}) copy-start(bf16[256,128]{1,0:T(8,128)(2,1)} %param.18) | copy-start | bytes 196612
  54.3 0.7 copy-start.2
  71.5 7.3 %copy-start.10 = (bf16[256,128]{1,0:T(8,128)(2,1)S(1)}, bf16[256,128]{1,0:T(8,128)(2,1)}, u32[]{:S(2)}) copy-start(bf16[256,128]{1,0:T(8,128)(2,1)} %param.16) | copy-start | bytes 196612
  110.5 3.0 %copy-start.4 = (f32[4,2,64,64]{3,2,1,0:T(8,128)S(1)}, f32[4,2,64,64]{3,2,1,0:T(8,128)}, u32[]{:S(2)}) copy-start(f32[4,2,64,64]{3,2,1,0:T(8,128)} %get-tuple-element.44) | copy-start | bytes 393220
  110.5 3.0 %copy-start.5 = (f32[4,2,64,64]{2,3,1,0:T(8,128)S(1)}, f32[4,2,64,64]{2,3,1,0:T(8,128)}, u32[]{:S(2)}) copy-start(f32[4,2,64,64]{2,3,1,0:T(8,128)} %get-tuple-element.45) | copy-start | bytes 393220
  111.2 3.2 %copy-start.3 = (f32[2,4,64,64]{3,2,1,0:T(8,128)S(1)}, f32[2,4,64,64]{3,2,1,0:T(8,128)}, u32[]{:S(2)}) copy-start(f32[2,4,64,64]{3,2,1,0:T(8,128)} %copy-done.2) | copy-start | bytes 393220
  116.7 27.0 %copy-start.13 = (bf16[1,4096,64]{1,2,0:T(8,128)(2,1)S(1)}, bf16[1,4096,64]{1,2,0:T(8,128)(2,1)}, u32[]{:S(2)}) copy-start(bf16[1,4096,64]{1,2,0:T(8,128)(2,1)} %param.28) | copy-start | bytes 1572868
  139.4 4.3 %copy-start.12 = (bf16[32,20,4096]{2,0,1:T(8,128)(2,1)S(1)}, bf16[32,20,4096]{2,0,1:T(8,128)(2,1)}, u32[]{:S(2)}) copy-start(bf16[32,20,4096]{2,0,1:T(8,128)(2,1)} %all-gather.5.cloned.1.call-done) | copy-start | bytes 15728644
  152.4 6.0 %copy-start.14 = (f32[128]{0:T(128)S(1)}, f32[128]{0:T(128)}, u32[]{:S(2)}) copy-start(f32[128]{0:T(128)} %param.21) | copy-start | bytes 1540
  152.4 22.3 %all-to-all-start.2 = ((bf16[16,2,20480]{2,1,0:T(2,128)(2,1)}), bf16[16,2,20480]{2,1,0:T(2,128)(2,1)S(1)}, u32[]{:S(2)}, u32[]{:S(2)}) async-start(bf16[16,2,20480]{2,1,0:T(2,128)(2,1)} %reshape.393), calls=%async_computation.2 | async-start | bytes 2621440 | tf_op jit(solution)/shard_map/all_to_all | solution.py:80
  174.8 1.1 copy-start.1
  175.9 31.8 %all-to-all-start = ((bf16[16,16,4096]{2,1,0:T(8,128)(2,1)}), bf16[16,16,4096]{2,1,0:T(8,128)(2,1)S(1)}, u32[]{:S(2)}, u32[]{:S(2)}) async-start(bf16[16,16,4096]{2,1,0:T(8,128)(2,1)} %bitcast.344), calls=%async_computation | async-start | bytes 4194304 | tf_op jit(solution)/shard_map/all_to_all | solution.py:68
  196.3 28.2 %copy-start.11 = (f32[128,4]{0,1:T(4,128)S(1)}, f32[128,4]{0,1:T(4,128)}, u32[]{:S(2)}) copy-start(f32[128,4]{0,1:T(4,128)} %param.26) | copy-start | bytes 6148
  207.7 44.6 %all-to-all-start.3 = ((bf16[32,20,256]{2,1,0:T(8,128)(2,1)}), bf16[32,20,256]{2,1,0:T(8,128)(2,1)}, u32[]{:S(2)}, u32[]{:S(2)}) async-start(bf16[32,20,256]{2,1,0:T(8,128)(2,1)} %copy.71), calls=%async_computation.3 | async-start | bytes 786432 | tf_op jit(solution)/shard_map/all_to_all | solution.py:232
Sparse Core Ops, SparseCore 0:
  71.6 67.8 all-gather.4
where the time goes:
time: 264 us; the launch traced here: 263 us
  waiting for transfers between devices  87 us (33%)
  local copies, waits for them, and re-layouts  48 us (18%)
  starting transfers between devices  43.7 us (17%)
  matrix products  31.1 us (12%)
  blocking collectives  29 us (11%)
  between operations  15 us (6%)
  other arithmetic  9.4 us (4%)
    all_gather x2, blocking collectives, collected_together(): both, at, found = (lax.all_gather(jnp.concatenate(lines), axis), 0, {})  29 us
    all_to_all x1, waiting for transfers between devices, expert_half(): lax.all_to_all(result, EP, split_axis=0, concat_axis=0, tiled=True)  26.7 us
    all_gather x1, waiting for transfers between devices, expert_half(): rows_piece = lax.all_gather(arrived, 'tp', axis=3, tiled=True)  22.8 us
    dot_general x56, matrix products, einsum_exact(): return jnp.einsum(form, left, right, precision=EXACT_MATMUL)  21.4 us
    all_to_all x1, starting transfers between devices, expert_half(): lax.all_to_all(result, EP, split_axis=0, concat_axis=0, tiled=True)  16.8 us
    all_to_all x1, starting transfers between devices, expert_half(): arrived = lax.all_to_all(piece, EP, split_axis=0, concat_axis=0, tiled=True)  16.7 us
    all_to_all x1, waiting for transfers between devices, expert_half(): arrived = lax.all_to_all(piece, EP, split_axis=0, concat_axis=0, tiled=True)  15.2 us
    unnamed x34, local copies, waits for them, and re-layouts  14.6 us
  transfers between devices with their start and end apart: 5, of which 5 were waited for; matrix products, arithmetic and copies ran while one was open for 19% of the time, Pallas kernels for 0%

commit v1 on v0

v1 whole, which is shorter than its diff:
```python
import jax
import jax.numpy as jnp
from jax import lax
from jax.experimental import pallas as pl
from jax.experimental.pallas import tpu as pltpu
from jax.sharding import Mesh
from jax.sharding import PartitionSpec as P

HD = 64
BLOCK = 64
EP = ("ep_0", "ep_1")
TP = ("tp_y", "tp_x")
EP_TP = ("ep_0", "ep_1", "tp_y", "tp_x")
EXPERTS = 32
CAP = 20
SLOT = 2 * CAP
GROUP = 8

EXACT_MATMUL = lax.Precision.HIGHEST


def iota(shape, dim):
    return lax.broadcasted_iota(jnp.int32, shape, dim)


def nt(a, b):
    return lax.dot_general(a, b, (((1,), (1,)), ((), ())), preferred_element_type=jnp.float32)


def mm(a, b):
    return jnp.dot(a, b, preferred_element_type=jnp.float32)


def call(kernel, outs, *args):
    return pl.pallas_call(kernel, out_shape=outs)(*args)


def prep_kernel(x, xs, gain, routes, weights, out, rank_out, share_out):
    rows = x.shape[0]
    full = x[...].astype(jnp.float32)
    scale = lax.rsqrt(jnp.mean(full * full, axis=-1, keepdims=True) + 1.0)
    piece = (xs[...].astype(jnp.float32) * scale * gain[...]).astype(jnp.bfloat16)
    w = weights[...]
    portion = w / jnp.sum(w, axis=-1, keepdims=True)
    expert = iota((rows, EXPERTS), 1)
    chosen = jnp.zeros((rows, EXPERTS), jnp.float32)
    share = jnp.zeros((rows, EXPERTS), jnp.float32)
    for j in range(routes.shape[1]):
        hit = routes[:, j : j + 1] == expert
        chosen = jnp.where(hit, 1.0, chosen)
        share = jnp.where(hit, portion[:, j : j + 1], share)
    earlier = (iota((rows, rows), 1) <= iota((rows, rows), 0)).astype(jnp.bfloat16)
    rank = mm(earlier, chosen.astype(jnp.bfloat16)) * chosen
    rank_out[...] = rank
    share_out[...] = share
    total = EXPERTS * SLOT
    q = iota((total, EXPERTS), 0)
    spread = (q // SLOT == iota((total, EXPERTS), 1)).astype(jnp.bfloat16)
    seat = (iota((total, rows), 0) % CAP + 1).astype(jnp.float32)
    pick = (nt(spread, rank.astype(jnp.bfloat16)) == seat).astype(jnp.bfloat16)
    both = mm(pick, piece)
    second = iota((total, 128), 0) % SLOT >= CAP
    out[...] = jnp.where(second, both[:, 128:], both[:, :128]).astype(jnp.bfloat16)


def combine_kernel(back, rank, share, out):
    rows = rank.shape[0]
    total = EXPERTS * SLOT
    spread = (iota((total, EXPERTS), 0) // SLOT == iota((total, EXPERTS), 1)).astype(jnp.bfloat16)
    q = iota((rows, total), 1)
    match = nt(rank[...].astype(jnp.bfloat16), spread) == (q % CAP + 1).astype(jnp.float32)
    second = q % SLOT >= CAP
    high = share[...].astype(jnp.bfloat16)
    low = (share[...] - high.astype(jnp.float32)).astype(jnp.bfloat16)
    values = back[...]
    first_half = jnp.zeros((rows, 128), jnp.float32)
    second_half = jnp.zeros((rows, 128), jnp.float32)
    for part in (high, low):
        wide = jnp.where(match, nt(part, spread), 0.0)
        first_half += mm(jnp.where(second, 0.0, wide).astype(jnp.bfloat16), values)
        second_half += mm(jnp.where(second, wide, 0.0).astype(jnp.bfloat16), values)
    out[:, :128] = first_half.astype(out.dtype)
    out[:, 128:] = second_half.astype(out.dtype)


def selector(half):
    r = iota((GROUP * CAP, GROUP * SLOT), 0)
    return (iota((GROUP * CAP, GROUP * SLOT), 1) == r // CAP * SLOT + r % CAP + half * CAP).astype(
        jnp.bfloat16
    )


def gate_up_kernel(gathered, weights, out):
    picks = (selector(0), selector(1))
    joined = jnp.concatenate([weights[k] for k in range(weights.shape[0])], axis=1)
    for g in range(EXPERTS // GROUP):
        pieces = []
        for k in range(gathered.shape[0]):
            seen = gathered[k, g * GROUP * SLOT : (g + 1) * GROUP * SLOT, :]
            for pick in picks:
                pieces.append(mm(pick, seen).astype(jnp.bfloat16))
        out[g] = mm(jnp.concatenate(pieces, axis=1), joined).astype(jnp.bfloat16)


def hidden_kernel(parts, out):
    both = jnp.zeros(parts.shape[1:], jnp.float32)
    for k in range(parts.shape[0]):
        both += parts[k].astype(jnp.float32)
    made = []
    for k in range(both.shape[1] // 128):
        v = both[:, k * 128 : (k + 1) * 128]
        made.append(jax.nn.silu(v) * pltpu.roll(v, 64, 1))
    left = iota((both.shape[0], 128), 1) < 64
    for k in range(len(made) // 2):
        out[:, k * 128 : (k + 1) * 128] = jnp.where(
            left, made[2 * k], pltpu.roll(made[2 * k + 1], 64, 1)
        ).astype(jnp.bfloat16)


def down_kernel(hidden, weights, out):
    picks = (selector(0), selector(1))
    side = 4
    tall = []
    for k in range(side):
        tall.append(
            jnp.concatenate(
                [weights[(side * m + k) * 64 : (side * m + k + 1) * 64, :] for m in range(side)], 0
            )
        )
    for g in range(side):
        total = mm(hidden[side * g], tall[0])
        for k in range(1, side):
            total += mm(hidden[side * g + k], tall[k])
        total = total.astype(jnp.bfloat16)
        placed = jnp.zeros((GROUP * SLOT, 128), jnp.float32)
        for half in range(2):
            placed += lax.dot_general(
                picks[half],
                total[:, half * 128 : (half + 1) * 128],
                (((0,), (0,)), ((), ())),
                preferred_element_type=jnp.float32,
            )
        out[g * GROUP * SLOT : (g + 1) * GROUP * SLOT, :] = placed.astype(jnp.bfloat16)


def exchanged(tiles, axis):
    return lax.all_to_all(tiles, axis, split_axis=0, concat_axis=0, tiled=True)


def sent_to_all(shard, axis):
    return exchanged(jnp.broadcast_to(shard, (lax.axis_size(axis), *shard.shape)), axis)


def einsum_exact(form, left, right):
    return jnp.einsum(form, left, right, precision=EXACT_MATMUL)


def block_tables(receptance, key_in, value_in, decay_in, rate_in):
    token_count, columns = receptance.shape
    head_count = columns // HD
    block_count = token_count // BLOCK

    def to_blocks(array):
        return (
            array.astype(jnp.float32)
            .reshape(block_count, BLOCK, head_count, HD)
            .transpose(2, 0, 1, 3)
        )

    readout = to_blocks(receptance)
    key_rows = to_blocks(key_in)
    value_rows = to_blocks(value_in)
    log_decay = -jnp.exp(-jax.nn.softplus(-to_blocks(decay_in)) - 0.5)
    learn_rate = jax.nn.sigmoid(to_blocks(rate_in))
    unit_key = key_rows / jnp.sqrt(jnp.sum(key_rows * key_rows, axis=-1, keepdims=True) + 1.0)
    inclusive = jnp.cumsum(log_decay, axis=2)
    exclusive = inclusive - log_decay
    block_total = inclusive[:, :, -1:, :]
    probe = -unit_key * jnp.exp(exclusive)
    removal = unit_key * learn_rate
    written = key_rows * learn_rate
    removal_back = removal * jnp.exp(-inclusive)
    written_back = written * jnp.exp(-inclusive)
    readout_scaled = readout * jnp.exp(inclusive)
    removal_tail = removal * jnp.exp(block_total - inclusive)
    written_tail = written * jnp.exp(block_total - inclusive)
    strict = jnp.tril(jnp.ones((BLOCK, BLOCK), jnp.float32), -1)
    closed = jnp.tril(jnp.ones((BLOCK, BLOCK), jnp.float32))
    lower = einsum_exact("hbck,hbsk->hbcs", probe, removal_back) * strict
    lower_write = einsum_exact("hbck,hbsk->hbcs", probe, written_back) * strict
    reach = einsum_exact("hbck,hbsk->hbcs", readout_scaled, removal_back) * closed
    reach_write = einsum_exact("hbck,hbsk->hbcs", readout_scaled, written_back) * closed
    inverse = jnp.eye(BLOCK, dtype=jnp.float32) + lower
    power = lower
    for doubling in range(BLOCK.bit_length() - 2):
        power = einsum_exact("hbcs,hbst->hbct", power, power)
        inverse = inverse + einsum_exact("hbcs,hbst->hbct", inverse, power)
    solved_probe = einsum_exact("hbcs,hbsk->hbck", inverse, probe)
    solved_values = einsum_exact(
        "hbcs,hbsv->hbcv", inverse, einsum_exact("hbcs,hbsv->hbcv", lower_write, value_rows)
    )
    transition = jnp.exp(block_total[:, :, 0, :])[..., None] * jnp.eye(
        HD, dtype=jnp.float32
    ) + einsum_exact("hbck,hbcj->hbkj", removal_tail, solved_probe)
    increment = einsum_exact("hbck,hbcv->hbkv", removal_tail, solved_values) + einsum_exact(
        "hbck,hbcv->hbkv", written_tail, value_rows
    )
    read_state = readout_scaled + einsum_exact("hbcs,hbsk->hbck", reach, solved_probe)
    local_out = einsum_exact("hbcs,hbsv->hbcv", reach, solved_values) + einsum_exact(
        "hbcs,hbsv->hbcv", reach_write, value_rows
    )
    return (transition, increment, read_state, local_out)


def entering(transition, increment):
    peers, position = (lax.axis_size(EP), lax.axis_index(EP))
    zero = jnp.zeros_like(transition)
    identity = jnp.broadcast_to(jnp.eye(HD, dtype=jnp.float32), transition.shape)
    inclusive = jnp.concatenate([transition, increment], axis=-1)
    exclusive = jnp.concatenate([identity, zero], axis=-1)

    def after(preceding, following):
        moved = einsum_exact("quc,qcd->qud", following[..., :HD], preceding)
        return moved + jnp.concatenate([zero, following[..., HD:]], axis=-1)

    shift = 1
    while shift < peers:
        pairs = [(i, i + shift) for i in range(peers - shift)]
        came = lax.ppermute(inclusive.astype(jnp.bfloat16), EP, pairs).astype(jnp.float32)
        later = position >= shift
        exclusive = jnp.where(later, after(came, exclusive), exclusive)
        inclusive = jnp.where(later, after(came, inclusive), inclusive)
        shift *= 2
    return exclusive[..., HD:]


def mixer_half(receptance, key_in, value_in, decay_in, rate_in, norm_gain, out_weight):
    transition, increment, read_state, local_out = block_tables(
        receptance, key_in, value_in, decay_in, rate_in
    )
    head_count, block_count = transition.shape[:2]
    device_map = transition[:, 0]
    device_add = increment[:, 0]
    for k in range(1, block_count):
        step = transition[:, k]
        device_map = einsum_exact("quc,qcd->qud", step, device_map)
        device_add = einsum_exact("quc,qcd->qud", step, device_add) + increment[:, k]
    state = entering(device_map, device_add)
    entries = []
    for k in range(block_count):
        entries.append(state)
        if k + 1 < block_count:
            state = einsum_exact("quc,qcd->qud", transition[:, k], state) + increment[:, k]
    entry_state = jnp.stack(entries, axis=1)
    heads_out = einsum_exact("hbck,hbkv->hbcv", read_state, entry_state) + local_out
    center = heads_out - jnp.mean(heads_out, axis=-1, keepdims=True)
    spread = jnp.mean(center * center, axis=-1, keepdims=True)
    normed = center * lax.rsqrt(spread + 1.0) * norm_gain.reshape(head_count, 1, 1, HD)
    mixed = normed.transpose(1, 2, 0, 3).reshape(receptance.shape).astype(jnp.bfloat16)
    product = jnp.dot(mixed, out_weight, preferred_element_type=jnp.float32).astype(jnp.bfloat16)
    peers = lax.axis_size(TP)
    tiles = exchanged(product.reshape(peers, product.shape[0] // peers, -1), TP)
    return jnp.sum(tiles.astype(jnp.float32), axis=0).astype(jnp.bfloat16)


def expert_half(moe_in, ffn_gain, routes, route_weights, gate_weight, up_weight, down_weight):
    rows, features = moe_in.shape
    tp = lax.axis_size(TP)
    width = features // tp
    at = lax.axis_index(TP) * width
    both = jnp.concatenate([gate_weight[0], up_weight[0]], axis=1)
    side = lax.axis_size("tp_y")
    weights = exchanged(both.reshape(side, features // side, -1), "tp_y")
    total = EXPERTS * SLOT
    f32 = jnp.float32
    outgoing, rank, share = call(
        prep_kernel,
        (
            jax.ShapeDtypeStruct((total, 128), jnp.bfloat16),
            jax.ShapeDtypeStruct((rows, EXPERTS), f32),
            jax.ShapeDtypeStruct((rows, EXPERTS), f32),
        ),
        moe_in,
        lax.dynamic_slice_in_dim(moe_in, at, width, 1),
        lax.dynamic_slice_in_dim(ffn_gain, at, width, 0).reshape(1, width),
        routes,
        route_weights,
    )
    arrived = exchanged(outgoing.reshape(EXPERTS, SLOT, 128), EP).reshape(total, 128)
    gathered = sent_to_all(arrived, "tp_x")
    share_rows = EXPERTS * CAP // side
    wide = weights.shape[0] * weights.shape[2]
    partial = call(
        gate_up_kernel, jax.ShapeDtypeStruct((side, share_rows, wide), jnp.bfloat16), gathered, weights
    )
    parts = exchanged(partial, "tp_y")
    hidden = call(hidden_kernel, jax.ShapeDtypeStruct((share_rows, wide // 2), jnp.bfloat16), parts)
    everyone = sent_to_all(hidden, TP)
    result = call(
        down_kernel, jax.ShapeDtypeStruct((total, 128), jnp.bfloat16), everyone, down_weight[0]
    )
    returned = exchanged(result.reshape(EXPERTS, SLOT, 128), EP).reshape(total, 128)
    return call(
        combine_kernel, jax.ShapeDtypeStruct((rows, width), jnp.bfloat16), returned, rank, share
    )


def local(
    receptance,
    key_in,
    value_in,
    decay_in,
    rate_in,
    norm_gain,
    out_weight,
    moe_in,
    ffn_gain,
    routes,
    route_weights,
    gate_weight,
    up_weight,
    down_weight,
):
    moe_out = expert_half(
        moe_in, ffn_gain, routes, route_weights, gate_weight, up_weight, down_weight
    )
    mixer_out = mixer_half(receptance, key_in, value_in, decay_in, rate_in, norm_gain, out_weight)
    return (mixer_out, moe_out)


def solution(mesh):
    finer = Mesh(mesh.devices.reshape(16, 2, 4, 4), EP_TP)
    placed = (
        P(EP, TP),
        P(EP, TP),
        P(EP, TP),
        P(EP, TP),
        P(EP, TP),
        P(TP),
        P(TP, None),
        P(EP, None),
        P(),
        P(EP, None),
        P(EP, None),
        P(EP, None, TP),
        P(EP, None, TP),
        P(EP, None, TP),
    )
    return jax.shard_map(
        local, mesh=finer, in_specs=placed, out_specs=(P(EP_TP, None), P(EP, TP)), check_vma=False
    )
```

time: 264 us -> 234 us (0.89)
  starting transfers between devices: 43.7 us -> 87.6 us
  blocking collectives: 29 us -> 0 us
  local copies, waits for them, and re-layouts: 48 us -> 21.3 us
  Pallas kernels: 0 us -> 15.5 us
  waiting for transfers between devices: 87 us -> 73.3 us
  between operations: 15 us -> 1.4 us
  matrix products: 31.1 us -> 25.5 us
    ppermute x0 -> x5, starting transfers between devices: none -> 36 us  [entering(): lax.ppermute(inclusive.astype(jnp.bfloat16), EP, pairs).astype(jnp.float32)]
    all_gather x2 -> x0, blocking collectives: 29 us -> none  [collected_together(): both, at, found = (lax.all_gather(jnp.concatenate(lines), axis), 0, {})]
    all_gather x1 -> x0, waiting for transfers between devices: 22.8 us -> none  [expert_half(): rows_piece = lax.all_gather(arrived, 'tp', axis=3, tiled=True)]
    pallas_call x0 -> x5, Pallas kernels: none -> 15.5 us  [call(): return pl.pallas_call(kernel, out_shape=outs)(*args)]
    all_to_all x4 -> x7, starting transfers between devices: 43.5 us -> 51.6 us  [exchanged(): return lax.all_to_all(tiles, axis, split_axis=0, concat_axis=0, tiled=True)]
    dot_general x3 -> x0, matrix products: 7.71 us -> none  [the longest x1 4.25 us: expert_half(): jnp.einsum('secn,enf->secf', rows_piece, gate_weight, preferred_element_t...]
    gather x2 -> x0, local copies, waits for them, and re-layouts: 7.33 us -> none  [the longest x1 5.37 us: expert_half(): normed_rows[source]]
    transpose x2 -> x0, local copies, waits for them, and re-layouts: 5.38 us -> none  [joined_along(): tiles = jnp.moveaxis(tiles, 0, dim)]
  transfers between devices with their start and end apart: 5 -> 12, of which waited for: 5 -> 7; matrix products, arithmetic and copies ran while one was open for 19% -> 14% of each run, Pallas kernels for 0% -> 3%
where the time goes in v1:
time: 234 us; the launch traced here: 232 us
  starting transfers between devices  87.6 us (37%)
  waiting for transfers between devices  73.3 us (31%)
  matrix products  25.5 us (11%)
  local copies, waits for them, and re-layouts  21.3 us (9%)
  Pallas kernels  15.5 us (7%)
  other arithmetic  7.85 us (3%)
    all_to_all x7, waiting for transfers between devices, exchanged(): return lax.all_to_all(tiles, axis, split_axis=0, concat_axis=0, tiled=True)  68.2 us
    all_to_all x7, starting transfers between devices, exchanged(): return lax.all_to_all(tiles, axis, split_axis=0, concat_axis=0, tiled=True)  51.6 us
    ppermute x5, starting transfers between devices, entering(): lax.ppermute(inclusive.astype(jnp.bfloat16), EP, pairs).astype(jnp.float32)  36 us
    dot_general x42, matrix products, einsum_exact(): return jnp.einsum(form, left, right, precision=EXACT_MATMUL)  23.4 us
    pallas_call x5, Pallas kernels, call(): return pl.pallas_call(kernel, out_shape=outs)(*args)  15.5 us
    unnamed x58, local copies, waits for them, and re-layouts  9.86 us
    ppermute x5, waiting for transfers between devices, entering(): lax.ppermute(inclusive.astype(jnp.bfloat16), EP, pairs).astype(jnp.float32)  5.03 us
  transfers between devices with their start and end apart: 12, of which 7 were waited for; matrix products, arithmetic and copies ran while one was open for 14% of the time, Pallas kernels for 3%

profile of v1, /device:TPU:1, one launch (start us, length us, event | category | flops | bytes accessed | tf_op | source)
XLA Modules:
  0.0 232.3 jit_solution(14647036567206929262)
XLA Ops:
  17.4 4.9 %collective-permute-start = (bf16[2,64,128]{2,1,0:T(8,128)(2,1)}, bf16[2,64,128]{2,1,0:T(8,128)(2,1)}, u32[]{:S(2)}, u32[]{:S(2)}) collective-permute-start(bf16[2,64,128]{2,1,0:T(8,128)(2,1)} %fusion.52), channel_id=1, source_target_pairs={{0,16},{16,32},{32,48},{48,64},{64,80},{80,96},{96,112},{112,128},... | collective-permute-start | bytes 98312 | tf_op jit(solution)/shard_map/ppermute | solution.py:229
  22.3 1.5 copy.45
  23.8 2.4 %copy.46 = bf16[1,4096,64]{2,1,0:T(8,128)(2,1)} copy(bf16[1,4096,64]{1,2,0:T(8,128)(2,1)} %param.26) | data formatting | bytes 1048576 | tf_op args[12]
  26.2 2.8 %pad_maximum_fusion = bf16[4,1024,128]{2,1,0:T(8,128)(2,1)} fusion(bf16[4,1024,64]{2,1,0:T(8,128)(2,1)} %bitcast.201, bf16[4,1024,64]{2,1,0:T(8,128)(2,1)S(1)} %bitcast.200), kind=kLoop, calls=%fused_computation.38 | loop fusion | flops 2097152 | bytes 2097152 | tf_op jit(solution)/shard_map/concatenate | solution.py:271
  28.9 4.2 %all-to-all-start.3 = ((bf16[4,1024,128]{2,1,0:T(8,128)(2,1)}), bf16[4,1024,128]{2,1,0:T(8,128)(2,1)S(1)}, u32[]{:S(2)}, u32[]{:S(2)}) async-start(bf16[4,1024,128]{2,1,0:T(8,128)(2,1)} %pad_maximum_fusion), calls=%async_computation.3 | async-start | bytes 2097152 | tf_op jit(solution)/shard_map/all_to_all | solution.py:147
  34.8 1.5 convolution_multiply_fusion.3
  36.3 2.2 fusion.73
  41.0 1.5 constant_dynamic-slice_fusion.xs
  45.4 3.1 %shard_map.149 = (bf16[1280,128]{1,0:T(8,128)(2,1)}, f32[128,32]{1,0:T(8,128)}, f32[128,32]{1,0:T(8,128)}) custom-call(bf16[128,4096]{1,0:T(8,128)(2,1)} %x.19, bf16[128,256]{1,0:T(8,128)(2,1)} %constant_dynamic-slice_fusion.xs, f32[1,256]{1,0:T(1,128)} %bitcast.211, s32[128,4]{1,0:T(8,128)} %copy.43.routes, f32[128,4]{1,0:T(8,128)} %copy.44.weights), custom_call_target="tpu_custom_call" | custom-call | tf_op jit(solution)/shard_map/pallas_call | solution.py:35
  48.5 15.0 %all-to-all-start.1 = ((bf16[32,40,128]{2,1,0:T(8,128)(2,1)}), bf16[32,40,128]{2,1,0:T(8,128)(2,1)S(1)}, u32[]{:S(2)}, u32[]{:S(2)}) async-start(bf16[32,40,128]{2,1,0:T(8,128)(2,1)} %bitcast.208), calls=%async_computation.1 | async-start | bytes 655360 | tf_op jit(solution)/shard_map/all_to_all | solution.py:147
  64.5 3.3 %collective-permute-start.1 = (bf16[2,64,128]{2,1,0:T(8,128)(2,1)S(1)}, bf16[2,64,128]{2,1,0:T(8,128)(2,1)S(1)}, u32[]{:S(2)}, u32[]{:S(2)}) collective-permute-start(bf16[2,64,128]{2,1,0:T(8,128)(2,1)S(1)} %get-tuple-element.12), channel_id=1, source_target_pairs={{0,32},{16,48},{32,64},{48,80},{64,96},{80,112},{96,128},{112,144}... | collective-permute-start | bytes 98312 | tf_op jit(solution)/shard_map/ppermute | solution.py:229
  68.9 4.3 %collective-permute-done.1 = bf16[2,64,128]{2,1,0:T(8,128)(2,1)S(1)} collective-permute-done((bf16[2,64,128]{2,1,0:T(8,128)(2,1)S(1)}, bf16[2,64,128]{2,1,0:T(8,128)(2,1)S(1)}, u32[]{:S(2)}, u32[]{:S(2)}) %collective-permute-start.1) | collective-permute-done | bytes 32800 | tf_op jit(solution)/shard_map/ppermute | solution.py:229
  73.4 9.0 %collective-permute-start.2 = (bf16[2,64,128]{2,1,0:T(8,128)(2,1)S(1)}, bf16[2,64,128]{2,1,0:T(8,128)(2,1)S(1)}, u32[]{:S(2)}, u32[]{:S(2)}) collective-permute-start(bf16[2,64,128]{2,1,0:T(8,128)(2,1)S(1)} %get-tuple-element.14), channel_id=1, source_target_pairs={{0,64},{16,80},{32,96},{48,112},{64,128},{80,144},{96,160},{112,17... | collective-permute-start | bytes 98312 | tf_op jit(solution)/shard_map/ppermute | solution.py:229
  84.2 10.6 %collective-permute-start.3 = (bf16[2,64,128]{2,1,0:T(8,128)(2,1)}, bf16[2,64,128]{2,1,0:T(8,128)(2,1)}, u32[]{:S(2)}, u32[]{:S(2)}) collective-permute-start(bf16[2,64,128]{2,1,0:T(8,128)(2,1)} %get-tuple-element.16), channel_id=1, source_target_pairs={{0,128},{16,144},{32,160},{48,176},{64,192},{80,208},{96,224},{112... | collective-permute-start | bytes 98312 | tf_op jit(solution)/shard_map/ppermute | solution.py:229
  97.0 4.1 %all-to-all-start.2 = ((bf16[4,1280,128]{2,1,0:T(8,128)(2,1)}), bf16[4,1280,128]{2,1,0:T(8,128)(2,1)S(1)}, u32[]{:S(2)}, u32[]{:S(2)}) async-start(bf16[4,1280,128]{2,1,0:T(8,128)(2,1)} %broadcast_in_dim.16), calls=%async_computation.2 | async-start | bytes 2621440 | tf_op jit(solution)/shard_map/all_to_all | solution.py:147
  102.1 8.2 %collective-permute-start.4 = (bf16[2,64,128]{2,1,0:T(8,128)(2,1)S(1)}, bf16[2,64,128]{2,1,0:T(8,128)(2,1)S(1)}, u32[]{:S(2)}, u32[]{:S(2)}) collective-permute-start(bf16[2,64,128]{2,1,0:T(8,128)(2,1)S(1)} %fusion.9), channel_id=1, source_target_pairs={{0,256},{16,272},{32,288},{48,304},{64,320},{80,336},{96,352},{112... | collective-permute-start | bytes 98312 | tf_op jit(solution)/shard_map/ppermute | solution.py:229
  112.0 4.9 %all-to-all-done.2.gathered = bf16[4,1280,128]{2,1,0:T(8,128)(2,1)S(1)} async-done(((bf16[4,1280,128]{2,1,0:T(8,128)(2,1)}), bf16[4,1280,128]{2,1,0:T(8,128)(2,1)S(1)}, u32[]{:S(2)}, u32[]{:S(2)}) %all-to-all-start.2) | async-done | bytes 1310752 | tf_op jit(solution)/shard_map/all_to_all | solution.py:147
  118.0 4.4 %shard_map.150 = bf16[4,160,512]{2,1,0:T(8,128)(2,1)} custom-call(bf16[4,1280,128]{2,1,0:T(8,128)(2,1)} %copy-done.2, bf16[4,1024,128]{2,1,0:T(8,128)(2,1)} %copy-done.3), custom_call_target="tpu_custom_call" | custom-call | tf_op jit(solution)/shard_map/pallas_call | solution.py:35
  122.3 3.7 %all-to-all-start.4 = ((bf16[4,160,512]{2,1,0:T(8,128)(2,1)}), bf16[4,160,512]{2,1,0:T(8,128)(2,1)S(1)}, u32[]{:S(2)}, u32[]{:S(2)}) async-start(bf16[4,160,512]{2,1,0:T(8,128)(2,1)} %shard_map.150), calls=%async_computation.4 | async-start | bytes 1310720 | tf_op jit(solution)/shard_map/all_to_all | solution.py:147
  126.3 1.5 fusion.17
  127.8 5.9 %all-to-all-done.4.parts = bf16[4,160,512]{2,1,0:T(8,128)(2,1)S(1)} async-done(((bf16[4,160,512]{2,1,0:T(8,128)(2,1)}), bf16[4,160,512]{2,1,0:T(8,128)(2,1)S(1)}, u32[]{:S(2)}, u32[]{:S(2)}) %all-to-all-start.4) | async-done | bytes 655392 | tf_op jit(solution)/shard_map/all_to_all | solution.py:147
  134.5 1.9 shard_map.151
  136.5 2.1 broadcast_in_dim.17
  138.6 3.7 %all-to-all-start.5 = ((bf16[16,160,256]{2,1,0:T(8,128)(2,1)}), bf16[16,160,256]{2,1,0:T(8,128)(2,1)S(1)}, u32[]{:S(2)}, u32[]{:S(2)}) async-start(bf16[16,160,256]{2,1,0:T(8,128)(2,1)} %broadcast_in_dim.17), calls=%async_computation.5 | async-start | bytes 2621440 | tf_op jit(solution)/shard_map/all_to_all | solution.py:147
  143.1 2.1 convolution_convert_fusion
  145.2 12.9 %all-to-all-done.5.hidden = bf16[16,160,256]{2,1,0:T(8,128)(2,1)S(1)} async-done(((bf16[16,160,256]{2,1,0:T(8,128)(2,1)}), bf16[16,160,256]{2,1,0:T(8,128)(2,1)S(1)}, u32[]{:S(2)}, u32[]{:S(2)}) %all-to-all-start.5) | async-done | bytes 1310752 | tf_op jit(solution)/shard_map/all_to_all | solution.py:147
  159.2 3.9 %all-to-all-start = ((bf16[16,16,4096]{2,1,0:T(8,128)(2,1)}), bf16[16,16,4096]{2,1,0:T(8,128)(2,1)S(1)}, u32[]{:S(2)}, u32[]{:S(2)}) async-start(bf16[16,16,4096]{2,1,0:T(8,128)(2,1)} %bitcast.199), calls=%async_computation | async-start | bytes 4194304 | tf_op jit(solution)/shard_map/all_to_all | solution.py:147
  163.1 3.6 %shard_map.152 = bf16[1280,128]{1,0:T(8,128)(2,1)} custom-call(bf16[16,160,256]{2,1,0:T(8,128)(2,1)} %copy-done.1, bf16[1024,256]{1,0:T(8,128)(2,1)} %bitcast.207), custom_call_target="tpu_custom_call" | custom-call | tf_op jit(solution)/shard_map/pallas_call | solution.py:35
  166.7 20.5 %all-to-all-done = bf16[16,16,4096]{2,1,0:T(8,128)(2,1)S(1)} async-done(((bf16[16,16,4096]{2,1,0:T(8,128)(2,1)}), bf16[16,16,4096]{2,1,0:T(8,128)(2,1)S(1)}, u32[]{:S(2)}, u32[]{:S(2)}) %all-to-all-start) | async-done | bytes 2097184 | tf_op jit(solution)/shard_map/all_to_all | solution.py:147
  187.2 16.9 %all-to-all-start.6 = ((bf16[32,40,128]{2,1,0:T(8,128)(2,1)}), bf16[32,40,128]{2,1,0:T(8,128)(2,1)S(1)}, u32[]{:S(2)}, u32[]{:S(2)}) async-start(bf16[32,40,128]{2,1,0:T(8,128)(2,1)} %bitcast.204), calls=%async_computation.6 | async-start | bytes 655360 | tf_op jit(solution)/shard_map/all_to_all | solution.py:147
  205.1 24.0 %all-to-all-done.6 = bf16[32,40,128]{2,1,0:T(8,128)(2,1)S(1)} async-done(((bf16[32,40,128]{2,1,0:T(8,128)(2,1)}), bf16[32,40,128]{2,1,0:T(8,128)(2,1)S(1)}, u32[]{:S(2)}, u32[]{:S(2)}) %all-to-all-start.6) | async-done | bytes 327712 | tf_op jit(solution)/shard_map/all_to_all | solution.py:147
  229.8 2.5 %shard_map.153 = bf16[128,256]{1,0:T(8,128)(2,1)} custom-call(bf16[1280,128]{1,0:T(8,128)(2,1)} %bitcast.202, f32[128,32]{1,0:T(8,128)} %get-tuple-element.6.rank, f32[128,32]{1,0:T(8,128)} %get-tuple-element.7.share), custom_call_target="tpu_custom_call" | custom-call | tf_op jit(solution)/shard_map/pallas_call | solution.py:35
  (141 shorter events, 37.8 us)
Async XLA Ops:
  0.6 142.5 %copy-start = (bf16[128,4096]{1,0:T(8,128)(2,1)S(1)}, bf16[128,4096]{1,0:T(8,128)(2,1)}, u32[]{:S(2)}) copy-start(bf16[128,4096]{1,0:T(8,128)(2,1)} %param.20) | copy-start | bytes 3145732
  0.7 13.7 %copy-start.20 = (f32[64,64]{1,0:T(8,128)}, f32[64,64]{1,0:T(8,128)S(1)}, u32[]{:S(2)}) copy-start(f32[64,64]{1,0:T(8,128)S(1)} %fusion.54) | copy-start | bytes 49156
  12.3 3.5 %copy-start.10 = (f32[2,4,64,64]{3,2,1,0:T(8,128)}, f32[2,4,64,64]{3,2,1,0:T(8,128)S(1)}, u32[]{:S(2)}) copy-start(f32[2,4,64,64]{3,2,1,0:T(8,128)S(1)} %fusion.62) | copy-start | bytes 393220
  15.6 10.6 %copy-start.6 = (f32[2,4,64,64]{3,2,0,1:T(8,128)}, f32[2,4,64,64]{3,2,0,1:T(8,128)S(1)}, u32[]{:S(2)}) copy-start(f32[2,4,64,64]{3,2,0,1:T(8,128)S(1)} %convolution_add_fusion.6) | copy-start | bytes 393220
  17.4 46.2 %collective-permute-start = (bf16[2,64,128]{2,1,0:T(8,128)(2,1)}, bf16[2,64,128]{2,1,0:T(8,128)(2,1)}, u32[]{:S(2)}, u32[]{:S(2)}) collective-permute-start(bf16[2,64,128]{2,1,0:T(8,128)(2,1)} %fusion.52), channel_id=1, source_target_pairs={{0,16},{16,32},{32,48},{48,64},{64,80},{80,96},{96,112},{112,128},... | collective-permute-start | bytes 98312 | tf_op jit(solution)/shard_map/ppermute | solution.py:229
  28.9 19.6 %all-to-all-start.3 = ((bf16[4,1024,128]{2,1,0:T(8,128)(2,1)}), bf16[4,1024,128]{2,1,0:T(8,128)(2,1)S(1)}, u32[]{:S(2)}, u32[]{:S(2)}) async-start(bf16[4,1024,128]{2,1,0:T(8,128)(2,1)} %pad_maximum_fusion), calls=%async_computation.3 | async-start | bytes 2097152 | tf_op jit(solution)/shard_map/all_to_all | solution.py:147
  34.8 3.8 %copy-start.11 = (f32[2,4,64,64]{3,2,1,0:T(8,128)S(1)}, f32[2,4,64,64]{3,2,1,0:T(8,128)}, u32[]{:S(2)}) copy-start(f32[2,4,64,64]{3,2,1,0:T(8,128)} %copy-done.10) | copy-start | bytes 393220
  34.8 4.9 %copy-start.22 = (f32[64,64]{1,0:T(8,128)S(1)}, f32[64,64]{1,0:T(8,128)}, u32[]{:S(2)}) copy-start(f32[64,64]{1,0:T(8,128)} %fusion.53) | copy-start | bytes 49156
  36.3 6.2 %copy-start.26 = (f32[128]{0:T(128)S(1)}, f32[128]{0:T(128)}, u32[]{:S(2)}) copy-start(f32[128]{0:T(128)} %param.19) | copy-start | bytes 1540
  36.3 7.6 %copy-start.24 = (s32[128,4]{0,1:T(4,128)S(1)}, s32[128,4]{0,1:T(4,128)}, u32[]{:S(2)}) copy-start(s32[128,4]{0,1:T(4,128)} %param.23) | copy-start | bytes 6148
  36.3 8.3 %copy-start.25 = (f32[128,4]{0,1:T(4,128)S(1)}, f32[128,4]{0,1:T(4,128)}, u32[]{:S(2)}) copy-start(f32[128,4]{0,1:T(4,128)} %param.24) | copy-start | bytes 6148
  41.0 22.5 %copy-start.16 = (f32[2,64,64]{2,1,0:T(8,128)S(1)}, f32[2,64,64]{2,1,0:T(8,128)}, u32[]{:S(2)}) copy-start(f32[2,64,64]{2,1,0:T(8,128)} %copy-done.15) | copy-start | bytes 98308
  41.0 22.5 %copy-start.19 = (f32[2,64,64]{2,1,0:T(8,128)S(1)}, f32[2,64,64]{2,1,0:T(8,128)}, u32[]{:S(2)}) copy-start(f32[2,64,64]{2,1,0:T(8,128)} %copy-done.18) | copy-start | bytes 98308
  41.0 26.7 %copy-start.21 = (f32[64,64]{1,0:T(8,128)S(1)}, f32[64,64]{1,0:T(8,128)}, u32[]{:S(2)}) copy-start(f32[64,64]{1,0:T(8,128)} %copy-done.20) | copy-start | bytes 49156
  48.5 48.5 %copy-start.3 = (bf16[4,1024,128]{2,1,0:T(8,128)(2,1)}, bf16[4,1024,128]{2,1,0:T(8,128)(2,1)S(1)}, u32[]{:S(2)}) copy-start(bf16[4,1024,128]{2,1,0:T(8,128)(2,1)S(1)} %all-to-all-done.3.weights) | copy-start | bytes 3145732
  48.5 47.3 %all-to-all-start.1 = ((bf16[32,40,128]{2,1,0:T(8,128)(2,1)}), bf16[32,40,128]{2,1,0:T(8,128)(2,1)S(1)}, u32[]{:S(2)}, u32[]{:S(2)}) async-start(bf16[32,40,128]{2,1,0:T(8,128)(2,1)} %bitcast.208), calls=%async_computation.1 | async-start | bytes 655360 | tf_op jit(solution)/shard_map/all_to_all | solution.py:147
  64.5 8.7 %collective-permute-start.1 = (bf16[2,64,128]{2,1,0:T(8,128)(2,1)S(1)}, bf16[2,64,128]{2,1,0:T(8,128)(2,1)S(1)}, u32[]{:S(2)}, u32[]{:S(2)}) collective-permute-start(bf16[2,64,128]{2,1,0:T(8,128)(2,1)S(1)} %get-tuple-element.12), channel_id=1, source_target_pairs={{0,32},{16,48},{32,64},{48,80},{64,96},{80,112},{96,128},{112,144}... | collective-permute-start | bytes 98312 | tf_op jit(solution)/shard_map/ppermute | solution.py:229
  73.4 10.0 %collective-permute-start.2 = (bf16[2,64,128]{2,1,0:T(8,128)(2,1)S(1)}, bf16[2,64,128]{2,1,0:T(8,128)(2,1)S(1)}, u32[]{:S(2)}, u32[]{:S(2)}) collective-permute-start(bf16[2,64,128]{2,1,0:T(8,128)(2,1)S(1)} %get-tuple-element.14), channel_id=1, source_target_pairs={{0,64},{16,80},{32,96},{48,112},{64,128},{80,144},{96,160},{112,17... | collective-permute-start | bytes 98312 | tf_op jit(solution)/shard_map/ppermute | solution.py:229
  84.2 17.0 %collective-permute-start.3 = (bf16[2,64,128]{2,1,0:T(8,128)(2,1)}, bf16[2,64,128]{2,1,0:T(8,128)(2,1)}, u32[]{:S(2)}, u32[]{:S(2)}) collective-permute-start(bf16[2,64,128]{2,1,0:T(8,128)(2,1)} %get-tuple-element.16), channel_id=1, source_target_pairs={{0,128},{16,144},{32,160},{48,176},{64,192},{80,208},{96,224},{112... | collective-permute-start | bytes 98312 | tf_op jit(solution)/shard_map/ppermute | solution.py:229
  95.8 15.7 %copy-start.7 = (f32[2,4,64,64]{3,2,0,1:T(8,128)S(1)}, f32[2,4,64,64]{3,2,0,1:T(8,128)}, u32[]{:S(2)}) copy-start(f32[2,4,64,64]{3,2,0,1:T(8,128)} %copy-done.6) | copy-start | bytes 393220
  97.0 13.3 %copy-start.23 = (f32[2,64,64]{2,1,0:T(8,128)S(1)}, f32[2,64,64]{2,1,0:T(8,128)}, u32[]{:S(2)}) copy-start(f32[2,64,64]{2,1,0:T(8,128)} %slice.120) | copy-start | bytes 98308
  97.0 19.9 %all-to-all-start.2 = ((bf16[4,1280,128]{2,1,0:T(8,128)(2,1)}), bf16[4,1280,128]{2,1,0:T(8,128)(2,1)S(1)}, u32[]{:S(2)}, u32[]{:S(2)}) async-start(bf16[4,1280,128]{2,1,0:T(8,128)(2,1)} %broadcast_in_dim.16), calls=%async_computation.2 | async-start | bytes 2621440 | tf_op jit(solution)/shard_map/all_to_all | solution.py:147
  102.1 9.2 %collective-permute-start.4 = (bf16[2,64,128]{2,1,0:T(8,128)(2,1)S(1)}, bf16[2,64,128]{2,1,0:T(8,128)(2,1)S(1)}, u32[]{:S(2)}, u32[]{:S(2)}) collective-permute-start(bf16[2,64,128]{2,1,0:T(8,128)(2,1)S(1)} %fusion.9), channel_id=1, source_target_pairs={{0,256},{16,272},{32,288},{48,304},{64,320},{80,336},{96,352},{112... | collective-permute-start | bytes 98312 | tf_op jit(solution)/shard_map/ppermute | solution.py:229
  111.8 10.6 %copy-start.14 = (f32[2,64,64]{2,1,0:T(8,128)}, f32[2,64,64]{2,1,0:T(8,128)S(1)}, u32[]{:S(2)}) copy-start(f32[2,64,64]{2,1,0:T(8,128)S(1)} %convolution_add_fusion.11) | copy-start | bytes 98308
  112.0 14.3 %copy-start.17 = (f32[2,64,64]{2,1,0:T(8,128)}, f32[2,64,64]{2,1,0:T(8,128)S(1)}, u32[]{:S(2)}) copy-start(f32[2,64,64]{2,1,0:T(8,128)S(1)} %convolution_add_fusion.10) | copy-start | bytes 98308
  112.0 14.3 %copy-start.9 = (f32[2,4,64,64]{3,2,1,0:T(8,128)S(1)}, f32[2,4,64,64]{3,2,1,0:T(8,128)}, u32[]{:S(2)}) copy-start(f32[2,4,64,64]{3,2,1,0:T(8,128)} %convolution_add_fusion.8) | copy-start | bytes 393220
  122.3 11.3 %all-to-all-start.4 = ((bf16[4,160,512]{2,1,0:T(8,128)(2,1)}), bf16[4,160,512]{2,1,0:T(8,128)(2,1)S(1)}, u32[]{:S(2)}, u32[]{:S(2)}) async-start(bf16[4,160,512]{2,1,0:T(8,128)(2,1)} %shard_map.150), calls=%async_computation.4 | async-start | bytes 1310720 | tf_op jit(solution)/shard_map/all_to_all | solution.py:147
  136.5 5.8 %copy-start.12 = (f32[2,4,64,64]{2,3,1,0:T(8,128)S(1)}, f32[2,4,64,64]{2,3,1,0:T(8,128)}, u32[]{:S(2)}) copy-start(f32[2,4,64,64]{2,3,1,0:T(8,128)} %fusion.73) | copy-start | bytes 393220
  136.5 5.9 %copy-start.13 = (f32[2,4,64,64]{3,2,1,0:T(8,128)S(1)}, f32[2,4,64,64]{3,2,1,0:T(8,128)}, u32[]{:S(2)}) copy-start(f32[2,4,64,64]{3,2,1,0:T(8,128)} %convolution_multiply_fusion) | copy-start | bytes 393220
  138.6 19.5 %all-to-all-start.5 = ((bf16[16,160,256]{2,1,0:T(8,128)(2,1)}), bf16[16,160,256]{2,1,0:T(8,128)(2,1)S(1)}, u32[]{:S(2)}, u32[]{:S(2)}) async-start(bf16[16,160,256]{2,1,0:T(8,128)(2,1)} %broadcast_in_dim.17), calls=%async_computation.5 | async-start | bytes 2621440 | tf_op jit(solution)/shard_map/all_to_all | solution.py:147
  159.2 28.0 %all-to-all-start = ((bf16[16,16,4096]{2,1,0:T(8,128)(2,1)}), bf16[16,16,4096]{2,1,0:T(8,128)(2,1)S(1)}, u32[]{:S(2)}, u32[]{:S(2)}) async-start(bf16[16,16,4096]{2,1,0:T(8,128)(2,1)} %bitcast.199), calls=%async_computation | async-start | bytes 4194304 | tf_op jit(solution)/shard_map/all_to_all | solution.py:147
  187.2 41.9 %all-to-all-start.6 = ((bf16[32,40,128]{2,1,0:T(8,128)(2,1)}), bf16[32,40,128]{2,1,0:T(8,128)(2,1)S(1)}, u32[]{:S(2)}, u32[]{:S(2)}) async-start(bf16[32,40,128]{2,1,0:T(8,128)(2,1)} %bitcast.204), calls=%async_computation.6 | async-start | bytes 655360 | tf_op jit(solution)/shard_map/all_to_all | solution.py:147
  (7 other events, 6.2 us)

commit v2 on v1

v2 whole, which is shorter than its diff:
```python
import jax
import jax.numpy as jnp
from jax import lax
from jax.experimental import pallas as pl
from jax.experimental.pallas import tpu as pltpu
from jax.sharding import Mesh
from jax.sharding import PartitionSpec as P

HD = 64
BLOCK = 64
EP = ("ep_0", "ep_1")
TP = ("tp_y", "tp_x")
EP_TP = ("ep_0", "ep_1", "tp_y", "tp_x")
EXPERTS = 32
CAP = 20
SLOT = 2 * CAP
GROUP = 8


def iota(shape, dim):
    return lax.broadcasted_iota(jnp.int32, shape, dim)


def nt(a, b):
    return lax.dot_general(a, b, (((1,), (1,)), ((), ())), preferred_element_type=jnp.float32)


def mm(a, b):
    return jnp.dot(a, b, preferred_element_type=jnp.float32)


NN = (((1,), (0,)), ((), ()))
NT = (((1,), (1,)), ((), ()))
TN = (((0,), (0,)), ((), ()))


def halves(a):
    high = a.astype(jnp.bfloat16)
    return high, (a - high.astype(jnp.float32)).astype(jnp.bfloat16)


def dot(a, b, dims):
    return lax.dot_general(a, b, dims, preferred_element_type=jnp.float32)


def fine_dot(a, b, dims=NN):
    ah, al = halves(a)
    bh, bl = halves(b)
    return dot(ah, bh, dims) + dot(ah, bl, dims) + dot(al, bh, dims)


def call(kernel, outs, *args, scalars=0, scratch=()):
    whole = [pl.BlockSpec(memory_space=pltpu.VMEM)] * (len(args) - scalars)
    return pl.pallas_call(
        kernel,
        out_shape=outs,
        in_specs=[pl.BlockSpec(memory_space=pltpu.SMEM)] * scalars + whole,
        scratch_shapes=list(scratch),
    )(*args)


def shape(dims, dtype=jnp.bfloat16):
    return jax.ShapeDtypeStruct(dims, dtype)


def prep_kernel(place, x, gain, routes, weights, out, rank_out, share_out):
    rows = x.shape[0]
    full = x[...].astype(jnp.float32)
    scale = lax.rsqrt(jnp.mean(full * full, axis=-1, keepdims=True) + 1.0)
    mine = pl.ds(pl.multiple_of(place[0] * 256, 256), 256)
    piece = (x[:, mine].astype(jnp.float32) * scale * gain[:, mine]).astype(jnp.bfloat16)
    w = weights[...]
    portion = w / jnp.sum(w, axis=0, keepdims=True)
    expert = iota((EXPERTS, rows), 0)
    chosen = jnp.zeros((EXPERTS, rows), jnp.float32)
    share = jnp.zeros((EXPERTS, rows), jnp.float32)
    for j in range(routes.shape[0]):
        hit = routes[j : j + 1, :] == expert
        chosen = jnp.where(hit, 1.0, chosen)
        share = jnp.where(hit, portion[j : j + 1, :], share)
    earlier = (iota((rows, rows), 0) <= iota((rows, rows), 1)).astype(jnp.bfloat16)
    rank = mm(chosen.astype(jnp.bfloat16), earlier) * chosen
    rank_out[...] = rank
    share_out[...] = share
    total = EXPERTS * SLOT
    q = iota((total, EXPERTS), 0)
    spread = (q // SLOT == iota((total, EXPERTS), 1)).astype(jnp.bfloat16)
    seat = (iota((total, rows), 0) % CAP + 1).astype(jnp.float32)
    pick = (mm(spread, rank.astype(jnp.bfloat16)) == seat).astype(jnp.bfloat16)
    both = mm(pick, piece)
    second = iota((total, 128), 0) % SLOT >= CAP
    out[...] = jnp.where(second, both[:, 128:], both[:, :128]).astype(jnp.bfloat16)


def combine_kernel(back, rank, share, out):
    rows = rank.shape[1]
    total = EXPERTS * SLOT
    rank = jnp.transpose(rank[...])
    share = jnp.transpose(share[...])
    spread = (iota((total, EXPERTS), 0) // SLOT == iota((total, EXPERTS), 1)).astype(jnp.bfloat16)
    q = iota((rows, total), 1)
    match = nt(rank.astype(jnp.bfloat16), spread) == (q % CAP + 1).astype(jnp.float32)
    second = q % SLOT >= CAP
    high, low = halves(share)
    values = back[...]
    first_half = jnp.zeros((rows, 128), jnp.float32)
    second_half = jnp.zeros((rows, 128), jnp.float32)
    for part in (high, low):
        wide = jnp.where(match, nt(part, spread), 0.0)
        first_half += mm(jnp.where(second, 0.0, wide).astype(jnp.bfloat16), values)
        second_half += mm(jnp.where(second, wide, 0.0).astype(jnp.bfloat16), values)
    out[:, :128] = first_half.astype(out.dtype)
    out[:, 128:] = second_half.astype(out.dtype)


def selector(half):
    r = iota((GROUP * CAP, GROUP * SLOT), 0)
    return (iota((GROUP * CAP, GROUP * SLOT), 1) == r // CAP * SLOT + r % CAP + half * CAP).astype(
        jnp.bfloat16
    )


def gate_up_kernel(place, gathered, w0, w1, w2, w3, out, weights):
    picks = (selector(0), selector(1))
    side = weights.shape[0]
    for back, w in enumerate((w0, w1, w2, w3)):
        weights[(place[0] + side - back) % side] = w[: weights.shape[1], :]
    joined = jnp.concatenate([weights[k] for k in range(side)], axis=1)
    for g in range(EXPERTS // GROUP):
        pieces = []
        for k in range(gathered.shape[0]):
            seen = gathered[k, g * GROUP * SLOT : (g + 1) * GROUP * SLOT, :]
            for pick in picks:
                pieces.append(mm(pick, seen).astype(jnp.bfloat16))
        out[g] = mm(jnp.concatenate(pieces, axis=1), joined).astype(jnp.bfloat16)


def hidden_kernel(parts, out):
    both = jnp.zeros(parts.shape[1:], jnp.float32)
    for k in range(parts.shape[0]):
        both += parts[k].astype(jnp.float32)
    made = []
    for k in range(both.shape[1] // 128):
        v = both[:, k * 128 : (k + 1) * 128]
        made.append(jax.nn.silu(v) * pltpu.roll(v, 64, 1))
    left = iota((both.shape[0], 128), 1) < 64
    for k in range(len(made) // 2):
        value = jnp.where(left, made[2 * k], pltpu.roll(made[2 * k + 1], 64, 1))
        for peer in range(out.shape[0]):
            out[peer, :, k * 128 : (k + 1) * 128] = value.astype(jnp.bfloat16)


def down_kernel(hidden, weights, out):
    picks = (selector(0), selector(1))
    side = 4
    tall = []
    for k in range(side):
        tall.append(
            jnp.concatenate(
                [weights[(side * m + k) * 64 : (side * m + k + 1) * 64, :] for m in range(side)], 0
            )
        )
    for g in range(side):
        total = mm(hidden[side * g], tall[0])
        for k in range(1, side):
            total += mm(hidden[side * g + k], tall[k])
        total = total.astype(jnp.bfloat16)
        placed = jnp.zeros((GROUP * SLOT, 128), jnp.float32)
        for half in range(2):
            placed += lax.dot_general(
                picks[half],
                total[:, half * 128 : (half + 1) * 128],
                (((0,), (0,)), ((), ())),
                preferred_element_type=jnp.float32,
            )
        out[g * GROUP * SLOT : (g + 1) * GROUP * SLOT, :] = placed.astype(jnp.bfloat16)


def exchanged(tiles, axis):
    return lax.all_to_all(tiles, axis, split_axis=0, concat_axis=0, tiled=True)


def sent_to_all(shard, axis):
    return exchanged(jnp.broadcast_to(shard, (lax.axis_size(axis), *shard.shape)), axis)


def head_sums(a):
    left = iota(a.shape, 1) < HD
    low = jnp.sum(jnp.where(left, a, 0.0), axis=-1, keepdims=True)
    high = jnp.sum(jnp.where(left, 0.0, a), axis=-1, keepdims=True)
    return jnp.where(left, low, high)


def tables_kernel(receptance, key_in, value_in, decay_in, rate_in, inc, inc_send, read, local_out):
    f32 = jnp.float32
    size = (BLOCK, BLOCK)
    strict = (iota(size, 1) < iota(size, 0)).astype(f32)
    closed = (iota(size, 1) <= iota(size, 0)).astype(f32)
    eye = (iota(size, 1) == iota(size, 0)).astype(f32)
    summing = closed.astype(jnp.bfloat16)
    count = receptance.shape[0] // BLOCK
    heads = receptance.shape[1] // HD
    state = [jnp.concatenate([eye, jnp.zeros(size, f32)], axis=1) for _ in range(heads)]
    blocks = []
    for b in range(count):
        at = slice(b * BLOCK, (b + 1) * BLOCK)
        readout = receptance[at, :].astype(f32)
        key = key_in[at, :].astype(f32)
        value = value_in[at, :].astype(f32)
        log_decay = -jnp.exp(-jax.nn.softplus(-decay_in[at, :].astype(f32)) - 0.5)
        rate = jax.nn.sigmoid(rate_in[at, :].astype(f32))
        unit = key / jnp.sqrt(head_sums(key * key) + 1.0)
        first, _ = halves(log_decay)
        middle = (log_decay - first.astype(f32)).astype(jnp.bfloat16)
        last = (log_decay - first.astype(f32) - middle.astype(f32)).astype(jnp.bfloat16)
        inclusive = mm(summing, first) + mm(summing, middle) + mm(summing, last)
        total = inclusive[BLOCK - 1 :, :]
        probe = -unit * jnp.exp(inclusive - log_decay)
        removal = unit * rate
        written = key * rate
        grow = jnp.exp(-inclusive)
        tail = jnp.exp(total - inclusive)
        blocks.append(
            (
                probe,
                readout * jnp.exp(inclusive),
                removal * grow,
                written * grow,
                removal * tail,
                written * tail,
                value,
                jnp.exp(total),
            )
        )
    work = []
    for b in range(count):
        for h in range(heads):
            side = slice(h * HD, (h + 1) * HD)
            cut = [a[:, side] for a in blocks[b]]
            probe, readout, removal, written, removal_tail, written_tail, value, total = cut
            meet = fine_dot(
                jnp.concatenate([probe, readout], 0), jnp.concatenate([removal, written], 0), NT
            )
            work.append(
                dict(
                    lower=meet[:BLOCK, :BLOCK] * strict,
                    write=meet[:BLOCK, BLOCK:] * strict,
                    reach=meet[BLOCK:, :BLOCK] * closed,
                    reach_write=meet[BLOCK:, BLOCK:] * closed,
                    probe=probe,
                    readout=readout,
                    removal_tail=removal_tail,
                    written_tail=written_tail,
                    value=value,
                    total=total,
                )
            )
    inverses = [eye + w["lower"] for w in work]
    powers = [fine_dot(w["lower"], w["lower"]) for w in work]
    for step in range(BLOCK.bit_length() - 2):
        for k in range(len(work)):
            if step + 3 < BLOCK.bit_length():
                both = fine_dot(jnp.concatenate([inverses[k], powers[k]], 0), powers[k])
                inverses[k] = inverses[k] + both[:BLOCK]
                powers[k] = both[BLOCK:]
            else:
                inverses[k] = inverses[k] + fine_dot(inverses[k], powers[k])
    zero = jnp.zeros(size, f32)
    steps = []
    for k, w in enumerate(work):
        seen = fine_dot(w["write"], w["value"])
        solved = fine_dot(inverses[k], jnp.concatenate([w["probe"], seen], 1))
        right = jnp.concatenate([solved, jnp.concatenate([zero, w["value"]], 1)], 0)
        moved = fine_dot(jnp.concatenate([w["removal_tail"], w["written_tail"]], 0), right, TN)
        heard = fine_dot(jnp.concatenate([w["reach"], w["reach_write"]], 1), right)
        steps.append(
            (
                jnp.concatenate([w["readout"] + heard[:, :HD], eye * w["total"] + moved[:, :HD]], 0),
                jnp.concatenate([heard[:, HD:], moved[:, HD:]], 0),
            )
        )
    for b in range(count):
        at = slice(b * BLOCK, (b + 1) * BLOCK)
        reads = []
        locals_ = []
        for h in range(heads):
            maps, adds = steps[b * heads + h]
            new = fine_dot(maps, state[h])
            added = new[:, HD:] + adds
            reads.append(new[:BLOCK, :HD])
            locals_.append(added[:BLOCK])
            state[h] = jnp.concatenate([new[BLOCK:, :HD], added[BLOCK:]], 1)
        read[at, :] = jnp.concatenate(reads, 1)
        local_out[at, :] = jnp.concatenate(locals_, 1)
    for h in range(heads):
        inc[h] = state[h]
        inc_send[h] = state[h].astype(jnp.bfloat16)


def round_kernel(later, came, inc, exc, inc_out, exc_out, send_out):
    heads, rows, lanes = inc.shape
    go = later[0] > 0
    right = iota((2 * rows, lanes), 1) >= HD
    for h in range(heads):
        old = jnp.concatenate([inc[h], exc[h]], 0)
        high, low = halves(old[:, :HD])
        new = mm(high, came[h]) + mm(low, came[h]) + jnp.where(right, old, 0.0)
        new = jnp.where(go, new, old)
        inc_out[h] = new[:rows]
        exc_out[h] = new[rows:]
        send_out[h] = new[:rows].astype(jnp.bfloat16)


def readout_kernel(read, local_out, exc, gain, out):
    first = exc[0][:, HD:]
    second = exc[1][:, HD:]
    zero = jnp.zeros_like(first)
    state = jnp.concatenate(
        [jnp.concatenate([first, zero], 1), jnp.concatenate([zero, second], 1)], 0
    )
    seen = fine_dot(read[...], state) + local_out[...]
    center = seen - head_sums(seen) / HD
    spread = head_sums(center * center) / HD
    out[...] = (center * lax.rsqrt(spread + 1.0) * gain[...]).astype(jnp.bfloat16)


def pack_kernel(place, gate, up, out_weight, p0, p1, p2, p3):
    side = 4
    length = gate.shape[0] // side
    for ahead, p in enumerate((p0, p1, p2, p3)):
        target = (place[0] + ahead) % side
        at = pl.ds(pl.multiple_of(target * length, length), length)
        p[:length, :] = jnp.concatenate([gate[at, :], up[at, :]], axis=1)
        for c in range(length // 128):
            tile = pl.ds(pl.multiple_of(target * length + c * 128, 128), 128)
            p[length + c * 128 : length + (c + 1) * 128, :] = out_weight[:, tile]


def product_kernel(m0, m1, m2, m3, w0, w1, w2, w3, out):
    rows = jnp.concatenate([m[...] for m in (m0, m1, m2, m3)], 1)
    peers, each, columns = out.shape
    top = w0.shape[0] - columns
    for c in range(columns // 256):
        tiles = []
        for w in (w0, w1, w2, w3):
            low = top + c * 256
            tiles.append(jnp.concatenate([w[low : low + 128, :], w[low + 128 : low + 256, :]], 1))
        made = mm(rows, jnp.concatenate(tiles, 0)).astype(jnp.bfloat16)
        for p in range(peers):
            out[p, :, c * 256 : (c + 1) * 256] = made[p * each : (p + 1) * each]


def finish_kernel(tiles, out):
    side = 4
    width = tiles.shape[2]
    for y in range(side):
        total = tiles[side * y].astype(jnp.float32)
        for x in range(1, side):
            total += tiles[side * y + x].astype(jnp.float32)
        out[:, y * width : (y + 1) * width] = total.astype(jnp.bfloat16)


def turned(shard, axis, back):
    n = lax.axis_size(axis)
    return lax.ppermute(shard, axis, [(i, (i + back) % n) for i in range(n)])


def local(
    receptance,
    key_in,
    value_in,
    decay_in,
    rate_in,
    norm_gain,
    out_weight,
    moe_in,
    ffn_gain,
    routes,
    route_weights,
    gate_weight,
    up_weight,
    down_weight,
):
    f32 = jnp.float32
    rows, features = moe_in.shape
    tp = lax.axis_size(TP)
    side = lax.axis_size("tp_y")
    width = features // tp
    row_place = lax.axis_index("tp_y").astype(jnp.int32).reshape(1)
    total = EXPERTS * SLOT
    share_rows = EXPERTS * CAP // side
    outgoing, rank, share = call(
        prep_kernel,
        (shape((total, 128)), shape((EXPERTS, rows), f32), shape((EXPERTS, rows), f32)),
        lax.axis_index(TP).astype(jnp.int32).reshape(1),
        moe_in,
        ffn_gain.reshape(1, features),
        routes.T,
        route_weights.T,
        scalars=1,
    )
    arrived = exchanged(outgoing.reshape(EXPERTS, SLOT, 128), EP)
    packs = call(
        pack_kernel,
        [shape((2 * features // side, 128))] * side,
        row_place,
        gate_weight[0],
        up_weight[0],
        out_weight,
        scalars=1,
    )
    moved = [packs[0]] + [turned(packs[k], "tp_y", k) for k in range(1, side)]

    tokens, columns = receptance.shape
    heads = columns // HD
    pack = (heads, HD, 2 * HD)
    inc, send, read, local_out = call(
        tables_kernel,
        (shape(pack, f32), shape(pack), shape((tokens, columns), f32), shape((tokens, columns), f32)),
        receptance,
        key_in,
        value_in,
        decay_in,
        rate_in,
    )
    eye = jnp.concatenate([jnp.eye(HD, dtype=f32), jnp.zeros((HD, HD), f32)], 1)
    exc = jnp.broadcast_to(eye, pack)
    peers, position = (lax.axis_size(EP), lax.axis_index(EP))
    shift = 1
    while shift < peers:
        came = lax.ppermute(send, EP, [(i, i + shift) for i in range(peers - shift)])
        inc, exc, send = call(
            round_kernel,
            (shape(pack, f32), shape(pack, f32), shape(pack)),
            (position >= shift).astype(jnp.int32).reshape(1),
            came,
            inc,
            exc,
            scalars=1,
        )
        shift = 2 * shift
    mixed = call(
        readout_kernel,
        shape((tokens, columns)),
        read,
        local_out,
        exc,
        norm_gain.reshape(1, columns),
    )
    mixes = [mixed] + [turned(mixed, "tp_y", k) for k in range(1, side)]
    product = call(
        product_kernel, shape((tp, tokens // tp, features // side)), *mixes, *moved
    )

    gathered = sent_to_all(arrived.reshape(total, 128), "tp_x")
    wide = side * 128
    partial = call(
        gate_up_kernel,
        shape((side, share_rows, wide)),
        row_place,
        gathered,
        *moved,
        scalars=1,
        scratch=[pltpu.VMEM((side, features // side, 128), jnp.bfloat16)],
    )
    parts = exchanged(partial, "tp_y")
    hidden = call(hidden_kernel, shape((tp, share_rows, wide // 2)), parts)
    everyone = exchanged(hidden, TP)
    result = call(down_kernel, shape((total, 128)), everyone, down_weight[0])
    returned = exchanged(result.reshape(EXPERTS, SLOT, 128), EP)
    tiles = exchanged(product, TP)
    moe_out = call(combine_kernel, shape((rows, width)), returned.reshape(total, 128), rank, share)
    mixer_out = call(
        finish_kernel, shape((tokens // tp, side * product.shape[2])), tiles
    )
    return (mixer_out, moe_out)


def solution(mesh):
    finer = Mesh(mesh.devices.reshape(16, 2, 4, 4), EP_TP)
    placed = (
        P(EP, TP),
        P(EP, TP),
        P(EP, TP),
        P(EP, TP),
        P(EP, TP),
        P(TP),
        P(TP, None),
        P(EP, None),
        P(),
        P(EP, None),
        P(EP, None),
        P(EP, None, TP),
        P(EP, None, TP),
        P(EP, None, TP),
    )
    return jax.shard_map(
        local, mesh=finer, in_specs=placed, out_specs=(P(EP_TP, None), P(EP, TP)), check_vma=False
    )
```

time: 234 us -> 253 us (1.081)
  blocking collectives: 0 us -> 53.6 us
  Pallas kernels: 15.5 us -> 42.7 us
  matrix products: 25.5 us -> 0 us
  waiting for transfers between devices: 73.3 us -> 57.8 us
  local copies, waits for them, and re-layouts: 21.3 us -> 9.59 us
  other arithmetic: 7.85 us -> 0.02 us
    all_to_all x0 -> x2, blocking collectives: none -> 53.6 us  [exchanged(): return lax.all_to_all(tiles, axis, split_axis=0, concat_axis=0, tiled=True)]
    all_to_all x7 -> x4, waiting for transfers between devices: 68.2 us -> 28.6 us  [exchanged(): return lax.all_to_all(tiles, axis, split_axis=0, concat_axis=0, tiled=True)]
    pallas_call x5 -> x15, Pallas kernels: 15.5 us -> 42.7 us  [call(): pl.pallas_call(kernel, out_shape=outs, in_specs=[pl.BlockSpec(memory_spac...]
    dot_general x43 -> x0, matrix products: 25.5 us -> none  [the longest x42 23.4 us: einsum_exact(): return jnp.einsum(form, left, right, precision=EXACT_MATMUL)]
    ppermute x5 -> x11, waiting for transfers between devices: 5.03 us -> 29.2 us  [the longest x6 22.7 us: turned(): return lax.ppermute(shard, axis, [(i, (i + back) % n) for i in range(n)])]
    all_to_all x7 -> x4, starting transfers between devices: 51.6 us -> 36.9 us  [exchanged(): return lax.all_to_all(tiles, axis, split_axis=0, concat_axis=0, tiled=True)]
    ppermute x5 -> x11, starting transfers between devices: 36 us -> 49.7 us  [the longest x5 28.7 us: local(): lax.ppermute(send, EP, [(i, i + shift) for i in range(peers - shift)])]
    dynamic_slice x2 -> x0, local copies, waits for them, and re-layouts: 2.83 us -> none  [the longest x1 1.5 us: expert_half(): lax.dynamic_slice_in_dim(moe_in, at, width, 1)]
  transfers between devices with their start and end apart: 12 -> 15, of which waited for: 7 -> 11; matrix products, arithmetic and copies ran while one was open for 14% -> 1% of each run, Pallas kernels for 3% -> 12%
where the time goes in v2:
time: 253 us; the launch traced here: 251 us
  starting transfers between devices  86.6 us (34%)
  waiting for transfers between devices  57.8 us (23%)
  blocking collectives  53.6 us (21%)
  Pallas kernels  42.7 us (17%)
  local copies, waits for them, and re-layouts  9.59 us (4%)
    all_to_all x2, blocking collectives, exchanged(): return lax.all_to_all(tiles, axis, split_axis=0, concat_axis=0, tiled=True)  53.6 us
    pallas_call x15, Pallas kernels, call(): pl.pallas_call(kernel, out_shape=outs, in_specs=[pl.BlockSpec(memory_spac...  42.7 us
    all_to_all x4, starting transfers between devices, exchanged(): return lax.all_to_all(tiles, axis, split_axis=0, concat_axis=0, tiled=True)  36.9 us
    ppermute x5, starting transfers between devices, local(): lax.ppermute(send, EP, [(i, i + shift) for i in range(peers - shift)])  28.7 us
    all_to_all x4, waiting for transfers between devices, exchanged(): return lax.all_to_all(tiles, axis, split_axis=0, concat_axis=0, tiled=True)  28.6 us
    ppermute x6, waiting for transfers between devices, turned(): return lax.ppermute(shard, axis, [(i, (i + back) % n) for i in range(n)])  22.7 us
    ppermute x6, starting transfers between devices, turned(): return lax.ppermute(shard, axis, [(i, (i + back) % n) for i in range(n)])  21 us
    unnamed x36, local copies, waits for them, and re-layouts  7.69 us
  transfers between devices with their start and end apart: 15, of which 11 were waited for; matrix products, arithmetic and copies ran while one was open for 1% of the time, Pallas kernels for 12%

profile of v2, /device:TPU:1, one launch (start us, length us, event | category | flops | bytes accessed | tf_op | source)
XLA Modules:
  0.0 251.2 jit_solution(178122390550969602)
XLA Ops:
  0.6 2.9 %shard_map.159 = (bf16[1280,128]{1,0:T(8,128)(2,1)}, f32[32,128]{1,0:T(8,128)}, f32[32,128]{1,0:T(8,128)}) custom-call(s32[1]{0:T(128)} %bitcast.9.place, bf16[128,4096]{1,0:T(8,128)(2,1)} %x.3, f32[1,4096]{1,0:T(1,128)} %bitcast.25, s32[4,128]{1,0:T(4,128)} %bitcast.26, f32[4,128]{1,0:T(4,128)} %bitcast.27), custom_call_target="tpu_custom_call" | custom-call | tf_op jit(solution)/shard_map/pallas_call | solution.py:54
  3.5 41.7 %all_to_all.30 = bf16[32,40,128]{2,1,0:T(8,128)(2,1)S(1)} all-to-all(bf16[32,40,128]{2,1,0:T(8,128)(2,1)} %bitcast.24), channel_id=1, replica_groups=mesh['ep_0'=16,'ep_1'=2,'tp_y'=4,'tp_x'=4] {'ep_0','ep_1'}, dimensions={0} | all-to-all | bytes 655360 | tf_op jit(solution)/shard_map/all_to_all | solution.py:180
  46.5 4.1 %all-to-all-start.2 = ((bf16[4,1280,128]{2,1,0:T(8,128)(2,1)}), bf16[4,1280,128]{2,1,0:T(8,128)(2,1)S(1)}, u32[]{:S(2)}, u32[]{:S(2)}) async-start(bf16[4,1280,128]{2,1,0:T(8,128)(2,1)} %broadcast_in_dim.8), calls=%async_computation.2 | async-start | bytes 2621440 | tf_op jit(solution)/shard_map/all_to_all | solution.py:180
  53.3 3.5 %shard_map.156 = (bf16[2048,128]{1,0:T(8,128)(2,1)}, bf16[2048,128]{1,0:T(8,128)(2,1)}, bf16[2048,128]{1,0:T(8,128)(2,1)}, bf16[2048,128]{1,0:T(8,128)(2,1)}) custom-call(s32[1]{0:T(128)} %bitcast.6.place, bf16[4096,64]{1,0:T(8,128)(2,1)} %bitcast.18, bf16[4096,64]{1,0:T(8,128)(2,1)} %bitcast.19, bf16[128,4096]{1,0:T(8,128)(2,1)} %out_weight.1), custom_call_target="tpu_custom_call" | custom-call | tf_op jit(solution)/shard_map/pallas_call | solution.py:54
  56.8 4.6 %collective-permute-start.10 = (bf16[2048,128]{1,0:T(8,128)(2,1)}, bf16[2048,128]{1,0:T(8,128)(2,1)S(1)}, u32[]{:S(2)}, u32[]{:S(2)}) collective-permute-start(bf16[2048,128]{1,0:T(8,128)(2,1)} %get-tuple-element.46), channel_id=1, source_target_pairs={{0,12},{4,0},{8,4},{12,8},{1,13},{5,1},{9,5},{13,9},{2,14},{6,2},{... | collective-permute-start | bytes 1572872 | tf_op jit(solution)/shard_map/ppermute | solution.py:365
  61.5 1.9 collective-permute-start.8
  63.4 3.5 %collective-permute-start.9 = (bf16[2048,128]{1,0:T(8,128)(2,1)}, bf16[2048,128]{1,0:T(8,128)(2,1)S(1)}, u32[]{:S(2)}, u32[]{:S(2)}) collective-permute-start(bf16[2048,128]{1,0:T(8,128)(2,1)} %get-tuple-element.45), channel_id=1, source_target_pairs={{0,8},{4,12},{8,0},{12,4},{1,9},{5,13},{9,1},{13,5},{2,10},{6,14},... | collective-permute-start | bytes 1572872 | tf_op jit(solution)/shard_map/ppermute | solution.py:365
  66.9 6.2 %collective-permute-done.10.w3 = bf16[2048,128]{1,0:T(8,128)(2,1)S(1)} collective-permute-done((bf16[2048,128]{1,0:T(8,128)(2,1)}, bf16[2048,128]{1,0:T(8,128)(2,1)S(1)}, u32[]{:S(2)}, u32[]{:S(2)}) %collective-permute-start.10) | collective-permute-done | bytes 524320 | tf_op jit(solution)/shard_map/ppermute | solution.py:365
  73.1 4.9 %collective-permute-done.8.w1 = bf16[2048,128]{1,0:T(8,128)(2,1)S(1)} collective-permute-done((bf16[2048,128]{1,0:T(8,128)(2,1)}, bf16[2048,128]{1,0:T(8,128)(2,1)S(1)}, u32[]{:S(2)}, u32[]{:S(2)}) %collective-permute-start.8) | collective-permute-done | bytes 524320 | tf_op jit(solution)/shard_map/ppermute | solution.py:365
  78.0 9.2 %collective-permute-done.9.w2 = bf16[2048,128]{1,0:T(8,128)(2,1)S(1)} collective-permute-done((bf16[2048,128]{1,0:T(8,128)(2,1)}, bf16[2048,128]{1,0:T(8,128)(2,1)S(1)}, u32[]{:S(2)}, u32[]{:S(2)}) %collective-permute-start.9) | collective-permute-done | bytes 524320 | tf_op jit(solution)/shard_map/ppermute | solution.py:365
  88.5 4.7 %shard_map.160 = bf16[4,160,512]{2,1,0:T(8,128)(2,1)} custom-call(s32[1]{0:T(128)} %bitcast.6.place, bf16[4,1280,128]{2,1,0:T(8,128)(2,1)} %copy-done.1, bf16[2048,128]{1,0:T(8,128)(2,1)} %get-tuple-element.43.w0, bf16[2048,128]{1,0:T(8,128)(2,1)} %copy-done.4, bf16[2048,128]{1,0:T(8,128)(2,1)} %copy-done.5, bf16[2048,128]{1,0:T(8,128)(2,1)} %copy-done.3), custom_call_target="tpu_custom_call" | custom-call | tf_op jit(solution)/shard_map/pallas_call | solution.py:54
  93.2 11.9 %all_to_all.31.parts = bf16[4,160,512]{2,1,0:T(8,128)(2,1)} all-to-all(bf16[4,160,512]{2,1,0:T(8,128)(2,1)} %shard_map.160), channel_id=1, replica_groups=mesh['ep_0'=16,'ep_1'=2,'tp_y'=4,'tp_x'=4] {'tp_y'}, dimensions={0} | all-to-all | bytes 1310720 | tf_op jit(solution)/shard_map/all_to_all | solution.py:180
  105.0 2.6 %shard_map.161 = bf16[16,160,256]{2,1,0:T(8,128)(2,1)} custom-call(bf16[4,160,512]{2,1,0:T(8,128)(2,1)} %all_to_all.31.parts), custom_call_target="tpu_custom_call" | custom-call | tf_op jit(solution)/shard_map/pallas_call | solution.py:54
  107.6 4.7 %all-to-all-start.4 = ((bf16[16,160,256]{2,1,0:T(8,128)(2,1)}), bf16[16,160,256]{2,1,0:T(8,128)(2,1)S(1)}, u32[]{:S(2)}, u32[]{:S(2)}) async-start(bf16[16,160,256]{2,1,0:T(8,128)(2,1)} %shard_map.161), calls=%async_computation.4 | async-start | bytes 2621440 | tf_op jit(solution)/shard_map/all_to_all | solution.py:180
  112.3 7.8 %shard_map.149 = (f32[2,64,128]{2,1,0:T(8,128)}, bf16[2,64,128]{2,1,0:T(8,128)(2,1)}, f32[256,128]{1,0:T(8,128)}, f32[256,128]{1,0:T(8,128)}) custom-call(bf16[256,128]{1,0:T(8,128)(2,1)} %receptance.1, bf16[256,128]{1,0:T(8,128)(2,1)} %key_in.1, bf16[256,128]{1,0:T(8,128)(2,1)} %value_in.1, bf16[256,128]{1,0:T(8,128)(2,1)} %decay_in.1, bf16[256,128]{1,0:T(8,128)(2,1)} %rate_in.1), custom_call_target="tpu_custom_call" | custom-call | tf_op jit(solution)/shard_map/pallas_call | solution.py:54
  120.1 5.9 %collective-permute-start = (bf16[2,64,128]{2,1,0:T(8,128)(2,1)}, bf16[2,64,128]{2,1,0:T(8,128)(2,1)S(1)}, u32[]{:S(2)}, u32[]{:S(2)}) collective-permute-start(bf16[2,64,128]{2,1,0:T(8,128)(2,1)} %get-tuple-element.28), channel_id=1, source_target_pairs={{0,16},{16,32},{32,48},{48,64},{64,80},{80,96},{96,112},{112,128},... | collective-permute-start | bytes 98312 | tf_op jit(solution)/shard_map/ppermute | solution.py:431
  129.6 5.5 %collective-permute-start.1 = (bf16[2,64,128]{2,1,0:T(8,128)(2,1)}, bf16[2,64,128]{2,1,0:T(8,128)(2,1)S(1)}, u32[]{:S(2)}, u32[]{:S(2)}) collective-permute-start(bf16[2,64,128]{2,1,0:T(8,128)(2,1)} %get-tuple-element.30), channel_id=1, source_target_pairs={{0,32},{16,48},{32,64},{48,80},{64,96},{80,112},{96,128},{112,144}... | collective-permute-start | bytes 98312 | tf_op jit(solution)/shard_map/ppermute | solution.py:431
  138.7 3.6 %collective-permute-start.2 = (bf16[2,64,128]{2,1,0:T(8,128)(2,1)}, bf16[2,64,128]{2,1,0:T(8,128)(2,1)S(1)}, u32[]{:S(2)}, u32[]{:S(2)}) collective-permute-start(bf16[2,64,128]{2,1,0:T(8,128)(2,1)} %get-tuple-element.33), channel_id=1, source_target_pairs={{0,64},{16,80},{32,96},{48,112},{64,128},{80,144},{96,160},{112,17... | collective-permute-start | bytes 98312 | tf_op jit(solution)/shard_map/ppermute | solution.py:431
  145.9 6.0 %collective-permute-start.3 = (bf16[2,64,128]{2,1,0:T(8,128)(2,1)}, bf16[2,64,128]{2,1,0:T(8,128)(2,1)S(1)}, u32[]{:S(2)}, u32[]{:S(2)}) collective-permute-start(bf16[2,64,128]{2,1,0:T(8,128)(2,1)} %get-tuple-element.36), channel_id=1, source_target_pairs={{0,128},{16,144},{32,160},{48,176},{64,192},{80,208},{96,224},{112... | collective-permute-start | bytes 98312 | tf_op jit(solution)/shard_map/ppermute | solution.py:431
  155.6 7.7 %collective-permute-start.4 = (bf16[2,64,128]{2,1,0:T(8,128)(2,1)}, bf16[2,64,128]{2,1,0:T(8,128)(2,1)S(1)}, u32[]{:S(2)}, u32[]{:S(2)}) collective-permute-start(bf16[2,64,128]{2,1,0:T(8,128)(2,1)} %get-tuple-element.39), channel_id=1, source_target_pairs={{0,256},{16,272},{32,288},{48,304},{64,320},{80,336},{96,352},{112... | collective-permute-start | bytes 98312 | tf_op jit(solution)/shard_map/ppermute | solution.py:431
  166.9 2.1 shard_map.155.m0
  169.0 3.5 %collective-permute-start.5 = (bf16[256,128]{1,0:T(8,128)(2,1)}, bf16[256,128]{1,0:T(8,128)(2,1)S(1)}, u32[]{:S(2)}, u32[]{:S(2)}) collective-permute-start(bf16[256,128]{1,0:T(8,128)(2,1)} %shard_map.155.m0), channel_id=1, source_target_pairs={{0,4},{4,8},{8,12},{12,0},{1,5},{5,9},{9,13},{13,1},{2,6},{6,10},{... | collective-permute-start | bytes 196616 | tf_op jit(solution)/shard_map/ppermute | solution.py:365
  172.6 4.3 %collective-permute-start.6 = (bf16[256,128]{1,0:T(8,128)(2,1)}, bf16[256,128]{1,0:T(8,128)(2,1)S(1)}, u32[]{:S(2)}, u32[]{:S(2)}) collective-permute-start(bf16[256,128]{1,0:T(8,128)(2,1)} %shard_map.155.m0), channel_id=1, source_target_pairs={{0,8},{4,12},{8,0},{12,4},{1,9},{5,13},{9,1},{13,5},{2,10},{6,14},... | collective-permute-start | bytes 196616 | tf_op jit(solution)/shard_map/ppermute | solution.py:365
  176.9 3.1 %collective-permute-start.7 = (bf16[256,128]{1,0:T(8,128)(2,1)}, bf16[256,128]{1,0:T(8,128)(2,1)S(1)}, u32[]{:S(2)}, u32[]{:S(2)}) collective-permute-start(bf16[256,128]{1,0:T(8,128)(2,1)} %shard_map.155.m0), channel_id=1, source_target_pairs={{0,12},{4,0},{8,4},{12,8},{1,13},{5,1},{9,5},{13,9},{2,14},{6,2},{... | collective-permute-start | bytes 196616 | tf_op jit(solution)/shard_map/ppermute | solution.py:365
  180.0 2.4 collective-permute-done.7.m3
  183.0 2.9 %shard_map.157 = bf16[16,16,1024]{2,1,0:T(8,128)(2,1)} custom-call(bf16[256,128]{1,0:T(8,128)(2,1)} %shard_map.155.m0, bf16[256,128]{1,0:T(8,128)(2,1)} %copy-done.9, bf16[256,128]{1,0:T(8,128)(2,1)} %copy-done.10, bf16[256,128]{1,0:T(8,128)(2,1)} %copy-done.11, bf16[2048,128]{1,0:T(8,128)(2,1)} %get-tuple-element.43.w0, bf16[2048,128]{1,0:T(8,128)(2,1)} %copy-done.4, ...), custom_call_target="tpu_custom_call" | custom-call | tf_op jit(solution)/shard_map/pallas_call | solution.py:54
  185.9 5.9 %all-to-all-start = ((bf16[16,16,1024]{2,1,0:T(8,128)(2,1)}), bf16[16,16,1024]{2,1,0:T(8,128)(2,1)S(1)}, u32[]{:S(2)}, u32[]{:S(2)}) async-start(bf16[16,16,1024]{2,1,0:T(8,128)(2,1)} %shard_map.157), calls=%async_computation | async-start | bytes 1048576 | tf_op jit(solution)/shard_map/all_to_all | solution.py:180
  191.8 3.6 %shard_map.162 = bf16[1280,128]{1,0:T(8,128)(2,1)} custom-call(bf16[16,160,256]{2,1,0:T(8,128)(2,1)} %copy-done, bf16[1024,256]{1,0:T(8,128)(2,1)} %bitcast.23), custom_call_target="tpu_custom_call" | custom-call | tf_op jit(solution)/shard_map/pallas_call | solution.py:54
  195.4 5.4 %all-to-all-done.tiles = bf16[16,16,1024]{2,1,0:T(8,128)(2,1)S(1)} async-done(((bf16[16,16,1024]{2,1,0:T(8,128)(2,1)}), bf16[16,16,1024]{2,1,0:T(8,128)(2,1)S(1)}, u32[]{:S(2)}, u32[]{:S(2)}) %all-to-all-start) | async-done | bytes 524320 | tf_op jit(solution)/shard_map/all_to_all | solution.py:180
  200.8 22.2 %all-to-all-start.5 = ((bf16[32,40,128]{2,1,0:T(8,128)(2,1)}), bf16[32,40,128]{2,1,0:T(8,128)(2,1)S(1)}, u32[]{:S(2)}, u32[]{:S(2)}) async-start(bf16[32,40,128]{2,1,0:T(8,128)(2,1)} %bitcast.22), calls=%async_computation.5 | async-start | bytes 655360 | tf_op jit(solution)/shard_map/all_to_all | solution.py:180
  224.8 23.2 %all-to-all-done.5 = bf16[32,40,128]{2,1,0:T(8,128)(2,1)S(1)} async-done(((bf16[32,40,128]{2,1,0:T(8,128)(2,1)}), bf16[32,40,128]{2,1,0:T(8,128)(2,1)S(1)}, u32[]{:S(2)}, u32[]{:S(2)}) %all-to-all-start.5) | async-done | bytes 327712 | tf_op jit(solution)/shard_map/all_to_all | solution.py:180
  248.7 2.5 shard_map.163
  (55 shorter events, 26.4 us)
Async XLA Ops:
  46.5 4.1 %copy-start.7 = (bf16[1,4096,64]{1,2,0:T(8,128)(2,1)S(1)}, bf16[1,4096,64]{1,2,0:T(8,128)(2,1)}, u32[]{:S(2)}) copy-start(bf16[1,4096,64]{1,2,0:T(8,128)(2,1)} %param.25) | copy-start | bytes 1572868
  46.5 40.7 %all-to-all-start.2 = ((bf16[4,1280,128]{2,1,0:T(8,128)(2,1)}), bf16[4,1280,128]{2,1,0:T(8,128)(2,1)S(1)}, u32[]{:S(2)}, u32[]{:S(2)}) async-start(bf16[4,1280,128]{2,1,0:T(8,128)(2,1)} %broadcast_in_dim.8), calls=%async_computation.2 | async-start | bytes 2621440 | tf_op jit(solution)/shard_map/all_to_all | solution.py:180
  50.7 1.3 copy-start.8
  56.8 16.3 %collective-permute-start.10 = (bf16[2048,128]{1,0:T(8,128)(2,1)}, bf16[2048,128]{1,0:T(8,128)(2,1)S(1)}, u32[]{:S(2)}, u32[]{:S(2)}) collective-permute-start(bf16[2048,128]{1,0:T(8,128)(2,1)} %get-tuple-element.46), channel_id=1, source_target_pairs={{0,12},{4,0},{8,4},{12,8},{1,13},{5,1},{9,5},{13,9},{2,14},{6,2},{... | collective-permute-start | bytes 1572872 | tf_op jit(solution)/shard_map/ppermute | solution.py:365
  61.5 16.5 %collective-permute-start.8 = (bf16[2048,128]{1,0:T(8,128)(2,1)}, bf16[2048,128]{1,0:T(8,128)(2,1)S(1)}, u32[]{:S(2)}, u32[]{:S(2)}) collective-permute-start(bf16[2048,128]{1,0:T(8,128)(2,1)} %get-tuple-element.44), channel_id=1, source_target_pairs={{0,4},{4,8},{8,12},{12,0},{1,5},{5,9},{9,13},{13,1},{2,6},{6,10},{... | collective-permute-start | bytes 1572872 | tf_op jit(solution)/shard_map/ppermute | solution.py:365
  63.4 23.8 %collective-permute-start.9 = (bf16[2048,128]{1,0:T(8,128)(2,1)}, bf16[2048,128]{1,0:T(8,128)(2,1)S(1)}, u32[]{:S(2)}, u32[]{:S(2)}) collective-permute-start(bf16[2048,128]{1,0:T(8,128)(2,1)} %get-tuple-element.45), channel_id=1, source_target_pairs={{0,8},{4,12},{8,0},{12,4},{1,9},{5,13},{9,1},{13,5},{2,10},{6,14},... | collective-permute-start | bytes 1572872 | tf_op jit(solution)/shard_map/ppermute | solution.py:365
  73.1 14.2 %copy-start.3 = (bf16[2048,128]{1,0:T(8,128)(2,1)}, bf16[2048,128]{1,0:T(8,128)(2,1)S(1)}, u32[]{:S(2)}) copy-start(bf16[2048,128]{1,0:T(8,128)(2,1)S(1)} %collective-permute-done.10.w3) | copy-start | bytes 1572868
  78.0 9.2 %copy-start.4 = (bf16[2048,128]{1,0:T(8,128)(2,1)}, bf16[2048,128]{1,0:T(8,128)(2,1)S(1)}, u32[]{:S(2)}) copy-start(bf16[2048,128]{1,0:T(8,128)(2,1)S(1)} %collective-permute-done.8.w1) | copy-start | bytes 1572868
  87.2 0.8 copy-start.5
  87.2 1.3 copy-start.1
  107.6 78.2 %all-to-all-start.4 = ((bf16[16,160,256]{2,1,0:T(8,128)(2,1)}), bf16[16,160,256]{2,1,0:T(8,128)(2,1)S(1)}, u32[]{:S(2)}, u32[]{:S(2)}) async-start(bf16[16,160,256]{2,1,0:T(8,128)(2,1)} %shard_map.161), calls=%async_computation.4 | async-start | bytes 2621440 | tf_op jit(solution)/shard_map/all_to_all | solution.py:180
  120.1 7.2 %collective-permute-start = (bf16[2,64,128]{2,1,0:T(8,128)(2,1)}, bf16[2,64,128]{2,1,0:T(8,128)(2,1)S(1)}, u32[]{:S(2)}, u32[]{:S(2)}) collective-permute-start(bf16[2,64,128]{2,1,0:T(8,128)(2,1)} %get-tuple-element.28), channel_id=1, source_target_pairs={{0,16},{16,32},{32,48},{48,64},{64,80},{80,96},{96,112},{112,128},... | collective-permute-start | bytes 98312 | tf_op jit(solution)/shard_map/ppermute | solution.py:431
  127.3 0.6 copy-start.12
  129.6 6.8 %collective-permute-start.1 = (bf16[2,64,128]{2,1,0:T(8,128)(2,1)}, bf16[2,64,128]{2,1,0:T(8,128)(2,1)S(1)}, u32[]{:S(2)}, u32[]{:S(2)}) collective-permute-start(bf16[2,64,128]{2,1,0:T(8,128)(2,1)} %get-tuple-element.30), channel_id=1, source_target_pairs={{0,32},{16,48},{32,64},{48,80},{64,96},{80,112},{96,128},{112,144}... | collective-permute-start | bytes 98312 | tf_op jit(solution)/shard_map/ppermute | solution.py:431
  136.4 0.6 copy-start.14
  138.7 4.9 %collective-permute-start.2 = (bf16[2,64,128]{2,1,0:T(8,128)(2,1)}, bf16[2,64,128]{2,1,0:T(8,128)(2,1)S(1)}, u32[]{:S(2)}, u32[]{:S(2)}) collective-permute-start(bf16[2,64,128]{2,1,0:T(8,128)(2,1)} %get-tuple-element.33), channel_id=1, source_target_pairs={{0,64},{16,80},{32,96},{48,112},{64,128},{80,144},{96,160},{112,17... | collective-permute-start | bytes 98312 | tf_op jit(solution)/shard_map/ppermute | solution.py:431
  143.6 0.6 copy-start.15
  145.9 7.3 %collective-permute-start.3 = (bf16[2,64,128]{2,1,0:T(8,128)(2,1)}, bf16[2,64,128]{2,1,0:T(8,128)(2,1)S(1)}, u32[]{:S(2)}, u32[]{:S(2)}) collective-permute-start(bf16[2,64,128]{2,1,0:T(8,128)(2,1)} %get-tuple-element.36), channel_id=1, source_target_pairs={{0,128},{16,144},{32,160},{48,176},{64,192},{80,208},{96,224},{112... | collective-permute-start | bytes 98312 | tf_op jit(solution)/shard_map/ppermute | solution.py:431
  153.3 0.6 copy-start.16
  155.6 9.1 %collective-permute-start.4 = (bf16[2,64,128]{2,1,0:T(8,128)(2,1)}, bf16[2,64,128]{2,1,0:T(8,128)(2,1)S(1)}, u32[]{:S(2)}, u32[]{:S(2)}) collective-permute-start(bf16[2,64,128]{2,1,0:T(8,128)(2,1)} %get-tuple-element.39), channel_id=1, source_target_pairs={{0,256},{16,272},{32,288},{48,304},{64,320},{80,336},{96,352},{112... | collective-permute-start | bytes 98312 | tf_op jit(solution)/shard_map/ppermute | solution.py:431
  164.6 0.6 copy-start.13
  169.0 11.0 %collective-permute-start.5 = (bf16[256,128]{1,0:T(8,128)(2,1)}, bf16[256,128]{1,0:T(8,128)(2,1)S(1)}, u32[]{:S(2)}, u32[]{:S(2)}) collective-permute-start(bf16[256,128]{1,0:T(8,128)(2,1)} %shard_map.155.m0), channel_id=1, source_target_pairs={{0,4},{4,8},{8,12},{12,0},{1,5},{5,9},{9,13},{13,1},{2,6},{6,10},{... | collective-permute-start | bytes 196616 | tf_op jit(solution)/shard_map/ppermute | solution.py:365
  172.6 7.4 %collective-permute-start.6 = (bf16[256,128]{1,0:T(8,128)(2,1)}, bf16[256,128]{1,0:T(8,128)(2,1)S(1)}, u32[]{:S(2)}, u32[]{:S(2)}) collective-permute-start(bf16[256,128]{1,0:T(8,128)(2,1)} %shard_map.155.m0), channel_id=1, source_target_pairs={{0,8},{4,12},{8,0},{12,4},{1,9},{5,13},{9,1},{13,5},{2,10},{6,14},... | collective-permute-start | bytes 196616 | tf_op jit(solution)/shard_map/ppermute | solution.py:365
  176.9 5.5 %collective-permute-start.7 = (bf16[256,128]{1,0:T(8,128)(2,1)}, bf16[256,128]{1,0:T(8,128)(2,1)S(1)}, u32[]{:S(2)}, u32[]{:S(2)}) collective-permute-start(bf16[256,128]{1,0:T(8,128)(2,1)} %shard_map.155.m0), channel_id=1, source_target_pairs={{0,12},{4,0},{8,4},{12,8},{1,13},{5,1},{9,5},{13,9},{2,14},{6,2},{... | collective-permute-start | bytes 196616 | tf_op jit(solution)/shard_map/ppermute | solution.py:365
  180.0 2.4 copy-start.9
  180.0 2.4 copy-start.10
  182.4 0.6 copy-start.11
  185.9 5.9 %copy-start = (bf16[16,160,256]{2,1,0:T(8,128)(2,1)}, bf16[16,160,256]{2,1,0:T(8,128)(2,1)S(1)}, u32[]{:S(2)}) copy-start(bf16[16,160,256]{2,1,0:T(8,128)(2,1)S(1)} %all-to-all-done.4.hidden) | copy-start | bytes 3932164
  185.9 14.9 %all-to-all-start = ((bf16[16,16,1024]{2,1,0:T(8,128)(2,1)}), bf16[16,16,1024]{2,1,0:T(8,128)(2,1)S(1)}, u32[]{:S(2)}, u32[]{:S(2)}) async-start(bf16[16,16,1024]{2,1,0:T(8,128)(2,1)} %shard_map.157), calls=%async_computation | async-start | bytes 1048576 | tf_op jit(solution)/shard_map/all_to_all | solution.py:180
  200.8 22.2 %copy-start.2 = (bf16[16,16,1024]{2,1,0:T(8,128)(2,1)}, bf16[16,16,1024]{2,1,0:T(8,128)(2,1)S(1)}, u32[]{:S(2)}) copy-start(bf16[16,16,1024]{2,1,0:T(8,128)(2,1)S(1)} %all-to-all-done.tiles) | copy-start | bytes 1572868
  200.8 47.2 %all-to-all-start.5 = ((bf16[32,40,128]{2,1,0:T(8,128)(2,1)}), bf16[32,40,128]{2,1,0:T(8,128)(2,1)S(1)}, u32[]{:S(2)}, u32[]{:S(2)}) async-start(bf16[32,40,128]{2,1,0:T(8,128)(2,1)} %bitcast.22), calls=%async_computation.5 | async-start | bytes 655360 | tf_op jit(solution)/shard_map/all_to_all | solution.py:180
  248.0 0.7 copy-start.6

commit v3 on v2

--- a/solution.py
+++ b/solution.py
@@ -1,3 +1,5 @@
+import functools
+
 import jax
 import jax.numpy as jnp
 from jax import lax
@@ -15,6 +17,7 @@
 CAP = 20
 SLOT = 2 * CAP
 GROUP = 8
+LIMIT = 16 * 1024 * 1024
 
 
 def iota(shape, dim):
@@ -49,13 +52,14 @@
     return dot(ah, bh, dims) + dot(ah, bl, dims) + dot(al, bh, dims)
 
 
-def call(kernel, outs, *args, scalars=0, scratch=()):
+def call(kernel, outs, *args, scalars=0, scratch=(), limit=LIMIT):
     whole = [pl.BlockSpec(memory_space=pltpu.VMEM)] * (len(args) - scalars)
     return pl.pallas_call(
         kernel,
         out_shape=outs,
         in_specs=[pl.BlockSpec(memory_space=pltpu.SMEM)] * scalars + whole,
         scratch_shapes=list(scratch),
+        compiler_params=pltpu.CompilerParams(vmem_limit_bytes=limit),
     )(*args)
 
 
@@ -125,14 +129,14 @@
     side = weights.shape[0]
     for back, w in enumerate((w0, w1, w2, w3)):
         weights[(place[0] + side - back) % side] = w[: weights.shape[1], :]
-    joined = jnp.concatenate([weights[k] for k in range(side)], axis=1)
+    joined = jnp.concatenate([weights[k] for k in range(side)], axis=0)
     for g in range(EXPERTS // GROUP):
         pieces = []
         for k in range(gathered.shape[0]):
             seen = gathered[k, g * GROUP * SLOT : (g + 1) * GROUP * SLOT, :]
             for pick in picks:
                 pieces.append(mm(pick, seen).astype(jnp.bfloat16))
-        out[g] = mm(jnp.concatenate(pieces, axis=1), joined).astype(jnp.bfloat16)
+        out[g] = nt(jnp.concatenate(pieces, axis=1), joined).astype(jnp.bfloat16)
 
 
 def hidden_kernel(parts, out):
@@ -180,10 +184,6 @@
     return lax.all_to_all(tiles, axis, split_axis=0, concat_axis=0, tiled=True)
 
 
-def sent_to_all(shard, axis):
-    return exchanged(jnp.broadcast_to(shard, (lax.axis_size(axis), *shard.shape)), axis)
-
-
 def head_sums(a):
     left = iota(a.shape, 1) < HD
     low = jnp.sum(jnp.where(left, a, 0.0), axis=-1, keepdims=True)
@@ -191,7 +191,7 @@
     return jnp.where(left, low, high)
 
 
-def tables_kernel(receptance, key_in, value_in, decay_in, rate_in, inc, inc_send, read, local_out):
+def tables_kernel(receptance, key_in, value_in, decay_in, rate_in, begun, send, table):
     f32 = jnp.float32
     size = (BLOCK, BLOCK)
     strict = (iota(size, 1) < iota(size, 0)).astype(f32)
@@ -290,64 +290,76 @@
             reads.append(new[:BLOCK, :HD])
             locals_.append(added[:BLOCK])
             state[h] = jnp.concatenate([new[BLOCK:, :HD], added[BLOCK:]], 1)
-        read[at, :] = jnp.concatenate(reads, 1)
-        local_out[at, :] = jnp.concatenate(locals_, 1)
+        table[0, at, :] = jnp.concatenate(reads, 1)
+        table[1, at, :] = jnp.concatenate(locals_, 1)
     for h in range(heads):
-        inc[h] = state[h]
-        inc_send[h] = state[h].astype(jnp.bfloat16)
-
-
-def round_kernel(later, came, inc, exc, inc_out, exc_out, send_out):
-    heads, rows, lanes = inc.shape
-    go = later[0] > 0
-    right = iota((2 * rows, lanes), 1) >= HD
-    for h in range(heads):
-        old = jnp.concatenate([inc[h], exc[h]], 0)
+        begun[h, :HD] = state[h]
+        begun[h, HD:] = jnp.concatenate([eye, zero], 1)
+        send[h] = state[h].astype(jnp.bfloat16)
+
+
+def advanced(later, came, old):
+    right = iota(old.shape, 1) >= HD
+    high, low = halves(old[:, :HD])
+    new = mm(high, came) + mm(low, came) + jnp.where(right, old, 0.0)
+    return jnp.where(later, new, old)
+
+
+def round_kernel(position, came, state, state_out, send_out, *, shift):
+    for h in range(state.shape[0]):
+        new = advanced(position[0] >= shift, came[h], state[h])
+        state_out[h] = new
+        if len(send_out.shape) == 3:
+            send_out[h] = new[:HD].astype(jnp.bfloat16)
+        else:
+            send_out[:, h * HD : (h + 1) * HD] = new[:HD, HD:].astype(jnp.bfloat16)
+
+
+def readout_kernel(position, came, last, table, gain, out, *, shift):
+    later = position[0] >= shift
+    states = []
+    for h in range(last.shape[0]):
+        side = slice(h * HD, (h + 1) * HD)
+        old = last[h, HD:, :]
         high, low = halves(old[:, :HD])
-        new = mm(high, came[h]) + mm(low, came[h]) + jnp.where(right, old, 0.0)
-        new = jnp.where(go, new, old)
-        inc_out[h] = new[:rows]
-        exc_out[h] = new[rows:]
-        send_out[h] = new[:rows].astype(jnp.bfloat16)
-
-
-def readout_kernel(read, local_out, exc, gain, out):
-    first = exc[0][:, HD:]
-    second = exc[1][:, HD:]
+        new = mm(high, came[:, side]) + mm(low, came[:, side]) + old[:, HD:]
+        states.append(jnp.where(later, new, old[:, HD:]))
+    first, second = states
     zero = jnp.zeros_like(first)
     state = jnp.concatenate(
         [jnp.concatenate([first, zero], 1), jnp.concatenate([zero, second], 1)], 0
     )
-    seen = fine_dot(read[...], state) + local_out[...]
+    seen = fine_dot(table[0], state) + table[1]
     center = seen - head_sums(seen) / HD
     spread = head_sums(center * center) / HD
     out[...] = (center * lax.rsqrt(spread + 1.0) * gain[...]).astype(jnp.bfloat16)
 
 
+def copies_kernel(one, out):
+    for k in range(out.shape[0]):
+        out[k] = one[...]
+
+
 def pack_kernel(place, gate, up, out_weight, p0, p1, p2, p3):
     side = 4
-    length = gate.shape[0] // side
+    hidden, features = gate.shape
+    length = features // side
     for ahead, p in enumerate((p0, p1, p2, p3)):
         target = (place[0] + ahead) % side
         at = pl.ds(pl.multiple_of(target * length, length), length)
-        p[:length, :] = jnp.concatenate([gate[at, :], up[at, :]], axis=1)
-        for c in range(length // 128):
-            tile = pl.ds(pl.multiple_of(target * length + c * 128, 128), 128)
-            p[length + c * 128 : length + (c + 1) * 128, :] = out_weight[:, tile]
+        p[:hidden, :] = gate[:, at]
+        p[hidden : 2 * hidden, :] = up[:, at]
+        p[2 * hidden :, :] = out_weight[:, at]
 
 
 def product_kernel(m0, m1, m2, m3, w0, w1, w2, w3, out):
     rows = jnp.concatenate([m[...] for m in (m0, m1, m2, m3)], 1)
-    peers, each, columns = out.shape
-    top = w0.shape[0] - columns
-    for c in range(columns // 256):
-        tiles = []
-        for w in (w0, w1, w2, w3):
-            low = top + c * 256
-            tiles.append(jnp.concatenate([w[low : low + 128, :], w[low + 128 : low + 256, :]], 1))
-        made = mm(rows, jnp.concatenate(tiles, 0)).astype(jnp.bfloat16)
-        for p in range(peers):
-            out[p, :, c * 256 : (c + 1) * 256] = made[p * each : (p + 1) * each]
+    count = rows.shape[1] // 4
+    weights = jnp.concatenate([w[w.shape[0] - count :, :] for w in (w0, w1, w2, w3)], 0)
+    made = mm(rows, weights).astype(jnp.bfloat16)
+    peers, each, _ = out.shape
+    for p in range(peers):
+        out[p] = made[p * each : (p + 1) * each]
 
 
 def finish_kernel(tiles, out):
@@ -398,14 +410,15 @@
         routes.T,
         route_weights.T,
         scalars=1,
+        limit=None,
     )
     arrived = exchanged(outgoing.reshape(EXPERTS, SLOT, 128), EP)
     packs = call(
         pack_kernel,
-        [shape((2 * features // side, 128))] * side,
+        [shape((256, features // side))] * side,
         row_place,
-        gate_weight[0],
-        up_weight[0],
+        gate_weight[0].T,
+        up_weight[0].T,
         out_weight,
         scalars=1,
     )
@@ -414,45 +427,51 @@
     tokens, columns = receptance.shape
     heads = columns // HD
     pack = (heads, HD, 2 * HD)
-    inc, send, read, local_out = call(
+    stack = (heads, 2 * HD, 2 * HD)
+    flat = (tokens, columns)
+    state, send, table = call(
         tables_kernel,
-        (shape(pack, f32), shape(pack), shape((tokens, columns), f32), shape((tokens, columns), f32)),
+        (shape(stack, f32), shape(pack), shape((2, *flat), f32)),
         receptance,
         key_in,
         value_in,
         decay_in,
         rate_in,
     )
-    eye = jnp.concatenate([jnp.eye(HD, dtype=f32), jnp.zeros((HD, HD), f32)], 1)
-    exc = jnp.broadcast_to(eye, pack)
-    peers, position = (lax.axis_size(EP), lax.axis_index(EP))
+    peers = lax.axis_size(EP)
+    position = lax.axis_index(EP).astype(jnp.int32).reshape(1)
     shift = 1
     while shift < peers:
         came = lax.ppermute(send, EP, [(i, i + shift) for i in range(peers - shift)])
-        inc, exc, send = call(
-            round_kernel,
-            (shape(pack, f32), shape(pack, f32), shape(pack)),
-            (position >= shift).astype(jnp.int32).reshape(1),
-            came,
-            inc,
-            exc,
-            scalars=1,
-        )
+        if 2 * shift < peers:
+            state, send = call(
+                functools.partial(round_kernel, shift=shift),
+                (shape(stack, f32), shape(pack if 4 * shift < peers else (HD, 2 * HD))),
+                position,
+                came,
+                state,
+                scalars=1,
+            )
         shift = 2 * shift
     mixed = call(
-        readout_kernel,
-        shape((tokens, columns)),
-        read,
-        local_out,
-        exc,
+        functools.partial(readout_kernel, shift=shift // 2),
+        shape(flat),
+        position,
+        came,
+        state,
+        table,
         norm_gain.reshape(1, columns),
+        scalars=1,
     )
     mixes = [mixed] + [turned(mixed, "tp_y", k) for k in range(1, side)]
     product = call(
         product_kernel, shape((tp, tokens // tp, features // side)), *mixes, *moved
     )
 
-    gathered = sent_to_all(arrived.reshape(total, 128), "tp_x")
+    copies = call(
+        copies_kernel, shape((side, total, 128)), arrived.reshape(total, 128)
+    )
+    gathered = exchanged(copies, "tp_x")
     wide = side * 128
     partial = call(
         gate_up_kernel,
@@ -461,7 +480,7 @@
         gathered,
         *moved,
         scalars=1,
-        scratch=[pltpu.VMEM((side, features // side, 128), jnp.bfloat16)],
+        scratch=[pltpu.VMEM((side, 128, features // side), jnp.bfloat16)],
     )
     parts = exchanged(partial, "tp_y")
     hidden = call(hidden_kernel, shape((tp, share_rows, wide // 2)), parts)

time: 253 us -> 230 us (0.909)
  Pallas kernels: 42.7 us -> 21.9 us
  starting transfers between devices: 86.6 us -> 82.9 us
    pallas_call x15, Pallas kernels: 42.7 us -> 21.9 us  [call(): pl.pallas_call(kernel, out_shape=outs, in_specs=[pl.BlockSpec(memory_spac...]
    ppermute x5, starting transfers between devices: 28.7 us -> 25.4 us  [local(): lax.ppermute(send, EP, [(i, i + shift) for i in range(peers - shift)])]
    unnamed x36 -> x30, local copies, waits for them, and re-layouts: 7.69 us -> 8.74 us
  transfers between devices with their start and end apart: 15 -> 15, of which waited for: 11 -> 12; matrix products, arithmetic and copies ran while one was open for 1% -> 0% of each run, Pallas kernels for 12% -> 5%
where the time goes in v3:
time: 230 us; the launch traced here: 228 us
  starting transfers between devices  82.9 us (36%)
  waiting for transfers between devices  58 us (25%)
  blocking collectives  55.9 us (24%)
  Pallas kernels  21.9 us (10%)
  local copies, waits for them, and re-layouts  8.74 us (4%)
    all_to_all x2, blocking collectives, exchanged(): return lax.all_to_all(tiles, axis, split_axis=0, concat_axis=0, tiled=True)  55.9 us
    all_to_all x4, starting transfers between devices, exchanged(): return lax.all_to_all(tiles, axis, split_axis=0, concat_axis=0, tiled=True)  37.1 us
    all_to_all x4, waiting for transfers between devices, exchanged(): return lax.all_to_all(tiles, axis, split_axis=0, concat_axis=0, tiled=True)  30.1 us
    ppermute x5, starting transfers between devices, local(): lax.ppermute(send, EP, [(i, i + shift) for i in range(peers - shift)])  25.4 us
    ppermute x6, waiting for transfers between devices, turned(): return lax.ppermute(shard, axis, [(i, (i + back) % n) for i in range(n)])  22.7 us
    pallas_call x15, Pallas kernels, call(): pl.pallas_call(kernel, out_shape=outs, in_specs=[pl.BlockSpec(memory_spac...  21.9 us
    ppermute x6, starting transfers between devices, turned(): return lax.ppermute(shard, axis, [(i, (i + back) % n) for i in range(n)])  20.5 us
    unnamed x30, local copies, waits for them, and re-layouts  8.74 us
  transfers between devices with their start and end apart: 15, of which 12 were waited for; matrix products, arithmetic and copies ran while one was open for 0% of the time, Pallas kernels for 5%

profile of v3, /device:TPU:1, one launch (start us, length us, event | category | flops | bytes accessed | tf_op | source)
XLA Modules:
  0.0 228.3 jit_solution(14019991741826532266)
XLA Ops:
  0.6 2.9 %shard_map.158 = (bf16[1280,128]{1,0:T(8,128)(2,1)}, f32[32,128]{1,0:T(8,128)}, f32[32,128]{1,0:T(8,128)}) custom-call(s32[1]{0:T(128)} %bitcast.7.place, bf16[128,4096]{1,0:T(8,128)(2,1)} %x.1, f32[1,4096]{1,0:T(1,128)} %bitcast.25, s32[4,128]{1,0:T(4,128)} %bitcast.26, f32[4,128]{1,0:T(4,128)} %bitcast.27), custom_call_target="tpu_custom_call" | custom-call | tf_op jit(solution)/shard_map/pallas_call | solution.py:57
  3.5 41.7 %all_to_all.30 = bf16[32,40,128]{2,1,0:T(8,128)(2,1)S(1)} all-to-all(bf16[32,40,128]{2,1,0:T(8,128)(2,1)} %bitcast.24), channel_id=1, replica_groups=mesh['ep_0'=16,'ep_1'=2,'tp_y'=4,'tp_x'=4] {'ep_0','ep_1'}, dimensions={0} | all-to-all | bytes 655360 | tf_op jit(solution)/shard_map/all_to_all | solution.py:184
  45.3 1.2 shard_map.159
  46.5 4.1 %all-to-all-start.2 = ((bf16[4,1280,128]{2,1,0:T(8,128)(2,1)}), bf16[4,1280,128]{2,1,0:T(8,128)(2,1)S(1)}, u32[]{:S(2)}, u32[]{:S(2)}) async-start(bf16[4,1280,128]{2,1,0:T(8,128)(2,1)} %shard_map.159), calls=%async_computation.2 | async-start | bytes 2621440 | tf_op jit(solution)/shard_map/all_to_all | solution.py:184
  51.8 3.2 %collective-permute-start.8 = (bf16[256,1024]{1,0:T(8,128)(2,1)S(1)}, bf16[256,1024]{1,0:T(8,128)(2,1)S(1)}, u32[]{:S(2)}, u32[]{:S(2)}) collective-permute-start(bf16[256,1024]{1,0:T(8,128)(2,1)S(1)} %get-tuple-element.32), channel_id=1, source_target_pairs={{0,4},{4,8},{8,12},{12,0},{1,5},{5,9},{9,13},{13,1},{2,6},{6,10},{... | collective-permute-start | bytes 1572872 | tf_op jit(solution)/shard_map/ppermute | solution.py:377
  55.1 4.5 %collective-permute-start.9 = (bf16[256,1024]{1,0:T(8,128)(2,1)S(1)}, bf16[256,1024]{1,0:T(8,128)(2,1)S(1)}, u32[]{:S(2)}, u32[]{:S(2)}) collective-permute-start(bf16[256,1024]{1,0:T(8,128)(2,1)S(1)} %get-tuple-element.33), channel_id=1, source_target_pairs={{0,8},{4,12},{8,0},{12,4},{1,9},{5,13},{9,1},{13,5},{2,10},{6,14},... | collective-permute-start | bytes 1572872 | tf_op jit(solution)/shard_map/ppermute | solution.py:377
  59.6 3.0 %collective-permute-start.10 = (bf16[256,1024]{1,0:T(8,128)(2,1)S(1)}, bf16[256,1024]{1,0:T(8,128)(2,1)S(1)}, u32[]{:S(2)}, u32[]{:S(2)}) collective-permute-start(bf16[256,1024]{1,0:T(8,128)(2,1)S(1)} %get-tuple-element.34), channel_id=1, source_target_pairs={{0,12},{4,0},{8,4},{12,8},{1,13},{5,1},{9,5},{13,9},{2,14},{6,2},{... | collective-permute-start | bytes 1572872 | tf_op jit(solution)/shard_map/ppermute | solution.py:377
  62.6 5.0 %collective-permute-done.8.w1 = bf16[256,1024]{1,0:T(8,128)(2,1)S(1)} collective-permute-done((bf16[256,1024]{1,0:T(8,128)(2,1)S(1)}, bf16[256,1024]{1,0:T(8,128)(2,1)S(1)}, u32[]{:S(2)}, u32[]{:S(2)}) %collective-permute-start.8) | collective-permute-done | bytes 524320 | tf_op jit(solution)/shard_map/ppermute | solution.py:377
  67.6 12.3 %collective-permute-done.9.w2 = bf16[256,1024]{1,0:T(8,128)(2,1)S(1)} collective-permute-done((bf16[256,1024]{1,0:T(8,128)(2,1)S(1)}, bf16[256,1024]{1,0:T(8,128)(2,1)S(1)}, u32[]{:S(2)}, u32[]{:S(2)}) %collective-permute-start.9) | collective-permute-done | bytes 524320 | tf_op jit(solution)/shard_map/ppermute | solution.py:377
  79.9 1.7 collective-permute-done.10.w3
  81.6 2.5 %shard_map.160 = bf16[4,160,512]{2,1,0:T(8,128)(2,1)S(1)} custom-call(s32[1]{0:T(128)} %bitcast.2.place, bf16[4,1280,128]{2,1,0:T(8,128)(2,1)S(1)} %all-to-all-done.2.gathered, bf16[256,1024]{1,0:T(8,128)(2,1)S(1)} %get-tuple-element.31.w0, bf16[256,1024]{1,0:T(8,128)(2,1)S(1)} %collective-permute-done.8.w1, ...), custom_call_target="tpu_custom_call" | custom-call | tf_op jit(solution)/shard_map/pallas_call | solution.py:57
  84.1 14.2 %all_to_all.31.parts = bf16[4,160,512]{2,1,0:T(8,128)(2,1)S(1)} all-to-all(bf16[4,160,512]{2,1,0:T(8,128)(2,1)S(1)} %shard_map.160), channel_id=1, replica_groups=mesh['ep_0'=16,'ep_1'=2,'tp_y'=4,'tp_x'=4] {'tp_y'}, dimensions={0} | all-to-all | bytes 1310720 | tf_op jit(solution)/shard_map/all_to_all | solution.py:184
  98.3 1.5 shard_map.161
  99.8 5.1 %all-to-all-start.4 = ((bf16[16,160,256]{2,1,0:T(8,128)(2,1)}), bf16[16,160,256]{2,1,0:T(8,128)(2,1)S(1)}, u32[]{:S(2)}, u32[]{:S(2)}) async-start(bf16[16,160,256]{2,1,0:T(8,128)(2,1)} %shard_map.161), calls=%async_computation.4 | async-start | bytes 2621440 | tf_op jit(solution)/shard_map/all_to_all | solution.py:184
  109.1 6.6 %shard_map.149 = (f32[2,128,128]{2,1,0:T(8,128)S(1)}, bf16[2,64,128]{2,1,0:T(8,128)(2,1)}, f32[2,256,128]{2,1,0:T(8,128)S(1)}) custom-call(bf16[256,128]{1,0:T(8,128)(2,1)S(1)} %copy-done.7, bf16[256,128]{1,0:T(8,128)(2,1)S(1)} %copy-done.8, bf16[256,128]{1,0:T(8,128)(2,1)S(1)} %copy-done.9, bf16[256,128]{1,0:T(8,128)(2,1)S(1)} %copy-done.10, ...), custom_call_target="tpu_custom_call" | custom-call | tf_op jit(solution)/shard_map/pallas_call | solution.py:57
  116.4 3.4 %collective-permute-start = (bf16[2,64,128]{2,1,0:T(8,128)(2,1)}, bf16[2,64,128]{2,1,0:T(8,128)(2,1)}, u32[]{:S(2)}, u32[]{:S(2)}) collective-permute-start(bf16[2,64,128]{2,1,0:T(8,128)(2,1)} %get-tuple-element.20), channel_id=1, source_target_pairs={{0,16},{16,32},{32,48},{48,64},{64,80},{80,96},{96,112},{112,128},... | collective-permute-start | bytes 98312 | tf_op jit(solution)/shard_map/ppermute | solution.py:445
  119.8 1.4 collective-permute-done.came
  122.1 3.3 %collective-permute-start.1 = (bf16[2,64,128]{2,1,0:T(8,128)(2,1)S(1)}, bf16[2,64,128]{2,1,0:T(8,128)(2,1)S(1)}, u32[]{:S(2)}, u32[]{:S(2)}) collective-permute-start(bf16[2,64,128]{2,1,0:T(8,128)(2,1)S(1)} %get-tuple-element.22), channel_id=1, source_target_pairs={{0,32},{16,48},{32,64},{48,80},{64,96},{80,112},{96,128},{112,144}... | collective-permute-start | bytes 98312 | tf_op jit(solution)/shard_map/ppermute | solution.py:445
  126.6 3.4 %collective-permute-start.2 = (bf16[2,64,128]{2,1,0:T(8,128)(2,1)S(1)}, bf16[2,64,128]{2,1,0:T(8,128)(2,1)S(1)}, u32[]{:S(2)}, u32[]{:S(2)}) collective-permute-start(bf16[2,64,128]{2,1,0:T(8,128)(2,1)S(1)} %get-tuple-element.24), channel_id=1, source_target_pairs={{0,64},{16,80},{32,96},{48,112},{64,128},{80,144},{96,160},{112,17... | collective-permute-start | bytes 98312 | tf_op jit(solution)/shard_map/ppermute | solution.py:445
  131.2 7.2 %collective-permute-start.3 = (bf16[2,64,128]{2,1,0:T(8,128)(2,1)S(1)}, bf16[2,64,128]{2,1,0:T(8,128)(2,1)S(1)}, u32[]{:S(2)}, u32[]{:S(2)}) collective-permute-start(bf16[2,64,128]{2,1,0:T(8,128)(2,1)S(1)} %get-tuple-element.26), channel_id=1, source_target_pairs={{0,128},{16,144},{32,160},{48,176},{64,192},{80,208},{96,224},{112... | collective-permute-start | bytes 98312 | tf_op jit(solution)/shard_map/ppermute | solution.py:445
  139.6 8.1 %collective-permute-start.4 = (bf16[64,128]{1,0:T(8,128)(2,1)S(1)}, bf16[64,128]{1,0:T(8,128)(2,1)S(1)}, u32[]{:S(2)}, u32[]{:S(2)}) collective-permute-start(bf16[64,128]{1,0:T(8,128)(2,1)S(1)} %get-tuple-element.28), channel_id=1, source_target_pairs={{0,256},{16,272},{32,288},{48,304},{64,320},{80,336},{96,352},{112... | collective-permute-start | bytes 49160 | tf_op jit(solution)/shard_map/ppermute | solution.py:445
  150.2 4.8 %collective-permute-start.7 = (bf16[256,128]{1,0:T(8,128)(2,1)S(1)}, bf16[256,128]{1,0:T(8,128)(2,1)S(1)}, u32[]{:S(2)}, u32[]{:S(2)}) collective-permute-start(bf16[256,128]{1,0:T(8,128)(2,1)S(1)} %shard_map.154.m0), channel_id=1, source_target_pairs={{0,12},{4,0},{8,4},{12,8},{1,13},{5,1},{9,5},{13,9},{2,14},{6,2},{... | collective-permute-start | bytes 196616 | tf_op jit(solution)/shard_map/ppermute | solution.py:377
  155.0 2.5 %collective-permute-start.6 = (bf16[256,128]{1,0:T(8,128)(2,1)S(1)}, bf16[256,128]{1,0:T(8,128)(2,1)S(1)}, u32[]{:S(2)}, u32[]{:S(2)}) collective-permute-start(bf16[256,128]{1,0:T(8,128)(2,1)S(1)} %shard_map.154.m0), channel_id=1, source_target_pairs={{0,8},{4,12},{8,0},{12,4},{1,9},{5,13},{9,1},{13,5},{2,10},{6,14},... | collective-permute-start | bytes 196616 | tf_op jit(solution)/shard_map/ppermute | solution.py:377
  157.5 2.5 %collective-permute-start.5 = (bf16[256,128]{1,0:T(8,128)(2,1)S(1)}, bf16[256,128]{1,0:T(8,128)(2,1)S(1)}, u32[]{:S(2)}, u32[]{:S(2)}) collective-permute-start(bf16[256,128]{1,0:T(8,128)(2,1)S(1)} %shard_map.154.m0), channel_id=1, source_target_pairs={{0,4},{4,8},{8,12},{12,0},{1,5},{5,9},{9,13},{13,1},{2,6},{6,10},{... | collective-permute-start | bytes 196616 | tf_op jit(solution)/shard_map/ppermute | solution.py:377
  160.0 1.5 collective-permute-done.6.m2
  161.5 2.2 collective-permute-done.5.m1
  164.9 5.0 %all-to-all-start = ((bf16[16,16,1024]{2,1,0:T(8,128)(2,1)}), bf16[16,16,1024]{2,1,0:T(8,128)(2,1)S(1)}, u32[]{:S(2)}, u32[]{:S(2)}) async-start(bf16[16,16,1024]{2,1,0:T(8,128)(2,1)} %copy-done), calls=%async_computation | async-start | bytes 1048576 | tf_op jit(solution)/shard_map/all_to_all | solution.py:184
  171.0 2.1 shard_map.162
  173.1 5.8 %all-to-all-done.tiles = bf16[16,16,1024]{2,1,0:T(8,128)(2,1)S(1)} async-done(((bf16[16,16,1024]{2,1,0:T(8,128)(2,1)}), bf16[16,16,1024]{2,1,0:T(8,128)(2,1)S(1)}, u32[]{:S(2)}, u32[]{:S(2)}) %all-to-all-start) | async-done | bytes 524320 | tf_op jit(solution)/shard_map/all_to_all | solution.py:184
  178.9 22.9 %all-to-all-start.5 = ((bf16[32,40,128]{2,1,0:T(8,128)(2,1)}), bf16[32,40,128]{2,1,0:T(8,128)(2,1)S(1)}, u32[]{:S(2)}, u32[]{:S(2)}) async-start(bf16[32,40,128]{2,1,0:T(8,128)(2,1)} %bitcast.14), calls=%async_computation.5 | async-start | bytes 655360 | tf_op jit(solution)/shard_map/all_to_all | solution.py:184
  202.5 24.3 %all-to-all-done.5 = bf16[32,40,128]{2,1,0:T(8,128)(2,1)S(1)} async-done(((bf16[32,40,128]{2,1,0:T(8,128)(2,1)}), bf16[32,40,128]{2,1,0:T(8,128)(2,1)S(1)}, u32[]{:S(2)}, u32[]{:S(2)}) %all-to-all-start.5) | async-done | bytes 327712 | tf_op jit(solution)/shard_map/all_to_all | solution.py:184
  226.7 1.5 shard_map.163
  (45 shorter events, 16.0 us)
Async XLA Ops:
  46.5 4.2 %copy-start.1 = (bf16[128,4096]{1,0:T(8,128)(2,1)S(1)}, bf16[128,4096]{1,0:T(8,128)(2,1)}, u32[]{:S(2)}) copy-start(bf16[128,4096]{1,0:T(8,128)(2,1)} %out_weight.1) | copy-start | bytes 3145732
  46.5 4.2 %copy-start.2 = (bf16[1,4096,64]{1,2,0:T(8,128)(2,1)S(1)}, bf16[1,4096,64]{1,2,0:T(8,128)(2,1)}, u32[]{:S(2)}) copy-start(bf16[1,4096,64]{1,2,0:T(8,128)(2,1)} %param.25) | copy-start | bytes 1572868
  46.5 35.1 %all-to-all-start.2 = ((bf16[4,1280,128]{2,1,0:T(8,128)(2,1)}), bf16[4,1280,128]{2,1,0:T(8,128)(2,1)S(1)}, u32[]{:S(2)}, u32[]{:S(2)}) async-start(bf16[4,1280,128]{2,1,0:T(8,128)(2,1)} %shard_map.159), calls=%async_computation.2 | async-start | bytes 2621440 | tf_op jit(solution)/shard_map/all_to_all | solution.py:184
  50.7 1.0 copy-start.3
  51.8 15.7 %collective-permute-start.8 = (bf16[256,1024]{1,0:T(8,128)(2,1)S(1)}, bf16[256,1024]{1,0:T(8,128)(2,1)S(1)}, u32[]{:S(2)}, u32[]{:S(2)}) collective-permute-start(bf16[256,1024]{1,0:T(8,128)(2,1)S(1)} %get-tuple-element.32), channel_id=1, source_target_pairs={{0,4},{4,8},{8,12},{12,0},{1,5},{5,9},{9,13},{13,1},{2,6},{6,10},{... | collective-permute-start | bytes 1572872 | tf_op jit(solution)/shard_map/ppermute | solution.py:377
  55.1 24.9 %collective-permute-start.9 = (bf16[256,1024]{1,0:T(8,128)(2,1)S(1)}, bf16[256,1024]{1,0:T(8,128)(2,1)S(1)}, u32[]{:S(2)}, u32[]{:S(2)}) collective-permute-start(bf16[256,1024]{1,0:T(8,128)(2,1)S(1)} %get-tuple-element.33), channel_id=1, source_target_pairs={{0,8},{4,12},{8,0},{12,4},{1,9},{5,13},{9,1},{13,5},{2,10},{6,14},... | collective-permute-start | bytes 1572872 | tf_op jit(solution)/shard_map/ppermute | solution.py:377
  59.6 22.0 %collective-permute-start.10 = (bf16[256,1024]{1,0:T(8,128)(2,1)S(1)}, bf16[256,1024]{1,0:T(8,128)(2,1)S(1)}, u32[]{:S(2)}, u32[]{:S(2)}) collective-permute-start(bf16[256,1024]{1,0:T(8,128)(2,1)S(1)} %get-tuple-element.34), channel_id=1, source_target_pairs={{0,12},{4,0},{8,4},{12,8},{1,13},{5,1},{9,5},{13,9},{2,14},{6,2},{... | collective-permute-start | bytes 1572872 | tf_op jit(solution)/shard_map/ppermute | solution.py:377
  99.8 48.8 %copy-start.14 = (f32[128]{0:T(128)S(1)}, f32[128]{0:T(128)}, u32[]{:S(2)}) copy-start(f32[128]{0:T(128)} %param.19) | copy-start | bytes 1540
  99.8 65.1 %all-to-all-start.4 = ((bf16[16,160,256]{2,1,0:T(8,128)(2,1)}), bf16[16,160,256]{2,1,0:T(8,128)(2,1)S(1)}, u32[]{:S(2)}, u32[]{:S(2)}) async-start(bf16[16,160,256]{2,1,0:T(8,128)(2,1)} %shard_map.161), calls=%async_computation.4 | async-start | bytes 2621440 | tf_op jit(solution)/shard_map/all_to_all | solution.py:184
  104.9 0.8 copy-start.7
  105.7 0.8 copy-start.8
  106.6 0.8 copy-start.9
  107.4 0.8 copy-start.10
  108.2 0.8 copy-start.11
  115.7 0.7 copy-start.5
  116.4 4.7 %collective-permute-start = (bf16[2,64,128]{2,1,0:T(8,128)(2,1)}, bf16[2,64,128]{2,1,0:T(8,128)(2,1)}, u32[]{:S(2)}, u32[]{:S(2)}) collective-permute-start(bf16[2,64,128]{2,1,0:T(8,128)(2,1)} %get-tuple-element.20), channel_id=1, source_target_pairs={{0,16},{16,32},{32,48},{48,64},{64,80},{80,96},{96,112},{112,128},... | collective-permute-start | bytes 98312 | tf_op jit(solution)/shard_map/ppermute | solution.py:445
  122.1 4.4 %collective-permute-start.1 = (bf16[2,64,128]{2,1,0:T(8,128)(2,1)S(1)}, bf16[2,64,128]{2,1,0:T(8,128)(2,1)S(1)}, u32[]{:S(2)}, u32[]{:S(2)}) collective-permute-start(bf16[2,64,128]{2,1,0:T(8,128)(2,1)S(1)} %get-tuple-element.22), channel_id=1, source_target_pairs={{0,32},{16,48},{32,64},{48,80},{64,96},{80,112},{96,128},{112,144}... | collective-permute-start | bytes 98312 | tf_op jit(solution)/shard_map/ppermute | solution.py:445
  126.6 4.4 %collective-permute-start.2 = (bf16[2,64,128]{2,1,0:T(8,128)(2,1)S(1)}, bf16[2,64,128]{2,1,0:T(8,128)(2,1)S(1)}, u32[]{:S(2)}, u32[]{:S(2)}) collective-permute-start(bf16[2,64,128]{2,1,0:T(8,128)(2,1)S(1)} %get-tuple-element.24), channel_id=1, source_target_pairs={{0,64},{16,80},{32,96},{48,112},{64,128},{80,144},{96,160},{112,17... | collective-permute-start | bytes 98312 | tf_op jit(solution)/shard_map/ppermute | solution.py:445
  131.2 8.2 %collective-permute-start.3 = (bf16[2,64,128]{2,1,0:T(8,128)(2,1)S(1)}, bf16[2,64,128]{2,1,0:T(8,128)(2,1)S(1)}, u32[]{:S(2)}, u32[]{:S(2)}) collective-permute-start(bf16[2,64,128]{2,1,0:T(8,128)(2,1)S(1)} %get-tuple-element.26), channel_id=1, source_target_pairs={{0,128},{16,144},{32,160},{48,176},{64,192},{80,208},{96,224},{112... | collective-permute-start | bytes 98312 | tf_op jit(solution)/shard_map/ppermute | solution.py:445
  139.6 9.0 %collective-permute-start.4 = (bf16[64,128]{1,0:T(8,128)(2,1)S(1)}, bf16[64,128]{1,0:T(8,128)(2,1)S(1)}, u32[]{:S(2)}, u32[]{:S(2)}) collective-permute-start(bf16[64,128]{1,0:T(8,128)(2,1)S(1)} %get-tuple-element.28), channel_id=1, source_target_pairs={{0,256},{16,272},{32,288},{48,304},{64,320},{80,336},{96,352},{112... | collective-permute-start | bytes 49160 | tf_op jit(solution)/shard_map/ppermute | solution.py:445
  148.6 1.0 copy-start.6
  150.2 9.8 %collective-permute-start.7 = (bf16[256,128]{1,0:T(8,128)(2,1)S(1)}, bf16[256,128]{1,0:T(8,128)(2,1)S(1)}, u32[]{:S(2)}, u32[]{:S(2)}) collective-permute-start(bf16[256,128]{1,0:T(8,128)(2,1)S(1)} %shard_map.154.m0), channel_id=1, source_target_pairs={{0,12},{4,0},{8,4},{12,8},{1,13},{5,1},{9,5},{13,9},{2,14},{6,2},{... | collective-permute-start | bytes 196616 | tf_op jit(solution)/shard_map/ppermute | solution.py:377
  155.0 6.5 %collective-permute-start.6 = (bf16[256,128]{1,0:T(8,128)(2,1)S(1)}, bf16[256,128]{1,0:T(8,128)(2,1)S(1)}, u32[]{:S(2)}, u32[]{:S(2)}) collective-permute-start(bf16[256,128]{1,0:T(8,128)(2,1)S(1)} %shard_map.154.m0), channel_id=1, source_target_pairs={{0,8},{4,12},{8,0},{12,4},{1,9},{5,13},{9,1},{13,5},{2,10},{6,14},... | collective-permute-start | bytes 196616 | tf_op jit(solution)/shard_map/ppermute | solution.py:377
  157.5 6.2 %collective-permute-start.5 = (bf16[256,128]{1,0:T(8,128)(2,1)S(1)}, bf16[256,128]{1,0:T(8,128)(2,1)S(1)}, u32[]{:S(2)}, u32[]{:S(2)}) collective-permute-start(bf16[256,128]{1,0:T(8,128)(2,1)S(1)} %shard_map.154.m0), channel_id=1, source_target_pairs={{0,4},{4,8},{8,12},{12,0},{1,5},{5,9},{9,13},{13,1},{2,6},{6,10},{... | collective-permute-start | bytes 196616 | tf_op jit(solution)/shard_map/ppermute | solution.py:377
  164.1 0.8 copy-start
  164.9 14.0 %all-to-all-start = ((bf16[16,16,1024]{2,1,0:T(8,128)(2,1)}), bf16[16,16,1024]{2,1,0:T(8,128)(2,1)S(1)}, u32[]{:S(2)}, u32[]{:S(2)}) async-start(bf16[16,16,1024]{2,1,0:T(8,128)(2,1)} %copy-done), calls=%async_computation | async-start | bytes 1048576 | tf_op jit(solution)/shard_map/all_to_all | solution.py:184
  169.9 1.0 copy-start.4
  171.0 55.8 %copy-start.12 = (f32[32,128]{1,0:T(8,128)S(1)}, f32[32,128]{1,0:T(8,128)}, u32[]{:S(2)}) copy-start(f32[32,128]{1,0:T(8,128)} %get-tuple-element.36.rank) | copy-start | bytes 49156
  171.0 55.8 %copy-start.13 = (f32[32,128]{1,0:T(8,128)S(1)}, f32[32,128]{1,0:T(8,128)}, u32[]{:S(2)}) copy-start(f32[32,128]{1,0:T(8,128)} %get-tuple-element.37.share) | copy-start | bytes 49156
  178.9 47.8 %all-to-all-start.5 = ((bf16[32,40,128]{2,1,0:T(8,128)(2,1)}), bf16[32,40,128]{2,1,0:T(8,128)(2,1)S(1)}, u32[]{:S(2)}, u32[]{:S(2)}) async-start(bf16[32,40,128]{2,1,0:T(8,128)(2,1)} %bitcast.14), calls=%async_computation.5 | async-start | bytes 655360 | tf_op jit(solution)/shard_map/all_to_all | solution.py:184

commit v4 on v3

--- a/solution.py
+++ b/solution.py
@@ -124,19 +124,27 @@
     )
 
 
-def gate_up_kernel(place, gathered, w0, w1, w2, w3, out, weights):
-    picks = (selector(0), selector(1))
+def gate_up_kernel(place, gathered, w0, w1, w2, w3, out, weights, rows):
+    pick = jnp.concatenate([selector(0), selector(1)], axis=0)
     side = weights.shape[0]
     for back, w in enumerate((w0, w1, w2, w3)):
         weights[(place[0] + side - back) % side] = w[: weights.shape[1], :]
-    joined = jnp.concatenate([weights[k] for k in range(side)], axis=0)
+    each = GROUP * CAP
     for g in range(EXPERTS // GROUP):
-        pieces = []
         for k in range(gathered.shape[0]):
             seen = gathered[k, g * GROUP * SLOT : (g + 1) * GROUP * SLOT, :]
-            for pick in picks:
-                pieces.append(mm(pick, seen).astype(jnp.bfloat16))
-        out[g] = nt(jnp.concatenate(pieces, axis=1), joined).astype(jnp.bfloat16)
+            found = mm(pick, seen).astype(jnp.bfloat16)
+            for half in range(2):
+                at = (2 * k + half) * 128
+                rows[g * each : (g + 1) * each, at : at + 128] = found[
+                    half * each : (half + 1) * each
+                ]
+    whole = rows[...]
+    for k in range(side // 2):
+        pair = jnp.concatenate([weights[2 * k], weights[2 * k + 1]], axis=0)
+        made = nt(whole, pair).astype(jnp.bfloat16)
+        for g in range(EXPERTS // GROUP):
+            out[g, :, k * 256 : (k + 1) * 256] = made[g * each : (g + 1) * each]
 
 
 def hidden_kernel(parts, out):
@@ -352,24 +360,31 @@
         p[2 * hidden :, :] = out_weight[:, at]
 
 
-def product_kernel(m0, m1, m2, m3, w0, w1, w2, w3, out):
+def product_kernel(place, m0, m1, m2, m3, w0, w1, w2, w3, p0, p1, p2, p3, made):
     rows = jnp.concatenate([m[...] for m in (m0, m1, m2, m3)], 1)
     count = rows.shape[1] // 4
     weights = jnp.concatenate([w[w.shape[0] - count :, :] for w in (w0, w1, w2, w3)], 0)
-    made = mm(rows, weights).astype(jnp.bfloat16)
-    peers, each, _ = out.shape
+    whole = mm(rows, weights).astype(jnp.bfloat16)
+    peers, each, _ = made.shape
     for p in range(peers):
-        out[p] = made[p * each : (p + 1) * each]
+        made[p] = whole[p * each : (p + 1) * each]
+    side = p0.shape[0]
+    for ahead, part in enumerate((p0, p1, p2, p3)):
+        for y in range(side):
+            part[y] = made[side * y + (place[0] + ahead) % side]
+
+
+def adding_kernel(p0, p1, p2, p3, out):
+    for y in range(out.shape[0]):
+        total = p0[y].astype(jnp.float32) + p1[y].astype(jnp.float32)
+        total += p2[y].astype(jnp.float32) + p3[y].astype(jnp.float32)
+        out[y] = total.astype(jnp.bfloat16)
 
 
 def finish_kernel(tiles, out):
-    side = 4
-    width = tiles.shape[2]
+    side, _, width = tiles.shape
     for y in range(side):
-        total = tiles[side * y].astype(jnp.float32)
-        for x in range(1, side):
-            total += tiles[side * y + x].astype(jnp.float32)
-        out[:, y * width : (y + 1) * width] = total.astype(jnp.bfloat16)
+        out[:, y * width : (y + 1) * width] = tiles[y]
 
 
 def turned(shard, axis, back):
@@ -398,6 +413,7 @@
     tp = lax.axis_size(TP)
     side = lax.axis_size("tp_y")
     width = features // tp
+    column_place = lax.axis_index("tp_x").astype(jnp.int32).reshape(1)
     row_place = lax.axis_index("tp_y").astype(jnp.int32).reshape(1)
     total = EXPERTS * SLOT
     share_rows = EXPERTS * CAP // side
@@ -464,9 +480,18 @@
         scalars=1,
     )
     mixes = [mixed] + [turned(mixed, "tp_y", k) for k in range(1, side)]
-    product = call(
-        product_kernel, shape((tp, tokens // tp, features // side)), *mixes, *moved
-    )
+    quarter = (side, tokens // tp, features // side)
+    products = call(
+        product_kernel,
+        [shape(quarter)] * side,
+        column_place,
+        *mixes,
+        *moved,
+        scalars=1,
+        scratch=[pltpu.VMEM((tp, *quarter[1:]), jnp.bfloat16)],
+    )
+    shares = [products[0]] + [turned(products[k], "tp_x", k) for k in range(1, side)]
+    added = call(adding_kernel, shape(quarter), *shares)
 
     copies = call(
         copies_kernel, shape((side, total, 128)), arrived.reshape(total, 128)
@@ -480,18 +505,19 @@
         gathered,
         *moved,
         scalars=1,
-        scratch=[pltpu.VMEM((side, 128, features // side), jnp.bfloat16)],
+        scratch=[
+            pltpu.VMEM((side, 128, features // side), jnp.bfloat16),
+            pltpu.VMEM((EXPERTS * CAP, features // side), jnp.bfloat16),
+        ],
     )
     parts = exchanged(partial, "tp_y")
     hidden = call(hidden_kernel, shape((tp, share_rows, wide // 2)), parts)
     everyone = exchanged(hidden, TP)
     result = call(down_kernel, shape((total, 128)), everyone, down_weight[0])
     returned = exchanged(result.reshape(EXPERTS, SLOT, 128), EP)
-    tiles = exchanged(product, TP)
+    tiles = exchanged(added, "tp_y")
     moe_out = call(combine_kernel, shape((rows, width)), returned.reshape(total, 128), rank, share)
-    mixer_out = call(
-        finish_kernel, shape((tokens // tp, side * product.shape[2])), tiles
-    )
+    mixer_out = call(finish_kernel, shape((tokens // tp, features)), tiles)
     return (mixer_out, moe_out)
 
 

time: 230 us -> 238 us (1.035)
  starting transfers between devices: 82.9 us -> 93.1 us
    ppermute x6 -> x9, starting transfers between devices: 20.5 us -> 30.9 us  [turned(): return lax.ppermute(shard, axis, [(i, (i + back) % n) for i in range(n)])]
    all_to_all x4, waiting for transfers between devices: 30.1 us -> 25.9 us  [exchanged(): return lax.all_to_all(tiles, axis, split_axis=0, concat_axis=0, tiled=True)]
    ppermute x6 -> x9, waiting for transfers between devices: 22.7 us -> 25.3 us  [turned(): return lax.ppermute(shard, axis, [(i, (i + back) % n) for i in range(n)])]
    unnamed x30 -> x28, local copies, waits for them, and re-layouts: 8.74 us -> 7.95 us
    pallas_call x15 -> x16, Pallas kernels: 21.9 us -> 22.1 us  [call(): pl.pallas_call(kernel, out_shape=outs, in_specs=[pl.BlockSpec(memory_spac...]
  transfers between devices with their start and end apart: 15 -> 18, of which waited for: 12 -> 13; matrix products, arithmetic and copies ran while one was open for 0% -> 0% of each run, Pallas kernels for 5% -> 5%
where the time goes in v4:
time: 238 us; the launch traced here: 236 us
  starting transfers between devices  93.1 us (39%)
  waiting for transfers between devices  56.5 us (24%)
  blocking collectives  55.9 us (23%)
  Pallas kernels  22.1 us (9%)
  local copies, waits for them, and re-layouts  7.95 us (3%)
    all_to_all x2, blocking collectives, exchanged(): return lax.all_to_all(tiles, axis, split_axis=0, concat_axis=0, tiled=True)  55.9 us
    all_to_all x4, starting transfers between devices, exchanged(): return lax.all_to_all(tiles, axis, split_axis=0, concat_axis=0, tiled=True)  36.8 us
    ppermute x9, starting transfers between devices, turned(): return lax.ppermute(shard, axis, [(i, (i + back) % n) for i in range(n)])  30.9 us
    all_to_all x4, waiting for transfers between devices, exchanged(): return lax.all_to_all(tiles, axis, split_axis=0, concat_axis=0, tiled=True)  25.9 us
    ppermute x5, starting transfers between devices, local(): lax.ppermute(send, EP, [(i, i + shift) for i in range(peers - shift)])  25.4 us
    ppermute x9, waiting for transfers between devices, turned(): return lax.ppermute(shard, axis, [(i, (i + back) % n) for i in range(n)])  25.3 us
    pallas_call x16, Pallas kernels, call(): pl.pallas_call(kernel, out_shape=outs, in_specs=[pl.BlockSpec(memory_spac...  22.1 us
    unnamed x28, local copies, waits for them, and re-layouts  7.95 us
  transfers between devices with their start and end apart: 18, of which 13 were waited for; matrix products, arithmetic and copies ran while one was open for 0% of the time, Pallas kernels for 5%

profile of v4, /device:TPU:1, one launch (start us, length us, event | category | flops | bytes accessed | tf_op | source)
XLA Modules:
  0.0 236.4 jit_solution(17135752495681130968)
XLA Ops:
  0.6 2.9 %shard_map.159 = (bf16[1280,128]{1,0:T(8,128)(2,1)}, f32[32,128]{1,0:T(8,128)}, f32[32,128]{1,0:T(8,128)}) custom-call(s32[1]{0:T(128)} %bitcast.8.place, bf16[128,4096]{1,0:T(8,128)(2,1)} %x.1, f32[1,4096]{1,0:T(1,128)} %bitcast.26, s32[4,128]{1,0:T(4,128)} %bitcast.27, f32[4,128]{1,0:T(4,128)} %bitcast.28), custom_call_target="tpu_custom_call" | custom-call | tf_op jit(solution)/shard_map/pallas_call | solution.py:57
  3.5 41.7 %all_to_all.30 = bf16[32,40,128]{2,1,0:T(8,128)(2,1)S(1)} all-to-all(bf16[32,40,128]{2,1,0:T(8,128)(2,1)} %bitcast.25), channel_id=1, replica_groups=mesh['ep_0'=16,'ep_1'=2,'tp_y'=4,'tp_x'=4] {'ep_0','ep_1'}, dimensions={0} | all-to-all | bytes 655360 | tf_op jit(solution)/shard_map/all_to_all | solution.py:192
  46.5 4.1 %all-to-all-start.2 = ((bf16[4,1280,128]{2,1,0:T(8,128)(2,1)}), bf16[4,1280,128]{2,1,0:T(8,128)(2,1)S(1)}, u32[]{:S(2)}, u32[]{:S(2)}) async-start(bf16[4,1280,128]{2,1,0:T(8,128)(2,1)} %shard_map.160), calls=%async_computation.2 | async-start | bytes 2621440 | tf_op jit(solution)/shard_map/all_to_all | solution.py:192
  51.9 3.2 %collective-permute-start.8 = (bf16[256,1024]{1,0:T(8,128)(2,1)S(1)}, bf16[256,1024]{1,0:T(8,128)(2,1)S(1)}, u32[]{:S(2)}, u32[]{:S(2)}) collective-permute-start(bf16[256,1024]{1,0:T(8,128)(2,1)S(1)} %get-tuple-element.36), channel_id=1, source_target_pairs={{0,4},{4,8},{8,12},{12,0},{1,5},{5,9},{9,13},{13,1},{2,6},{6,10},{... | collective-permute-start | bytes 1572872 | tf_op jit(solution)/shard_map/ppermute | solution.py:392
  55.1 4.5 %collective-permute-start.9 = (bf16[256,1024]{1,0:T(8,128)(2,1)S(1)}, bf16[256,1024]{1,0:T(8,128)(2,1)S(1)}, u32[]{:S(2)}, u32[]{:S(2)}) collective-permute-start(bf16[256,1024]{1,0:T(8,128)(2,1)S(1)} %get-tuple-element.37), channel_id=1, source_target_pairs={{0,8},{4,12},{8,0},{12,4},{1,9},{5,13},{9,1},{13,5},{2,10},{6,14},... | collective-permute-start | bytes 1572872 | tf_op jit(solution)/shard_map/ppermute | solution.py:392
  59.6 3.0 %collective-permute-start.10 = (bf16[256,1024]{1,0:T(8,128)(2,1)S(1)}, bf16[256,1024]{1,0:T(8,128)(2,1)S(1)}, u32[]{:S(2)}, u32[]{:S(2)}) collective-permute-start(bf16[256,1024]{1,0:T(8,128)(2,1)S(1)} %get-tuple-element.38), channel_id=1, source_target_pairs={{0,12},{4,0},{8,4},{12,8},{1,13},{5,1},{9,5},{13,9},{2,14},{6,2},{... | collective-permute-start | bytes 1572872 | tf_op jit(solution)/shard_map/ppermute | solution.py:392
  62.6 5.0 %collective-permute-done.8.w1 = bf16[256,1024]{1,0:T(8,128)(2,1)S(1)} collective-permute-done((bf16[256,1024]{1,0:T(8,128)(2,1)S(1)}, bf16[256,1024]{1,0:T(8,128)(2,1)S(1)}, u32[]{:S(2)}, u32[]{:S(2)}) %collective-permute-start.8) | collective-permute-done | bytes 524320 | tf_op jit(solution)/shard_map/ppermute | solution.py:392
  67.6 12.3 %collective-permute-done.9.w2 = bf16[256,1024]{1,0:T(8,128)(2,1)S(1)} collective-permute-done((bf16[256,1024]{1,0:T(8,128)(2,1)S(1)}, bf16[256,1024]{1,0:T(8,128)(2,1)S(1)}, u32[]{:S(2)}, u32[]{:S(2)}) %collective-permute-start.9) | collective-permute-done | bytes 524320 | tf_op jit(solution)/shard_map/ppermute | solution.py:392
  79.9 1.7 collective-permute-done.10.w3
  81.6 1.9 shard_map.161
  83.6 14.2 %all_to_all.31.parts = bf16[4,160,512]{2,1,0:T(8,128)(2,1)S(1)} all-to-all(bf16[4,160,512]{2,1,0:T(8,128)(2,1)S(1)} %shard_map.161), channel_id=1, replica_groups=mesh['ep_0'=16,'ep_1'=2,'tp_y'=4,'tp_x'=4] {'tp_y'}, dimensions={0} | all-to-all | bytes 1310720 | tf_op jit(solution)/shard_map/all_to_all | solution.py:192
  99.3 5.1 %all-to-all-start.4 = ((bf16[16,160,256]{2,1,0:T(8,128)(2,1)}), bf16[16,160,256]{2,1,0:T(8,128)(2,1)S(1)}, u32[]{:S(2)}, u32[]{:S(2)}) async-start(bf16[16,160,256]{2,1,0:T(8,128)(2,1)} %shard_map.162), calls=%async_computation.4 | async-start | bytes 2621440 | tf_op jit(solution)/shard_map/all_to_all | solution.py:192
  108.6 6.6 %shard_map.149 = (f32[2,128,128]{2,1,0:T(8,128)S(1)}, bf16[2,64,128]{2,1,0:T(8,128)(2,1)}, f32[2,256,128]{2,1,0:T(8,128)S(1)}) custom-call(bf16[256,128]{1,0:T(8,128)(2,1)S(1)} %copy-done.6, bf16[256,128]{1,0:T(8,128)(2,1)S(1)} %copy-done.7, bf16[256,128]{1,0:T(8,128)(2,1)S(1)} %copy-done.8, bf16[256,128]{1,0:T(8,128)(2,1)S(1)} %copy-done.9, ...), custom_call_target="tpu_custom_call" | custom-call | tf_op jit(solution)/shard_map/pallas_call | solution.py:57
  115.9 3.3 %collective-permute-start = (bf16[2,64,128]{2,1,0:T(8,128)(2,1)}, bf16[2,64,128]{2,1,0:T(8,128)(2,1)}, u32[]{:S(2)}, u32[]{:S(2)}) collective-permute-start(bf16[2,64,128]{2,1,0:T(8,128)(2,1)} %get-tuple-element.24), channel_id=1, source_target_pairs={{0,16},{16,32},{32,48},{48,64},{64,80},{80,96},{96,112},{112,128},... | collective-permute-start | bytes 98312 | tf_op jit(solution)/shard_map/ppermute | solution.py:461
  121.6 3.3 %collective-permute-start.1 = (bf16[2,64,128]{2,1,0:T(8,128)(2,1)S(1)}, bf16[2,64,128]{2,1,0:T(8,128)(2,1)S(1)}, u32[]{:S(2)}, u32[]{:S(2)}) collective-permute-start(bf16[2,64,128]{2,1,0:T(8,128)(2,1)S(1)} %get-tuple-element.26), channel_id=1, source_target_pairs={{0,32},{16,48},{32,64},{48,80},{64,96},{80,112},{96,128},{112,144}... | collective-permute-start | bytes 98312 | tf_op jit(solution)/shard_map/ppermute | solution.py:461
  126.1 3.4 %collective-permute-start.2 = (bf16[2,64,128]{2,1,0:T(8,128)(2,1)S(1)}, bf16[2,64,128]{2,1,0:T(8,128)(2,1)S(1)}, u32[]{:S(2)}, u32[]{:S(2)}) collective-permute-start(bf16[2,64,128]{2,1,0:T(8,128)(2,1)S(1)} %get-tuple-element.28), channel_id=1, source_target_pairs={{0,64},{16,80},{32,96},{48,112},{64,128},{80,144},{96,160},{112,17... | collective-permute-start | bytes 98312 | tf_op jit(solution)/shard_map/ppermute | solution.py:461
  130.7 7.2 %collective-permute-start.3 = (bf16[2,64,128]{2,1,0:T(8,128)(2,1)S(1)}, bf16[2,64,128]{2,1,0:T(8,128)(2,1)S(1)}, u32[]{:S(2)}, u32[]{:S(2)}) collective-permute-start(bf16[2,64,128]{2,1,0:T(8,128)(2,1)S(1)} %get-tuple-element.30), channel_id=1, source_target_pairs={{0,128},{16,144},{32,160},{48,176},{64,192},{80,208},{96,224},{112... | collective-permute-start | bytes 98312 | tf_op jit(solution)/shard_map/ppermute | solution.py:461
  139.1 8.1 %collective-permute-start.4 = (bf16[64,128]{1,0:T(8,128)(2,1)S(1)}, bf16[64,128]{1,0:T(8,128)(2,1)S(1)}, u32[]{:S(2)}, u32[]{:S(2)}) collective-permute-start(bf16[64,128]{1,0:T(8,128)(2,1)S(1)} %get-tuple-element.32), channel_id=1, source_target_pairs={{0,256},{16,272},{32,288},{48,304},{64,320},{80,336},{96,352},{112... | collective-permute-start | bytes 49160 | tf_op jit(solution)/shard_map/ppermute | solution.py:461
  149.7 4.8 %collective-permute-start.7 = (bf16[256,128]{1,0:T(8,128)(2,1)S(1)}, bf16[256,128]{1,0:T(8,128)(2,1)S(1)}, u32[]{:S(2)}, u32[]{:S(2)}) collective-permute-start(bf16[256,128]{1,0:T(8,128)(2,1)S(1)} %shard_map.154.m0), channel_id=1, source_target_pairs={{0,12},{4,0},{8,4},{12,8},{1,13},{5,1},{9,5},{13,9},{2,14},{6,2},{... | collective-permute-start | bytes 196616 | tf_op jit(solution)/shard_map/ppermute | solution.py:392
  154.5 2.5 %collective-permute-start.6 = (bf16[256,128]{1,0:T(8,128)(2,1)S(1)}, bf16[256,128]{1,0:T(8,128)(2,1)S(1)}, u32[]{:S(2)}, u32[]{:S(2)}) collective-permute-start(bf16[256,128]{1,0:T(8,128)(2,1)S(1)} %shard_map.154.m0), channel_id=1, source_target_pairs={{0,8},{4,12},{8,0},{12,4},{1,9},{5,13},{9,1},{13,5},{2,10},{6,14},... | collective-permute-start | bytes 196616 | tf_op jit(solution)/shard_map/ppermute | solution.py:392
  156.9 2.5 %collective-permute-start.5 = (bf16[256,128]{1,0:T(8,128)(2,1)S(1)}, bf16[256,128]{1,0:T(8,128)(2,1)S(1)}, u32[]{:S(2)}, u32[]{:S(2)}) collective-permute-start(bf16[256,128]{1,0:T(8,128)(2,1)S(1)} %shard_map.154.m0), channel_id=1, source_target_pairs={{0,4},{4,8},{8,12},{12,0},{1,5},{5,9},{9,13},{13,1},{2,6},{6,10},{... | collective-permute-start | bytes 196616 | tf_op jit(solution)/shard_map/ppermute | solution.py:392
  159.4 1.5 collective-permute-done.6.m2
  161.0 2.2 collective-permute-done.5.m1
  163.6 3.1 %collective-permute-start.11 = (bf16[4,16,1024]{2,1,0:T(8,128)(2,1)S(1)}, bf16[4,16,1024]{2,1,0:T(8,128)(2,1)S(1)}, u32[]{:S(2)}, u32[]{:S(2)}) collective-permute-start(bf16[4,16,1024]{2,1,0:T(8,128)(2,1)S(1)} %get-tuple-element.40), channel_id=1, source_target_pairs={{0,1},{1,2},{2,3},{3,0},{4,5},{5,6},{6,7},{7,4},{8,9},{9,10},{10,1... | collective-permute-start | bytes 393224 | tf_op jit(solution)/shard_map/ppermute | solution.py:392
  166.7 4.3 %collective-permute-start.12 = (bf16[4,16,1024]{2,1,0:T(8,128)(2,1)S(1)}, bf16[4,16,1024]{2,1,0:T(8,128)(2,1)S(1)}, u32[]{:S(2)}, u32[]{:S(2)}) collective-permute-start(bf16[4,16,1024]{2,1,0:T(8,128)(2,1)S(1)} %get-tuple-element.41), channel_id=1, source_target_pairs={{0,2},{1,3},{2,0},{3,1},{4,6},{5,7},{6,4},{7,5},{8,10},{9,11},{10,... | collective-permute-start | bytes 393224 | tf_op jit(solution)/shard_map/ppermute | solution.py:392
  171.1 3.1 %collective-permute-start.13 = (bf16[4,16,1024]{2,1,0:T(8,128)(2,1)S(1)}, bf16[4,16,1024]{2,1,0:T(8,128)(2,1)S(1)}, u32[]{:S(2)}, u32[]{:S(2)}) collective-permute-start(bf16[4,16,1024]{2,1,0:T(8,128)(2,1)S(1)} %get-tuple-element.42), channel_id=1, source_target_pairs={{0,3},{1,0},{2,1},{3,2},{4,7},{5,4},{6,5},{7,6},{8,11},{9,8},{10,9... | collective-permute-start | bytes 393224 | tf_op jit(solution)/shard_map/ppermute | solution.py:392
  174.2 2.6 %collective-permute-done.13.p3 = bf16[4,16,1024]{2,1,0:T(8,128)(2,1)S(1)} collective-permute-done((bf16[4,16,1024]{2,1,0:T(8,128)(2,1)S(1)}, bf16[4,16,1024]{2,1,0:T(8,128)(2,1)S(1)}, u32[]{:S(2)}, u32[]{:S(2)}) %collective-permute-start.13) | collective-permute-done | bytes 131104 | tf_op jit(solution)/shard_map/ppermute | solution.py:392
  177.5 3.3 %all-to-all-start = ((bf16[4,16,1024]{2,1,0:T(8,128)(2,1)}), bf16[4,16,1024]{2,1,0:T(8,128)(2,1)S(1)}, u32[]{:S(2)}, u32[]{:S(2)}) async-start(bf16[4,16,1024]{2,1,0:T(8,128)(2,1)} %shard_map.157), calls=%async_computation | async-start | bytes 262144 | tf_op jit(solution)/shard_map/all_to_all | solution.py:192
  181.9 2.1 shard_map.163
  184.0 1.6 all-to-all-done.tiles
  185.6 24.3 %all-to-all-start.5 = ((bf16[32,40,128]{2,1,0:T(8,128)(2,1)}), bf16[32,40,128]{2,1,0:T(8,128)(2,1)S(1)}, u32[]{:S(2)}, u32[]{:S(2)}) async-start(bf16[32,40,128]{2,1,0:T(8,128)(2,1)} %bitcast.15), calls=%async_computation.5 | async-start | bytes 655360 | tf_op jit(solution)/shard_map/all_to_all | solution.py:192
  210.6 24.3 %all-to-all-done.5 = bf16[32,40,128]{2,1,0:T(8,128)(2,1)S(1)} async-done(((bf16[32,40,128]{2,1,0:T(8,128)(2,1)}), bf16[32,40,128]{2,1,0:T(8,128)(2,1)S(1)}, u32[]{:S(2)}, u32[]{:S(2)}) %all-to-all-start.5) | async-done | bytes 327712 | tf_op jit(solution)/shard_map/all_to_all | solution.py:192
  (50 shorter events, 21.6 us)
Async XLA Ops:
  46.5 4.2 %copy-start = (bf16[128,4096]{1,0:T(8,128)(2,1)S(1)}, bf16[128,4096]{1,0:T(8,128)(2,1)}, u32[]{:S(2)}) copy-start(bf16[128,4096]{1,0:T(8,128)(2,1)} %out_weight.1) | copy-start | bytes 3145732
  46.5 4.2 %copy-start.1 = (bf16[1,4096,64]{1,2,0:T(8,128)(2,1)S(1)}, bf16[1,4096,64]{1,2,0:T(8,128)(2,1)}, u32[]{:S(2)}) copy-start(bf16[1,4096,64]{1,2,0:T(8,128)(2,1)} %param.25) | copy-start | bytes 1572868
  46.5 35.1 %all-to-all-start.2 = ((bf16[4,1280,128]{2,1,0:T(8,128)(2,1)}), bf16[4,1280,128]{2,1,0:T(8,128)(2,1)S(1)}, u32[]{:S(2)}, u32[]{:S(2)}) async-start(bf16[4,1280,128]{2,1,0:T(8,128)(2,1)} %shard_map.160), calls=%async_computation.2 | async-start | bytes 2621440 | tf_op jit(solution)/shard_map/all_to_all | solution.py:192
  50.7 1.0 copy-start.2
  51.9 15.7 %collective-permute-start.8 = (bf16[256,1024]{1,0:T(8,128)(2,1)S(1)}, bf16[256,1024]{1,0:T(8,128)(2,1)S(1)}, u32[]{:S(2)}, u32[]{:S(2)}) collective-permute-start(bf16[256,1024]{1,0:T(8,128)(2,1)S(1)} %get-tuple-element.36), channel_id=1, source_target_pairs={{0,4},{4,8},{8,12},{12,0},{1,5},{5,9},{9,13},{13,1},{2,6},{6,10},{... | collective-permute-start | bytes 1572872 | tf_op jit(solution)/shard_map/ppermute | solution.py:392
  55.1 24.9 %collective-permute-start.9 = (bf16[256,1024]{1,0:T(8,128)(2,1)S(1)}, bf16[256,1024]{1,0:T(8,128)(2,1)S(1)}, u32[]{:S(2)}, u32[]{:S(2)}) collective-permute-start(bf16[256,1024]{1,0:T(8,128)(2,1)S(1)} %get-tuple-element.37), channel_id=1, source_target_pairs={{0,8},{4,12},{8,0},{12,4},{1,9},{5,13},{9,1},{13,5},{2,10},{6,14},... | collective-permute-start | bytes 1572872 | tf_op jit(solution)/shard_map/ppermute | solution.py:392
  59.6 22.0 %collective-permute-start.10 = (bf16[256,1024]{1,0:T(8,128)(2,1)S(1)}, bf16[256,1024]{1,0:T(8,128)(2,1)S(1)}, u32[]{:S(2)}, u32[]{:S(2)}) collective-permute-start(bf16[256,1024]{1,0:T(8,128)(2,1)S(1)} %get-tuple-element.38), channel_id=1, source_target_pairs={{0,12},{4,0},{8,4},{12,8},{1,13},{5,1},{9,5},{13,9},{2,14},{6,2},{... | collective-permute-start | bytes 1572872 | tf_op jit(solution)/shard_map/ppermute | solution.py:392
  99.3 48.8 %copy-start.13 = (f32[128]{0:T(128)S(1)}, f32[128]{0:T(128)}, u32[]{:S(2)}) copy-start(f32[128]{0:T(128)} %param.19) | copy-start | bytes 1540
  99.3 78.2 %all-to-all-start.4 = ((bf16[16,160,256]{2,1,0:T(8,128)(2,1)}), bf16[16,160,256]{2,1,0:T(8,128)(2,1)S(1)}, u32[]{:S(2)}, u32[]{:S(2)}) async-start(bf16[16,160,256]{2,1,0:T(8,128)(2,1)} %shard_map.162), calls=%async_computation.4 | async-start | bytes 2621440 | tf_op jit(solution)/shard_map/all_to_all | solution.py:192
  104.4 0.8 copy-start.6
  105.2 0.8 copy-start.7
  106.0 0.8 copy-start.8
  106.9 0.8 copy-start.9
  107.7 0.8 copy-start.10
  115.2 0.7 copy-start.4
  115.9 4.7 %collective-permute-start = (bf16[2,64,128]{2,1,0:T(8,128)(2,1)}, bf16[2,64,128]{2,1,0:T(8,128)(2,1)}, u32[]{:S(2)}, u32[]{:S(2)}) collective-permute-start(bf16[2,64,128]{2,1,0:T(8,128)(2,1)} %get-tuple-element.24), channel_id=1, source_target_pairs={{0,16},{16,32},{32,48},{48,64},{64,80},{80,96},{96,112},{112,128},... | collective-permute-start | bytes 98312 | tf_op jit(solution)/shard_map/ppermute | solution.py:461
  121.6 4.4 %collective-permute-start.1 = (bf16[2,64,128]{2,1,0:T(8,128)(2,1)S(1)}, bf16[2,64,128]{2,1,0:T(8,128)(2,1)S(1)}, u32[]{:S(2)}, u32[]{:S(2)}) collective-permute-start(bf16[2,64,128]{2,1,0:T(8,128)(2,1)S(1)} %get-tuple-element.26), channel_id=1, source_target_pairs={{0,32},{16,48},{32,64},{48,80},{64,96},{80,112},{96,128},{112,144}... | collective-permute-start | bytes 98312 | tf_op jit(solution)/shard_map/ppermute | solution.py:461
  126.1 4.4 %collective-permute-start.2 = (bf16[2,64,128]{2,1,0:T(8,128)(2,1)S(1)}, bf16[2,64,128]{2,1,0:T(8,128)(2,1)S(1)}, u32[]{:S(2)}, u32[]{:S(2)}) collective-permute-start(bf16[2,64,128]{2,1,0:T(8,128)(2,1)S(1)} %get-tuple-element.28), channel_id=1, source_target_pairs={{0,64},{16,80},{32,96},{48,112},{64,128},{80,144},{96,160},{112,17... | collective-permute-start | bytes 98312 | tf_op jit(solution)/shard_map/ppermute | solution.py:461
  130.7 8.2 %collective-permute-start.3 = (bf16[2,64,128]{2,1,0:T(8,128)(2,1)S(1)}, bf16[2,64,128]{2,1,0:T(8,128)(2,1)S(1)}, u32[]{:S(2)}, u32[]{:S(2)}) collective-permute-start(bf16[2,64,128]{2,1,0:T(8,128)(2,1)S(1)} %get-tuple-element.30), channel_id=1, source_target_pairs={{0,128},{16,144},{32,160},{48,176},{64,192},{80,208},{96,224},{112... | collective-permute-start | bytes 98312 | tf_op jit(solution)/shard_map/ppermute | solution.py:461
  139.1 9.0 %collective-permute-start.4 = (bf16[64,128]{1,0:T(8,128)(2,1)S(1)}, bf16[64,128]{1,0:T(8,128)(2,1)S(1)}, u32[]{:S(2)}, u32[]{:S(2)}) collective-permute-start(bf16[64,128]{1,0:T(8,128)(2,1)S(1)} %get-tuple-element.32), channel_id=1, source_target_pairs={{0,256},{16,272},{32,288},{48,304},{64,320},{80,336},{96,352},{112... | collective-permute-start | bytes 49160 | tf_op jit(solution)/shard_map/ppermute | solution.py:461
  148.1 1.0 copy-start.5
  149.7 9.8 %collective-permute-start.7 = (bf16[256,128]{1,0:T(8,128)(2,1)S(1)}, bf16[256,128]{1,0:T(8,128)(2,1)S(1)}, u32[]{:S(2)}, u32[]{:S(2)}) collective-permute-start(bf16[256,128]{1,0:T(8,128)(2,1)S(1)} %shard_map.154.m0), channel_id=1, source_target_pairs={{0,12},{4,0},{8,4},{12,8},{1,13},{5,1},{9,5},{13,9},{2,14},{6,2},{... | collective-permute-start | bytes 196616 | tf_op jit(solution)/shard_map/ppermute | solution.py:392
  154.5 6.5 %collective-permute-start.6 = (bf16[256,128]{1,0:T(8,128)(2,1)S(1)}, bf16[256,128]{1,0:T(8,128)(2,1)S(1)}, u32[]{:S(2)}, u32[]{:S(2)}) collective-permute-start(bf16[256,128]{1,0:T(8,128)(2,1)S(1)} %shard_map.154.m0), channel_id=1, source_target_pairs={{0,8},{4,12},{8,0},{12,4},{1,9},{5,13},{9,1},{13,5},{2,10},{6,14},... | collective-permute-start | bytes 196616 | tf_op jit(solution)/shard_map/ppermute | solution.py:392
  156.9 6.2 %collective-permute-start.5 = (bf16[256,128]{1,0:T(8,128)(2,1)S(1)}, bf16[256,128]{1,0:T(8,128)(2,1)S(1)}, u32[]{:S(2)}, u32[]{:S(2)}) collective-permute-start(bf16[256,128]{1,0:T(8,128)(2,1)S(1)} %shard_map.154.m0), channel_id=1, source_target_pairs={{0,4},{4,8},{8,12},{12,0},{1,5},{5,9},{9,13},{13,1},{2,6},{6,10},{... | collective-permute-start | bytes 196616 | tf_op jit(solution)/shard_map/ppermute | solution.py:392
  163.6 10.5 %collective-permute-start.11 = (bf16[4,16,1024]{2,1,0:T(8,128)(2,1)S(1)}, bf16[4,16,1024]{2,1,0:T(8,128)(2,1)S(1)}, u32[]{:S(2)}, u32[]{:S(2)}) collective-permute-start(bf16[4,16,1024]{2,1,0:T(8,128)(2,1)S(1)} %get-tuple-element.40), channel_id=1, source_target_pairs={{0,1},{1,2},{2,3},{3,0},{4,5},{5,6},{6,7},{7,4},{8,9},{9,10},{10,1... | collective-permute-start | bytes 393224 | tf_op jit(solution)/shard_map/ppermute | solution.py:392
  166.7 7.4 %collective-permute-start.12 = (bf16[4,16,1024]{2,1,0:T(8,128)(2,1)S(1)}, bf16[4,16,1024]{2,1,0:T(8,128)(2,1)S(1)}, u32[]{:S(2)}, u32[]{:S(2)}) collective-permute-start(bf16[4,16,1024]{2,1,0:T(8,128)(2,1)S(1)} %get-tuple-element.41), channel_id=1, source_target_pairs={{0,2},{1,3},{2,0},{3,1},{4,6},{5,7},{6,4},{7,5},{8,10},{9,11},{10,... | collective-permute-start | bytes 393224 | tf_op jit(solution)/shard_map/ppermute | solution.py:392
  171.1 5.7 %collective-permute-start.13 = (bf16[4,16,1024]{2,1,0:T(8,128)(2,1)S(1)}, bf16[4,16,1024]{2,1,0:T(8,128)(2,1)S(1)}, u32[]{:S(2)}, u32[]{:S(2)}) collective-permute-start(bf16[4,16,1024]{2,1,0:T(8,128)(2,1)S(1)} %get-tuple-element.42), channel_id=1, source_target_pairs={{0,3},{1,0},{2,1},{3,2},{4,7},{5,4},{6,5},{7,6},{8,11},{9,8},{10,9... | collective-permute-start | bytes 393224 | tf_op jit(solution)/shard_map/ppermute | solution.py:392
  177.5 8.1 %all-to-all-start = ((bf16[4,16,1024]{2,1,0:T(8,128)(2,1)}), bf16[4,16,1024]{2,1,0:T(8,128)(2,1)S(1)}, u32[]{:S(2)}, u32[]{:S(2)}) async-start(bf16[4,16,1024]{2,1,0:T(8,128)(2,1)} %shard_map.157), calls=%async_computation | async-start | bytes 262144 | tf_op jit(solution)/shard_map/all_to_all | solution.py:192
  180.8 1.0 copy-start.3
  181.9 53.0 %copy-start.11 = (f32[32,128]{1,0:T(8,128)S(1)}, f32[32,128]{1,0:T(8,128)}, u32[]{:S(2)}) copy-start(f32[32,128]{1,0:T(8,128)} %get-tuple-element.44.rank) | copy-start | bytes 49156
  181.9 53.0 %copy-start.12 = (f32[32,128]{1,0:T(8,128)S(1)}, f32[32,128]{1,0:T(8,128)}, u32[]{:S(2)}) copy-start(f32[32,128]{1,0:T(8,128)} %get-tuple-element.45.share) | copy-start | bytes 49156
  185.6 49.3 %all-to-all-start.5 = ((bf16[32,40,128]{2,1,0:T(8,128)(2,1)}), bf16[32,40,128]{2,1,0:T(8,128)(2,1)S(1)}, u32[]{:S(2)}, u32[]{:S(2)}) async-start(bf16[32,40,128]{2,1,0:T(8,128)(2,1)} %bitcast.15), calls=%async_computation.5 | async-start | bytes 655360 | tf_op jit(solution)/shard_map/all_to_all | solution.py:192

commit v5 on v4

--- a/solution.py
+++ b/solution.py
@@ -52,12 +52,12 @@
     return dot(ah, bh, dims) + dot(ah, bl, dims) + dot(al, bh, dims)
 
 
-def call(kernel, outs, *args, scalars=0, scratch=(), limit=LIMIT):
+def call(kernel, outs, *args, scalars=0, scratch=(), limit=LIMIT, space=pltpu.SMEM):
     whole = [pl.BlockSpec(memory_space=pltpu.VMEM)] * (len(args) - scalars)
     return pl.pallas_call(
         kernel,
         out_shape=outs,
-        in_specs=[pl.BlockSpec(memory_space=pltpu.SMEM)] * scalars + whole,
+        in_specs=[pl.BlockSpec(memory_space=space)] * scalars + whole,
         scratch_shapes=list(scratch),
         compiler_params=pltpu.CompilerParams(vmem_limit_bytes=limit),
     )(*args)
@@ -162,8 +162,11 @@
             out[peer, :, k * 128 : (k + 1) * 128] = value.astype(jnp.bfloat16)
 
 
-def down_kernel(hidden, weights, out):
+def down_kernel(stored, hidden, out, weights, done):
+    fetch = pltpu.make_async_copy(stored, weights, done)
+    fetch.start()
     picks = (selector(0), selector(1))
+    fetch.wait()
     side = 4
     tall = []
     for k in range(side):
@@ -513,7 +516,18 @@
     parts = exchanged(partial, "tp_y")
     hidden = call(hidden_kernel, shape((tp, share_rows, wide // 2)), parts)
     everyone = exchanged(hidden, TP)
-    result = call(down_kernel, shape((total, 128)), everyone, down_weight[0])
+    result = call(
+        down_kernel,
+        shape((total, 128)),
+        down_weight[0],
+        everyone,
+        scalars=1,
+        space=pl.ANY,
+        scratch=[
+            pltpu.VMEM(down_weight.shape[1:], jnp.bfloat16),
+            pltpu.SemaphoreType.DMA(()),
+        ],
+    )
     returned = exchanged(result.reshape(EXPERTS, SLOT, 128), EP)
     tiles = exchanged(added, "tp_y")
     moe_out = call(combine_kernel, shape((rows, width)), returned.reshape(total, 128), rank, share)

time: 238 us -> 238 us (level)
  transfers between devices with their start and end apart: 18 -> 18, of which waited for: 13 -> 13; matrix products, arithmetic and copies ran while one was open for 0% -> 0% of each run, Pallas kernels for 5% -> 6%
where the time goes in v5:
time: 238 us; the launch traced here: 236 us
  starting transfers between devices  93.1 us (39%)
  waiting for transfers between devices  56.3 us (24%)
  blocking collectives  55.9 us (23%)
  Pallas kernels  22.2 us (9%)
  local copies, waits for them, and re-layouts  7.95 us (3%)
    all_to_all x2, blocking collectives, exchanged(): return lax.all_to_all(tiles, axis, split_axis=0, concat_axis=0, tiled=True)  55.9 us
    all_to_all x4, starting transfers between devices, exchanged(): return lax.all_to_all(tiles, axis, split_axis=0, concat_axis=0, tiled=True)  36.8 us
    ppermute x9, starting transfers between devices, turned(): return lax.ppermute(shard, axis, [(i, (i + back) % n) for i in range(n)])  30.9 us
    all_to_all x4, waiting for transfers between devices, exchanged(): return lax.all_to_all(tiles, axis, split_axis=0, concat_axis=0, tiled=True)  25.8 us
    ppermute x5, starting transfers between devices, local(): lax.ppermute(send, EP, [(i, i + shift) for i in range(peers - shift)])  25.4 us
    ppermute x9, waiting for transfers between devices, turned(): return lax.ppermute(shard, axis, [(i, (i + back) % n) for i in range(n)])  25.3 us
    pallas_call x16, Pallas kernels, call(): pl.pallas_call(kernel, out_shape=outs, in_specs=[pl.BlockSpec(memory_spac...  22.2 us
    unnamed x28, local copies, waits for them, and re-layouts  7.95 us
  transfers between devices with their start and end apart: 18, of which 13 were waited for; matrix products, arithmetic and copies ran while one was open for 0% of the time, Pallas kernels for 6%

profile of v5, /device:TPU:1, one launch (start us, length us, event | category | flops | bytes accessed | tf_op | source)
XLA Modules:
  0.0 236.4 jit_solution(2689541887362133516)
XLA Ops:
  0.6 2.9 %shard_map.159 = (bf16[1280,128]{1,0:T(8,128)(2,1)}, f32[32,128]{1,0:T(8,128)}, f32[32,128]{1,0:T(8,128)}) custom-call(s32[1]{0:T(128)} %bitcast.9.place, bf16[128,4096]{1,0:T(8,128)(2,1)} %x.1, f32[1,4096]{1,0:T(1,128)} %bitcast.26, s32[4,128]{1,0:T(4,128)} %bitcast.27, f32[4,128]{1,0:T(4,128)} %bitcast.28), custom_call_target="tpu_custom_call" | custom-call | tf_op jit(solution)/shard_map/pallas_call | solution.py:57
  3.5 41.7 %all_to_all.30 = bf16[32,40,128]{2,1,0:T(8,128)(2,1)S(1)} all-to-all(bf16[32,40,128]{2,1,0:T(8,128)(2,1)} %bitcast.25), channel_id=1, replica_groups=mesh['ep_0'=16,'ep_1'=2,'tp_y'=4,'tp_x'=4] {'ep_0','ep_1'}, dimensions={0} | all-to-all | bytes 655360 | tf_op jit(solution)/shard_map/all_to_all | solution.py:195
  46.5 4.1 %all-to-all-start.2 = ((bf16[4,1280,128]{2,1,0:T(8,128)(2,1)}), bf16[4,1280,128]{2,1,0:T(8,128)(2,1)S(1)}, u32[]{:S(2)}, u32[]{:S(2)}) async-start(bf16[4,1280,128]{2,1,0:T(8,128)(2,1)} %shard_map.160), calls=%async_computation.2 | async-start | bytes 2621440 | tf_op jit(solution)/shard_map/all_to_all | solution.py:195
  51.9 3.2 %collective-permute-start.8 = (bf16[256,1024]{1,0:T(8,128)(2,1)S(1)}, bf16[256,1024]{1,0:T(8,128)(2,1)S(1)}, u32[]{:S(2)}, u32[]{:S(2)}) collective-permute-start(bf16[256,1024]{1,0:T(8,128)(2,1)S(1)} %get-tuple-element.36), channel_id=1, source_target_pairs={{0,4},{4,8},{8,12},{12,0},{1,5},{5,9},{9,13},{13,1},{2,6},{6,10},{... | collective-permute-start | bytes 1572872 | tf_op jit(solution)/shard_map/ppermute | solution.py:395
  55.1 4.5 %collective-permute-start.9 = (bf16[256,1024]{1,0:T(8,128)(2,1)S(1)}, bf16[256,1024]{1,0:T(8,128)(2,1)S(1)}, u32[]{:S(2)}, u32[]{:S(2)}) collective-permute-start(bf16[256,1024]{1,0:T(8,128)(2,1)S(1)} %get-tuple-element.37), channel_id=1, source_target_pairs={{0,8},{4,12},{8,0},{12,4},{1,9},{5,13},{9,1},{13,5},{2,10},{6,14},... | collective-permute-start | bytes 1572872 | tf_op jit(solution)/shard_map/ppermute | solution.py:395
  59.6 3.0 %collective-permute-start.10 = (bf16[256,1024]{1,0:T(8,128)(2,1)S(1)}, bf16[256,1024]{1,0:T(8,128)(2,1)S(1)}, u32[]{:S(2)}, u32[]{:S(2)}) collective-permute-start(bf16[256,1024]{1,0:T(8,128)(2,1)S(1)} %get-tuple-element.38), channel_id=1, source_target_pairs={{0,12},{4,0},{8,4},{12,8},{1,13},{5,1},{9,5},{13,9},{2,14},{6,2},{... | collective-permute-start | bytes 1572872 | tf_op jit(solution)/shard_map/ppermute | solution.py:395
  62.6 5.0 %collective-permute-done.8.w1 = bf16[256,1024]{1,0:T(8,128)(2,1)S(1)} collective-permute-done((bf16[256,1024]{1,0:T(8,128)(2,1)S(1)}, bf16[256,1024]{1,0:T(8,128)(2,1)S(1)}, u32[]{:S(2)}, u32[]{:S(2)}) %collective-permute-start.8) | collective-permute-done | bytes 524320 | tf_op jit(solution)/shard_map/ppermute | solution.py:395
  67.6 12.3 %collective-permute-done.9.w2 = bf16[256,1024]{1,0:T(8,128)(2,1)S(1)} collective-permute-done((bf16[256,1024]{1,0:T(8,128)(2,1)S(1)}, bf16[256,1024]{1,0:T(8,128)(2,1)S(1)}, u32[]{:S(2)}, u32[]{:S(2)}) %collective-permute-start.9) | collective-permute-done | bytes 524320 | tf_op jit(solution)/shard_map/ppermute | solution.py:395
  79.9 1.7 collective-permute-done.10.w3
  81.6 1.9 shard_map.161
  83.6 14.2 %all_to_all.31.parts = bf16[4,160,512]{2,1,0:T(8,128)(2,1)S(1)} all-to-all(bf16[4,160,512]{2,1,0:T(8,128)(2,1)S(1)} %shard_map.161), channel_id=1, replica_groups=mesh['ep_0'=16,'ep_1'=2,'tp_y'=4,'tp_x'=4] {'tp_y'}, dimensions={0} | all-to-all | bytes 1310720 | tf_op jit(solution)/shard_map/all_to_all | solution.py:195
  97.7 1.5 shard_map.162
  99.3 5.1 %all-to-all-start.4 = ((bf16[16,160,256]{2,1,0:T(8,128)(2,1)}), bf16[16,160,256]{2,1,0:T(8,128)(2,1)S(1)}, u32[]{:S(2)}, u32[]{:S(2)}) async-start(bf16[16,160,256]{2,1,0:T(8,128)(2,1)} %shard_map.162), calls=%async_computation.4 | async-start | bytes 2621440 | tf_op jit(solution)/shard_map/all_to_all | solution.py:195
  108.6 6.6 %shard_map.149 = (f32[2,128,128]{2,1,0:T(8,128)S(1)}, bf16[2,64,128]{2,1,0:T(8,128)(2,1)}, f32[2,256,128]{2,1,0:T(8,128)S(1)}) custom-call(bf16[256,128]{1,0:T(8,128)(2,1)S(1)} %copy-done.6, bf16[256,128]{1,0:T(8,128)(2,1)S(1)} %copy-done.7, bf16[256,128]{1,0:T(8,128)(2,1)S(1)} %copy-done.8, bf16[256,128]{1,0:T(8,128)(2,1)S(1)} %copy-done.9, ...), custom_call_target="tpu_custom_call" | custom-call | tf_op jit(solution)/shard_map/pallas_call | solution.py:57
  115.9 3.3 %collective-permute-start = (bf16[2,64,128]{2,1,0:T(8,128)(2,1)}, bf16[2,64,128]{2,1,0:T(8,128)(2,1)}, u32[]{:S(2)}, u32[]{:S(2)}) collective-permute-start(bf16[2,64,128]{2,1,0:T(8,128)(2,1)} %get-tuple-element.24), channel_id=1, source_target_pairs={{0,16},{16,32},{32,48},{48,64},{64,80},{80,96},{96,112},{112,128},... | collective-permute-start | bytes 98312 | tf_op jit(solution)/shard_map/ppermute | solution.py:464
  121.6 3.3 %collective-permute-start.1 = (bf16[2,64,128]{2,1,0:T(8,128)(2,1)S(1)}, bf16[2,64,128]{2,1,0:T(8,128)(2,1)S(1)}, u32[]{:S(2)}, u32[]{:S(2)}) collective-permute-start(bf16[2,64,128]{2,1,0:T(8,128)(2,1)S(1)} %get-tuple-element.26), channel_id=1, source_target_pairs={{0,32},{16,48},{32,64},{48,80},{64,96},{80,112},{96,128},{112,144}... | collective-permute-start | bytes 98312 | tf_op jit(solution)/shard_map/ppermute | solution.py:464
  126.1 3.4 %collective-permute-start.2 = (bf16[2,64,128]{2,1,0:T(8,128)(2,1)S(1)}, bf16[2,64,128]{2,1,0:T(8,128)(2,1)S(1)}, u32[]{:S(2)}, u32[]{:S(2)}) collective-permute-start(bf16[2,64,128]{2,1,0:T(8,128)(2,1)S(1)} %get-tuple-element.28), channel_id=1, source_target_pairs={{0,64},{16,80},{32,96},{48,112},{64,128},{80,144},{96,160},{112,17... | collective-permute-start | bytes 98312 | tf_op jit(solution)/shard_map/ppermute | solution.py:464
  130.7 7.2 %collective-permute-start.3 = (bf16[2,64,128]{2,1,0:T(8,128)(2,1)S(1)}, bf16[2,64,128]{2,1,0:T(8,128)(2,1)S(1)}, u32[]{:S(2)}, u32[]{:S(2)}) collective-permute-start(bf16[2,64,128]{2,1,0:T(8,128)(2,1)S(1)} %get-tuple-element.30), channel_id=1, source_target_pairs={{0,128},{16,144},{32,160},{48,176},{64,192},{80,208},{96,224},{112... | collective-permute-start | bytes 98312 | tf_op jit(solution)/shard_map/ppermute | solution.py:464
  139.1 8.1 %collective-permute-start.4 = (bf16[64,128]{1,0:T(8,128)(2,1)S(1)}, bf16[64,128]{1,0:T(8,128)(2,1)S(1)}, u32[]{:S(2)}, u32[]{:S(2)}) collective-permute-start(bf16[64,128]{1,0:T(8,128)(2,1)S(1)} %get-tuple-element.32), channel_id=1, source_target_pairs={{0,256},{16,272},{32,288},{48,304},{64,320},{80,336},{96,352},{112... | collective-permute-start | bytes 49160 | tf_op jit(solution)/shard_map/ppermute | solution.py:464
  149.7 4.8 %collective-permute-start.7 = (bf16[256,128]{1,0:T(8,128)(2,1)S(1)}, bf16[256,128]{1,0:T(8,128)(2,1)S(1)}, u32[]{:S(2)}, u32[]{:S(2)}) collective-permute-start(bf16[256,128]{1,0:T(8,128)(2,1)S(1)} %shard_map.154.m0), channel_id=1, source_target_pairs={{0,12},{4,0},{8,4},{12,8},{1,13},{5,1},{9,5},{13,9},{2,14},{6,2},{... | collective-permute-start | bytes 196616 | tf_op jit(solution)/shard_map/ppermute | solution.py:395
  154.5 2.5 %collective-permute-start.6 = (bf16[256,128]{1,0:T(8,128)(2,1)S(1)}, bf16[256,128]{1,0:T(8,128)(2,1)S(1)}, u32[]{:S(2)}, u32[]{:S(2)}) collective-permute-start(bf16[256,128]{1,0:T(8,128)(2,1)S(1)} %shard_map.154.m0), channel_id=1, source_target_pairs={{0,8},{4,12},{8,0},{12,4},{1,9},{5,13},{9,1},{13,5},{2,10},{6,14},... | collective-permute-start | bytes 196616 | tf_op jit(solution)/shard_map/ppermute | solution.py:395
  156.9 2.5 %collective-permute-start.5 = (bf16[256,128]{1,0:T(8,128)(2,1)S(1)}, bf16[256,128]{1,0:T(8,128)(2,1)S(1)}, u32[]{:S(2)}, u32[]{:S(2)}) collective-permute-start(bf16[256,128]{1,0:T(8,128)(2,1)S(1)} %shard_map.154.m0), channel_id=1, source_target_pairs={{0,4},{4,8},{8,12},{12,0},{1,5},{5,9},{9,13},{13,1},{2,6},{6,10},{... | collective-permute-start | bytes 196616 | tf_op jit(solution)/shard_map/ppermute | solution.py:395
  159.4 1.5 collective-permute-done.6.m2
  161.0 2.2 collective-permute-done.5.m1
  163.6 3.1 %collective-permute-start.11 = (bf16[4,16,1024]{2,1,0:T(8,128)(2,1)S(1)}, bf16[4,16,1024]{2,1,0:T(8,128)(2,1)S(1)}, u32[]{:S(2)}, u32[]{:S(2)}) collective-permute-start(bf16[4,16,1024]{2,1,0:T(8,128)(2,1)S(1)} %get-tuple-element.40), channel_id=1, source_target_pairs={{0,1},{1,2},{2,3},{3,0},{4,5},{5,6},{6,7},{7,4},{8,9},{9,10},{10,1... | collective-permute-start | bytes 393224 | tf_op jit(solution)/shard_map/ppermute | solution.py:395
  166.7 4.3 %collective-permute-start.12 = (bf16[4,16,1024]{2,1,0:T(8,128)(2,1)S(1)}, bf16[4,16,1024]{2,1,0:T(8,128)(2,1)S(1)}, u32[]{:S(2)}, u32[]{:S(2)}) collective-permute-start(bf16[4,16,1024]{2,1,0:T(8,128)(2,1)S(1)} %get-tuple-element.41), channel_id=1, source_target_pairs={{0,2},{1,3},{2,0},{3,1},{4,6},{5,7},{6,4},{7,5},{8,10},{9,11},{10,... | collective-permute-start | bytes 393224 | tf_op jit(solution)/shard_map/ppermute | solution.py:395
  171.1 3.1 %collective-permute-start.13 = (bf16[4,16,1024]{2,1,0:T(8,128)(2,1)S(1)}, bf16[4,16,1024]{2,1,0:T(8,128)(2,1)S(1)}, u32[]{:S(2)}, u32[]{:S(2)}) collective-permute-start(bf16[4,16,1024]{2,1,0:T(8,128)(2,1)S(1)} %get-tuple-element.42), channel_id=1, source_target_pairs={{0,3},{1,0},{2,1},{3,2},{4,7},{5,4},{6,5},{7,6},{8,11},{9,8},{10,9... | collective-permute-start | bytes 393224 | tf_op jit(solution)/shard_map/ppermute | solution.py:395
  174.2 2.6 %collective-permute-done.13.p3 = bf16[4,16,1024]{2,1,0:T(8,128)(2,1)S(1)} collective-permute-done((bf16[4,16,1024]{2,1,0:T(8,128)(2,1)S(1)}, bf16[4,16,1024]{2,1,0:T(8,128)(2,1)S(1)}, u32[]{:S(2)}, u32[]{:S(2)}) %collective-permute-start.13) | collective-permute-done | bytes 131104 | tf_op jit(solution)/shard_map/ppermute | solution.py:395
  177.5 3.3 %all-to-all-start = ((bf16[4,16,1024]{2,1,0:T(8,128)(2,1)}), bf16[4,16,1024]{2,1,0:T(8,128)(2,1)S(1)}, u32[]{:S(2)}, u32[]{:S(2)}) async-start(bf16[4,16,1024]{2,1,0:T(8,128)(2,1)} %shard_map.157), calls=%async_computation | async-start | bytes 262144 | tf_op jit(solution)/shard_map/all_to_all | solution.py:195
  181.9 2.3 shard_map.163
  185.6 24.3 %all-to-all-start.5 = ((bf16[32,40,128]{2,1,0:T(8,128)(2,1)}), bf16[32,40,128]{2,1,0:T(8,128)(2,1)S(1)}, u32[]{:S(2)}, u32[]{:S(2)}) async-start(bf16[32,40,128]{2,1,0:T(8,128)(2,1)} %bitcast.15), calls=%async_computation.5 | async-start | bytes 655360 | tf_op jit(solution)/shard_map/all_to_all | solution.py:195
  210.6 24.3 %all-to-all-done.5 = bf16[32,40,128]{2,1,0:T(8,128)(2,1)S(1)} async-done(((bf16[32,40,128]{2,1,0:T(8,128)(2,1)}), bf16[32,40,128]{2,1,0:T(8,128)(2,1)S(1)}, u32[]{:S(2)}, u32[]{:S(2)}) %all-to-all-start.5) | async-done | bytes 327712 | tf_op jit(solution)/shard_map/all_to_all | solution.py:195
  (50 shorter events, 21.5 us)
Async XLA Ops:
  46.5 4.2 %copy-start = (bf16[128,4096]{1,0:T(8,128)(2,1)S(1)}, bf16[128,4096]{1,0:T(8,128)(2,1)}, u32[]{:S(2)}) copy-start(bf16[128,4096]{1,0:T(8,128)(2,1)} %out_weight.1) | copy-start | bytes 3145732
  46.5 4.2 %copy-start.1 = (bf16[1,4096,64]{1,2,0:T(8,128)(2,1)S(1)}, bf16[1,4096,64]{1,2,0:T(8,128)(2,1)}, u32[]{:S(2)}) copy-start(bf16[1,4096,64]{1,2,0:T(8,128)(2,1)} %param.25) | copy-start | bytes 1572868
  46.5 35.1 %all-to-all-start.2 = ((bf16[4,1280,128]{2,1,0:T(8,128)(2,1)}), bf16[4,1280,128]{2,1,0:T(8,128)(2,1)S(1)}, u32[]{:S(2)}, u32[]{:S(2)}) async-start(bf16[4,1280,128]{2,1,0:T(8,128)(2,1)} %shard_map.160), calls=%async_computation.2 | async-start | bytes 2621440 | tf_op jit(solution)/shard_map/all_to_all | solution.py:195
  50.7 1.0 copy-start.2
  51.9 15.7 %collective-permute-start.8 = (bf16[256,1024]{1,0:T(8,128)(2,1)S(1)}, bf16[256,1024]{1,0:T(8,128)(2,1)S(1)}, u32[]{:S(2)}, u32[]{:S(2)}) collective-permute-start(bf16[256,1024]{1,0:T(8,128)(2,1)S(1)} %get-tuple-element.36), channel_id=1, source_target_pairs={{0,4},{4,8},{8,12},{12,0},{1,5},{5,9},{9,13},{13,1},{2,6},{6,10},{... | collective-permute-start | bytes 1572872 | tf_op jit(solution)/shard_map/ppermute | solution.py:395
  55.1 24.9 %collective-permute-start.9 = (bf16[256,1024]{1,0:T(8,128)(2,1)S(1)}, bf16[256,1024]{1,0:T(8,128)(2,1)S(1)}, u32[]{:S(2)}, u32[]{:S(2)}) collective-permute-start(bf16[256,1024]{1,0:T(8,128)(2,1)S(1)} %get-tuple-element.37), channel_id=1, source_target_pairs={{0,8},{4,12},{8,0},{12,4},{1,9},{5,13},{9,1},{13,5},{2,10},{6,14},... | collective-permute-start | bytes 1572872 | tf_op jit(solution)/shard_map/ppermute | solution.py:395
  59.6 22.0 %collective-permute-start.10 = (bf16[256,1024]{1,0:T(8,128)(2,1)S(1)}, bf16[256,1024]{1,0:T(8,128)(2,1)S(1)}, u32[]{:S(2)}, u32[]{:S(2)}) collective-permute-start(bf16[256,1024]{1,0:T(8,128)(2,1)S(1)} %get-tuple-element.38), channel_id=1, source_target_pairs={{0,12},{4,0},{8,4},{12,8},{1,13},{5,1},{9,5},{13,9},{2,14},{6,2},{... | collective-permute-start | bytes 1572872 | tf_op jit(solution)/shard_map/ppermute | solution.py:395
  99.3 48.8 %copy-start.13 = (f32[128]{0:T(128)S(1)}, f32[128]{0:T(128)}, u32[]{:S(2)}) copy-start(f32[128]{0:T(128)} %param.19) | copy-start | bytes 1540
  99.3 78.2 %all-to-all-start.4 = ((bf16[16,160,256]{2,1,0:T(8,128)(2,1)}), bf16[16,160,256]{2,1,0:T(8,128)(2,1)S(1)}, u32[]{:S(2)}, u32[]{:S(2)}) async-start(bf16[16,160,256]{2,1,0:T(8,128)(2,1)} %shard_map.162), calls=%async_computation.4 | async-start | bytes 2621440 | tf_op jit(solution)/shard_map/all_to_all | solution.py:195
  104.4 0.8 copy-start.6
  105.2 0.8 copy-start.7
  106.0 0.8 copy-start.8
  106.9 0.8 copy-start.9
  107.7 0.8 copy-start.10
  115.2 0.7 copy-start.4
  115.9 4.7 %collective-permute-start = (bf16[2,64,128]{2,1,0:T(8,128)(2,1)}, bf16[2,64,128]{2,1,0:T(8,128)(2,1)}, u32[]{:S(2)}, u32[]{:S(2)}) collective-permute-start(bf16[2,64,128]{2,1,0:T(8,128)(2,1)} %get-tuple-element.24), channel_id=1, source_target_pairs={{0,16},{16,32},{32,48},{48,64},{64,80},{80,96},{96,112},{112,128},... | collective-permute-start | bytes 98312 | tf_op jit(solution)/shard_map/ppermute | solution.py:464
  121.6 4.4 %collective-permute-start.1 = (bf16[2,64,128]{2,1,0:T(8,128)(2,1)S(1)}, bf16[2,64,128]{2,1,0:T(8,128)(2,1)S(1)}, u32[]{:S(2)}, u32[]{:S(2)}) collective-permute-start(bf16[2,64,128]{2,1,0:T(8,128)(2,1)S(1)} %get-tuple-element.26), channel_id=1, source_target_pairs={{0,32},{16,48},{32,64},{48,80},{64,96},{80,112},{96,128},{112,144}... | collective-permute-start | bytes 98312 | tf_op jit(solution)/shard_map/ppermute | solution.py:464
  126.1 4.4 %collective-permute-start.2 = (bf16[2,64,128]{2,1,0:T(8,128)(2,1)S(1)}, bf16[2,64,128]{2,1,0:T(8,128)(2,1)S(1)}, u32[]{:S(2)}, u32[]{:S(2)}) collective-permute-start(bf16[2,64,128]{2,1,0:T(8,128)(2,1)S(1)} %get-tuple-element.28), channel_id=1, source_target_pairs={{0,64},{16,80},{32,96},{48,112},{64,128},{80,144},{96,160},{112,17... | collective-permute-start | bytes 98312 | tf_op jit(solution)/shard_map/ppermute | solution.py:464
  130.7 8.2 %collective-permute-start.3 = (bf16[2,64,128]{2,1,0:T(8,128)(2,1)S(1)}, bf16[2,64,128]{2,1,0:T(8,128)(2,1)S(1)}, u32[]{:S(2)}, u32[]{:S(2)}) collective-permute-start(bf16[2,64,128]{2,1,0:T(8,128)(2,1)S(1)} %get-tuple-element.30), channel_id=1, source_target_pairs={{0,128},{16,144},{32,160},{48,176},{64,192},{80,208},{96,224},{112... | collective-permute-start | bytes 98312 | tf_op jit(solution)/shard_map/ppermute | solution.py:464
  139.1 9.0 %collective-permute-start.4 = (bf16[64,128]{1,0:T(8,128)(2,1)S(1)}, bf16[64,128]{1,0:T(8,128)(2,1)S(1)}, u32[]{:S(2)}, u32[]{:S(2)}) collective-permute-start(bf16[64,128]{1,0:T(8,128)(2,1)S(1)} %get-tuple-element.32), channel_id=1, source_target_pairs={{0,256},{16,272},{32,288},{48,304},{64,320},{80,336},{96,352},{112... | collective-permute-start | bytes 49160 | tf_op jit(solution)/shard_map/ppermute | solution.py:464
  148.1 1.0 copy-start.5
  149.7 9.8 %collective-permute-start.7 = (bf16[256,128]{1,0:T(8,128)(2,1)S(1)}, bf16[256,128]{1,0:T(8,128)(2,1)S(1)}, u32[]{:S(2)}, u32[]{:S(2)}) collective-permute-start(bf16[256,128]{1,0:T(8,128)(2,1)S(1)} %shard_map.154.m0), channel_id=1, source_target_pairs={{0,12},{4,0},{8,4},{12,8},{1,13},{5,1},{9,5},{13,9},{2,14},{6,2},{... | collective-permute-start | bytes 196616 | tf_op jit(solution)/shard_map/ppermute | solution.py:395
  154.5 6.5 %collective-permute-start.6 = (bf16[256,128]{1,0:T(8,128)(2,1)S(1)}, bf16[256,128]{1,0:T(8,128)(2,1)S(1)}, u32[]{:S(2)}, u32[]{:S(2)}) collective-permute-start(bf16[256,128]{1,0:T(8,128)(2,1)S(1)} %shard_map.154.m0), channel_id=1, source_target_pairs={{0,8},{4,12},{8,0},{12,4},{1,9},{5,13},{9,1},{13,5},{2,10},{6,14},... | collective-permute-start | bytes 196616 | tf_op jit(solution)/shard_map/ppermute | solution.py:395
  156.9 6.2 %collective-permute-start.5 = (bf16[256,128]{1,0:T(8,128)(2,1)S(1)}, bf16[256,128]{1,0:T(8,128)(2,1)S(1)}, u32[]{:S(2)}, u32[]{:S(2)}) collective-permute-start(bf16[256,128]{1,0:T(8,128)(2,1)S(1)} %shard_map.154.m0), channel_id=1, source_target_pairs={{0,4},{4,8},{8,12},{12,0},{1,5},{5,9},{9,13},{13,1},{2,6},{6,10},{... | collective-permute-start | bytes 196616 | tf_op jit(solution)/shard_map/ppermute | solution.py:395
  163.6 10.5 %collective-permute-start.11 = (bf16[4,16,1024]{2,1,0:T(8,128)(2,1)S(1)}, bf16[4,16,1024]{2,1,0:T(8,128)(2,1)S(1)}, u32[]{:S(2)}, u32[]{:S(2)}) collective-permute-start(bf16[4,16,1024]{2,1,0:T(8,128)(2,1)S(1)} %get-tuple-element.40), channel_id=1, source_target_pairs={{0,1},{1,2},{2,3},{3,0},{4,5},{5,6},{6,7},{7,4},{8,9},{9,10},{10,1... | collective-permute-start | bytes 393224 | tf_op jit(solution)/shard_map/ppermute | solution.py:395
  166.7 7.4 %collective-permute-start.12 = (bf16[4,16,1024]{2,1,0:T(8,128)(2,1)S(1)}, bf16[4,16,1024]{2,1,0:T(8,128)(2,1)S(1)}, u32[]{:S(2)}, u32[]{:S(2)}) collective-permute-start(bf16[4,16,1024]{2,1,0:T(8,128)(2,1)S(1)} %get-tuple-element.41), channel_id=1, source_target_pairs={{0,2},{1,3},{2,0},{3,1},{4,6},{5,7},{6,4},{7,5},{8,10},{9,11},{10,... | collective-permute-start | bytes 393224 | tf_op jit(solution)/shard_map/ppermute | solution.py:395
  171.1 5.7 %collective-permute-start.13 = (bf16[4,16,1024]{2,1,0:T(8,128)(2,1)S(1)}, bf16[4,16,1024]{2,1,0:T(8,128)(2,1)S(1)}, u32[]{:S(2)}, u32[]{:S(2)}) collective-permute-start(bf16[4,16,1024]{2,1,0:T(8,128)(2,1)S(1)} %get-tuple-element.42), channel_id=1, source_target_pairs={{0,3},{1,0},{2,1},{3,2},{4,7},{5,4},{6,5},{7,6},{8,11},{9,8},{10,9... | collective-permute-start | bytes 393224 | tf_op jit(solution)/shard_map/ppermute | solution.py:395
  177.5 8.1 %all-to-all-start = ((bf16[4,16,1024]{2,1,0:T(8,128)(2,1)}), bf16[4,16,1024]{2,1,0:T(8,128)(2,1)S(1)}, u32[]{:S(2)}, u32[]{:S(2)}) async-start(bf16[4,16,1024]{2,1,0:T(8,128)(2,1)} %shard_map.157), calls=%async_computation | async-start | bytes 262144 | tf_op jit(solution)/shard_map/all_to_all | solution.py:195
  180.8 1.0 copy-start.3
  181.9 53.0 %copy-start.11 = (f32[32,128]{1,0:T(8,128)S(1)}, f32[32,128]{1,0:T(8,128)}, u32[]{:S(2)}) copy-start(f32[32,128]{1,0:T(8,128)} %get-tuple-element.44.rank) | copy-start | bytes 49156
  181.9 53.0 %copy-start.12 = (f32[32,128]{1,0:T(8,128)S(1)}, f32[32,128]{1,0:T(8,128)}, u32[]{:S(2)}) copy-start(f32[32,128]{1,0:T(8,128)} %get-tuple-element.45.share) | copy-start | bytes 49156
  185.6 49.3 %all-to-all-start.5 = ((bf16[32,40,128]{2,1,0:T(8,128)(2,1)}), bf16[32,40,128]{2,1,0:T(8,128)(2,1)S(1)}, u32[]{:S(2)}, u32[]{:S(2)}) async-start(bf16[32,40,128]{2,1,0:T(8,128)(2,1)} %bitcast.15), calls=%async_computation.5 | async-start | bytes 655360 | tf_op jit(solution)/shard_map/all_to_all | solution.py:195
